TPU v7x, 256 devices: a whole 4x4x8 slice. The times are simulated.
256 devices in a mesh: sp: 64 (over z, y, core), tp: 4 (over x).
Axes of the slice: x: 4, y: 4, z: 8, core: 2. Of those that a mesh axis runs over, the one named last changes fastest.
Arguments:
- query: bfloat16 [16384, 1024], P('sp', 'tp'), may hold values from -12 to 12
- key_rows: bfloat16 [16384, 512], P('sp', 'tp'), may hold values from -8 to 8
- value_rows: bfloat16 [16384, 512], P('sp', 'tp'), may hold values from -16 to 16
- stream: bfloat16 [16384, 2048], P(('sp', 'tp')), may hold values from -6 to 6
- out_weight: bfloat16 [1024, 2048], P('tp'), may hold values from -0.1875 to 0.1875
- norm_gain: float32 [2048], replicated, may hold values from 0.1 to 1.9
- route_ids: int32 [16384, 4], P(('sp', 'tp')), may hold values from 0 to 63, all different within a row; in each aligned block of 64 rows (0 to 63, 64 to 127, ...) at most 8 rows name the same one
- route_weights: float32 [16384, 4], P(('sp', 'tp')), may hold values from 0.1 to 1
- expert_gate: bfloat16 [64, 2048, 384], P('sp'), may hold values from -0.125 to 0.125
- expert_up: bfloat16 [64, 2048, 384], P('sp'), may hold values from -0.125 to 0.125
- expert_down: bfloat16 [64, 384, 2048], P('sp'), may hold values from -0.3125 to 0.3125
- shared_gate: bfloat16 [2048, 384], replicated, may hold values from -0.125 to 0.125
- shared_up: bfloat16 [2048, 384], replicated, may hold values from -0.125 to 0.125
- shared_down: bfloat16 [384, 2048], replicated, may hold values from -0.3125 to 0.3125
Outputs:
- result: bfloat16 [16384, 2048], P(('sp', 'tp'))
Inputs may be any that keep to these rules, and one draw needn't show every extreme that they name: `route_ids`: each row names 4 different experts. Within the rows of one device (aligned blocks of 64 rows) no expert is named more than 8 times, and in some blocks one expert is named exactly 8 times.
All inputs are finite; a program needn't handle non-finite values.
Results may differ from a plain program's by a relative error of at most 0.007.
Values may be sent and summed in bfloat16 or wider, within the bound.
No kernel may reach another device: no remote copies, remote signals or barrier semaphores. Data moves between devices by JAX's collectives and lax.ppermute only.
A program may use at most 128 MiB of HBM per device.

v0:
```python
import functools
import math

import jax
import jax.numpy as jnp
from jax import lax
from jax.experimental import pallas as pl
from jax.experimental.pallas import tpu as pltpu
from jax.sharding import Mesh
from jax.sharding import PartitionSpec as P


D = 2048
HD = 128
TOP_K = 4
SP = ("sp_0", "sp_1", "sp_2")
SP_TP = ("sp_0", "sp_1", "sp_2", "tp")


BK = 256
SCALE = math.log2(math.e) / math.sqrt(HD)


def shifted(value, axis, step):
    size = lax.axis_size(axis)
    return lax.ppermute(value, axis, [(i, (i + step) % size) for i in range(size)])


def counter_shifted(value):
    size = lax.axis_size("sp_0")
    pairs = [(2 * i, 2 * ((i + 1) % size)) for i in range(size)]
    pairs += [(2 * i + 1, 2 * ((i - 1) % size) + 1) for i in range(size)]
    return lax.ppermute(value, ("sp_0", "sp_2"), pairs)


def call(kernel, outs, args, scratch=(), flops=0):
    return pl.pallas_call(
        kernel,
        out_shape=[jax.ShapeDtypeStruct(*out) for out in outs],
        in_specs=[pl.BlockSpec(memory_space=pltpu.SMEM)]
        + [pl.BlockSpec(memory_space=pltpu.VMEM)] * (len(args) - 1),
        out_specs=[pl.BlockSpec(memory_space=pltpu.VMEM)] * len(outs),
        scratch_shapes=list(scratch),
        compiler_params=pltpu.CompilerParams(vmem_limit_bytes=24 * 2**20),
        cost_estimate=pl.CostEstimate(flops=flops, bytes_accessed=2**20, transcendentals=0),
    )(*args)


def assemble_kernel(y_size, at_ref, own_ref, other_ref, plane_ref):
    row, core = at_ref[1], at_ref[2]
    for k in range(y_size):
        place = (2 * ((row + y_size - k) % y_size) + y_size * core) % (2 * y_size)
        plane_ref[place + core] = own_ref[k]
        plane_ref[place + 1 - core] = other_ref[k]


def block_steps(
    q_ref, plane_ref, acc, carry, tri, level_buf, penalty_buf, first_row, tok, turn
):
    rows = acc.shape[0]
    shards = plane_ref.shape[0]

    def scores(j, slot, diagonal=False):
        keys = plane_ref[(j + turn) % shards, :, 0:HD]
        y = lax.dot_general(
            q_ref[pl.ds(first_row, rows), :],
            jnp.concatenate([keys, keys], axis=1),
            (((1,), (1,)), ((), ())),
            preferred_element_type=jnp.float32,
        )
        penalty = jnp.maximum(y, jnp.log2(1.0 + jnp.exp2(jnp.minimum(y, 126.0))))
        level = y - penalty
        if diagonal:
            query_at = lax.broadcasted_iota(jnp.int32, (rows, BK), 0) % tok
            visible = lax.broadcasted_iota(jnp.int32, (rows, BK), 1) < query_at
            penalty = jnp.where(visible, penalty, 0.0)
            level = jnp.where(visible, level, -1e30)
        level_buf[slot] = level
        penalty_buf[slot] = penalty.astype(jnp.bfloat16)

    def mix(j, slot):
        penalty = penalty_buf[slot]
        after = jnp.dot(penalty, tri[...], preferred_element_type=jnp.float32)
        so_far = carry[...]
        weights = jnp.exp2(level_buf[slot] - after - jnp.concatenate([so_far, so_far], axis=1))
        carry[...] = so_far + jnp.broadcast_to(
            after[:, 0:1] + penalty[:, 0:1].astype(jnp.float32), (rows, HD)
        )
        acc[...] += jnp.dot(
            weights.astype(jnp.bfloat16),
            plane_ref[(j + turn) % shards, :, HD : 2 * HD],
            preferred_element_type=jnp.float32,
        )

    def both(j, slot):
        mix(j, slot)
        scores(j - 1, 1 - slot)

    return scores, mix, both


def clear(acc, carry, tri):
    acc[...] = jnp.zeros_like(acc)
    carry[...] = jnp.zeros_like(carry)
    key_at = lax.broadcasted_iota(jnp.int32, (BK, BK), 0)
    later = key_at > lax.broadcasted_iota(jnp.int32, (BK, BK), 1)
    tri[...] = later.astype(jnp.float32).astype(jnp.bfloat16)


def own_plane_kernel(
    at_ref, own_ref, other_ref, plane_ref, q_ref, acc, carry, tri, level_buf, penalty_buf
):
    tok = own_ref.shape[0]
    heads = own_ref.shape[1] // HD
    rows = tok * heads
    core = at_ref[2]
    for place, ref in ((core, own_ref), (1 - core, other_ref)):
        for g in range(heads):
            scaled = ref[:, g * HD : (g + 1) * HD].astype(jnp.float32) * SCALE
            high = scaled.astype(jnp.bfloat16)
            target = pl.ds(pl.multiple_of(place * rows + g * tok, tok), tok)
            q_ref[target, 0:HD] = high
            q_ref[target, HD : 2 * HD] = (scaled - high.astype(jnp.float32)).astype(jnp.bfloat16)
    clear(acc, carry, tri)
    first_row = pl.multiple_of(core * rows, rows)
    scores, mix, both = block_steps(
        q_ref, plane_ref, acc, carry, tri, level_buf, penalty_buf, first_row, tok,
        plane_ref.shape[0] // 2 * core,
    )
    pos = 2 * at_ref[1] + core
    scores(pos, 0, diagonal=True)

    def step(i, _):
        both(pos - 2 * i, 0)
        both(pos - 2 * i - 1, 1)
        return 0

    lax.fori_loop(0, pos // 2, step, 0)

    @pl.when(pos % 2 == 1)
    def _():
        both(1, 0)
        mix(0, 1)

    @pl.when(pos % 2 == 0)
    def _():
        mix(0, 0)


def plane_kernel(
    distance, z_size, tok, last, at_ref, q_ref, plane_ref, acc_in, total_in, acc_out, total_out,
    acc, carry, tri, level_buf, penalty_buf
):
    rows = acc.shape[0]
    core = at_ref[2]
    below = jnp.where(core == 0, distance, z_size - distance)
    shards = plane_ref.shape[0]

    def part(h, _):
        first_row = pl.multiple_of(h * rows, rows)
        here = pl.ds(first_row, rows)
        clear(acc, carry, tri)

        @pl.when(below <= at_ref[0])
        def _():
            scores, mix, both = block_steps(
                q_ref, plane_ref, acc, carry, tri, level_buf, penalty_buf, first_row, tok,
                0 if last else shards // 2 * core,
            )
            scores(shards - 1, 0)

            def step(i, _):
                both(shards - 1 - 2 * i, 0)
                both(shards - 2 - 2 * i, 1)
                return 0

            lax.fori_loop(0, shards // 2 - 1, step, 0)
            both(1, 0)
            mix(0, 1)

        old, old_total = acc_in[here, :], total_in[here, :]
        new, new_total = acc[...], carry[...]
        upward = core == 0
        result = old * jnp.exp2(jnp.where(upward, 0.0, -new_total))
        result = result + new * jnp.exp2(jnp.where(upward, -old_total, 0.0))
        if last:
            place = jnp.where(h == core, 0, 1)
            acc_out[place] = result
            total_out[place] = old_total + new_total
        else:
            acc_out[here, :] = result
            total_out[here, :] = old_total + new_total
        return 0

    lax.fori_loop(0, 2, part, 0)


def merge_kernel(at_ref, own_ref, own_total, acc_ref, total_ref, theirs, their_total, out_ref):
    upward = at_ref[2] == 0
    tok = out_ref.shape[0]
    mine, other = acc_ref[0], theirs[...]
    newer_total = jnp.where(upward, total_ref[0], their_total[...])
    newer, older = jnp.where(upward, mine, other), jnp.where(upward, other, mine)
    mixed = own_ref[...] + jnp.exp2(-own_total[...]) * (newer + jnp.exp2(-newer_total) * older)
    for g in range(out_ref.shape[1] // HD):
        out_ref[:, g * HD : (g + 1) * HD] = mixed[g * tok : (g + 1) * tok].astype(out_ref.dtype)


def attention(at, query, keys, values):
    z_size, y_size = lax.axis_size("sp_0"), lax.axis_size("sp_1")
    tok = query.shape[0]
    rows = tok * (query.shape[1] // HD)
    other_query = shifted(query, "sp_2", 1)
    pair = jnp.concatenate([keys, values], axis=1)
    ring = [pair] + [None] * (y_size - 1)
    down = up = pair
    for k in range(1, y_size // 2 + 1):
        down = ring[k] = shifted(down, "sp_1", 1)
        if k < y_size - k:
            up = ring[y_size - k] = shifted(up, "sp_1", -1)
    own_rows = jnp.stack(ring)
    (plane,) = call(
        functools.partial(assemble_kernel, y_size),
        [((2 * y_size, tok, 2 * HD), jnp.bfloat16)],
        (at, own_rows, shifted(own_rows, "sp_2", 1)),
    )
    scratch = [
        pltpu.VMEM((BK, BK), jnp.bfloat16),
        pltpu.VMEM((2, rows, BK), jnp.float32),
        pltpu.VMEM((2, rows, BK), jnp.bfloat16),
    ]
    state = ((rows, HD), jnp.float32)
    both_state = ((2 * rows, HD), jnp.float32)
    work = 2 * y_size * rows * BK * HD * 16
    doubled, own, own_total = call(
        own_plane_kernel,
        [((2 * rows, 2 * HD), jnp.bfloat16), state, state],
        (at, query, other_query, plane),
        scratch,
        work // 2,
    )
    acc = total = jnp.zeros(*both_state)
    done = own
    for k in range(1, z_size // 2 + 1):
        last = k == z_size // 2
        if k > 1:
            plane, done = lax.optimization_barrier((plane, done))
            if k == 2:
                own = done
            done = acc
        if last:
            plane = plane[y_size:]
        plane = counter_shifted(plane)
        acc, total = call(
            functools.partial(plane_kernel, k, z_size, tok, last),
            [((2, rows, HD), jnp.float32)] * 2 if last else [both_state] * 2,
            (at, doubled, plane, acc, total),
            [pltpu.VMEM((rows, HD), jnp.float32)] * 2 + scratch,
            work * 2,
        )
    theirs = shifted(jnp.stack([acc[1], total[1]]), "sp_2", 1)
    return call(
        merge_kernel,
        [((tok, query.shape[1]), jnp.bfloat16)],
        (at, own, own_total, acc, total, theirs[0], theirs[1]),
    )[0]


def chosen_slots(slots, weights, count):
    slot = lax.broadcasted_iota(jnp.int32, (slots.shape[0], count), 1)
    picked = jnp.zeros(slot.shape, jnp.float32)
    for k in range(slots.shape[1]):
        picked += jnp.where(slot == slots[:, k : k + 1], weights[:, k : k + 1], 0.0)
    return picked


def project_kernel(
    at_ref, heads_ref, w0, w1, w2, w3, stream_ref, gain_ref, slots_ref, mid_ref, normed_ref, out_ref
):
    weights = (w0, w1, w2, w3)
    own = at_ref[3]
    attended = jnp.zeros(stream_ref.shape, jnp.float32)
    for k, weight in enumerate(weights):
        source = (own + len(weights) - k) % len(weights)
        attended += jnp.dot(heads_ref[source], weight[...], preferred_element_type=jnp.float32)
    mid = (stream_ref[...].astype(jnp.float32) + attended).astype(jnp.bfloat16)
    mid_ref[...] = mid
    wide = mid.astype(jnp.float32)
    scale = lax.rsqrt(jnp.mean(wide * wide, axis=1, keepdims=True) + 1e-06)
    normed = (wide * scale * gain_ref[...]).astype(jnp.bfloat16)
    normed_ref[...] = normed
    ones = jnp.ones(slots_ref.shape, jnp.float32)
    picked = chosen_slots(slots_ref[...], ones, out_ref.shape[0]).astype(jnp.bfloat16)
    out_ref[...] = lax.dot_general(
        picked, normed, (((0,), (0,)), ((), ())), preferred_element_type=jnp.float32
    ).astype(jnp.bfloat16)


def gated(rows, gate, up):
    gate_part = jnp.dot(rows, gate, preferred_element_type=jnp.float32)
    up_part = jnp.dot(rows, up, preferred_element_type=jnp.float32)
    return (gate_part / (1.0 + jnp.exp(-gate_part)) * up_part).astype(jnp.bfloat16)


def expert_kernel(at_ref, rows_ref, gate_ref, up_ref, down_ref, out_ref):
    chunk = 256

    def part(k, _):
        here = pl.ds(pl.multiple_of(k * chunk, chunk), chunk)
        hidden = gated(rows_ref[here, :], gate_ref[...], up_ref[...])
        out_ref[here, :] = jnp.dot(
            hidden, down_ref[...], preferred_element_type=jnp.float32
        ).astype(jnp.bfloat16)
        return 0

    lax.fori_loop(0, rows_ref.shape[0] // chunk, part, 0)


def shared_kernel(at_ref, normed_ref, mid_ref, gate_ref, up_ref, down_ref, base_ref):
    hidden = gated(normed_ref[...], gate_ref[...], up_ref[...])
    base_ref[...] = mid_ref[...].astype(jnp.float32) + jnp.dot(
        hidden, down_ref[...], preferred_element_type=jnp.float32
    )


def combine_kernel(at_ref, base_ref, rows_ref, slots_ref, weights_ref, out_ref):
    picked = chosen_slots(slots_ref[...], weights_ref[...], rows_ref.shape[0])
    high = picked.astype(jnp.bfloat16)
    low = (picked - high.astype(jnp.float32)).astype(jnp.bfloat16)
    routed = jnp.dot(high, rows_ref[...], preferred_element_type=jnp.float32)
    routed += jnp.dot(low, rows_ref[...], preferred_element_type=jnp.float32)
    out_ref[...] = (base_ref[...] + routed).astype(jnp.bfloat16)


def per_device(
    query,
    key_rows,
    value_rows,
    stream,
    out_weight,
    norm_gain,
    route_ids,
    route_weights,
    expert_gate,
    expert_up,
    expert_down,
    shared_gate,
    shared_up,
    shared_down,
):
    at = jnp.stack([lax.axis_index(axis) for axis in SP_TP])
    weight_below = shifted(out_weight, "tp", 1)
    weight_above = shifted(out_weight, "tp", -1)
    weight_far = shifted(weight_below, "tp", 1)
    out_weights = (out_weight, weight_below, weight_far, weight_above)
    own_rows = stream.shape[0]
    expert_count = lax.axis_size(SP) * expert_gate.shape[0]
    capacity = 2 * own_rows * TOP_K // expert_count
    slot_count = expert_count * capacity
    flat_ids = route_ids.reshape(-1)
    membership = (flat_ids[:, None] == jnp.arange(expert_count, dtype=jnp.int32)[None, :]).astype(
        jnp.int32
    )
    before = jnp.cumsum(membership, axis=0) - membership
    slot_rank = jnp.sum(before * membership, axis=1)
    slots = (flat_ids * capacity + slot_rank).reshape(route_ids.shape)
    heads_out = attention(at, query, key_rows, value_rows)
    token_heads = lax.all_to_all(
        heads_out.reshape(-1, own_rows, heads_out.shape[1]), "tp", 0, 0, tiled=True
    )
    wide = (own_rows, D)
    mid, normed, outgoing = call(
        project_kernel,
        [(wide, jnp.bfloat16), (wide, jnp.bfloat16), ((slot_count, D), jnp.bfloat16)],
        (at, token_heads, *out_weights, stream, norm_gain.reshape(1, D), slots),
        flops=2**29,
    )
    exchange = (lax.axis_size(SP), slot_count // lax.axis_size(SP), D)
    arrived = lax.all_to_all(outgoing.reshape(exchange), SP, 0, 0, tiled=True)
    (produced,) = call(
        expert_kernel,
        [((slot_count, D), jnp.bfloat16)],
        (at, arrived.reshape(slot_count, D), expert_gate[0], expert_up[0], expert_down[0]),
        flops=2**32,
    )
    returned = lax.all_to_all(produced.reshape(exchange), SP, 0, 0, tiled=True)
    (base,) = call(
        shared_kernel,
        [(wide, jnp.float32)],
        (at, normed, mid, shared_gate, shared_up, shared_down),
        flops=2**30,
    )
    return call(
        combine_kernel,
        [(wide, jnp.bfloat16)],
        (at, base, returned.reshape(slot_count, D), slots, route_weights),
        flops=2**28,
    )[0]


def solution(mesh):
    split = Mesh(mesh.devices.reshape(8, 4, 2, mesh.shape["tp"]), ("sp_0", "sp_1", "sp_2", "tp"))
    in_specs = (
        P(SP, "tp"),
        P(SP, "tp"),
        P(SP, "tp"),
        P(SP_TP, None),
        P("tp", None),
        P(),
        P(SP_TP, None),
        P(SP_TP, None),
        P(SP, None, None),
        P(SP, None, None),
        P(SP, None, None),
        P(),
        P(),
        P(),
    )
    out_specs = P(SP_TP, None)

    return jax.shard_map(
        per_device, mesh=split, in_specs=in_specs, out_specs=out_specs, check_vma=False
    )
```

profile of v0, /device:TPU:8, one launch (start us, length us, event | category | flops | bytes accessed | tf_op | source)
XLA Modules:
  0.0 235.3 jit_solution(14250865996381300882)
XLA Ops:
  1.7 1.7 collective-permute-start
  4.0 3.0 %collective-permute-done = bf16[256,256]{1,0:T(8,128)(2,1)S(1)} collective-permute-done((bf16[256,256]{1,0:T(8,128)(2,1)S(1)}, bf16[256,256]{1,0:T(8,128)(2,1)S(1)}, u32[]{:S(2)}, u32[]{:S(2)}) %collective-permute-start) | collective-permute-done | bytes 131104 | tf_op jit(solution)/shard_map/ppermute | solution.py:26
  7.0 1.6 collective-permute-start.1
  8.6 4.5 %collective-permute-done.1 = bf16[256,256]{1,0:T(8,128)(2,1)S(1)} collective-permute-done((bf16[256,256]{1,0:T(8,128)(2,1)S(1)}, bf16[256,256]{1,0:T(8,128)(2,1)S(1)}, u32[]{:S(2)}, u32[]{:S(2)}) %collective-permute-start.1) | collective-permute-done | bytes 131104 | tf_op jit(solution)/shard_map/ppermute | solution.py:26
  13.3 1.8 collective-permute-done.3.other_ref
  16.7 3.8 %collective-permute-start.5 = (bf16[256,256]{1,0:T(8,128)(2,1)S(1)}, bf16[256,256]{1,0:T(8,128)(2,1)S(1)}, u32[]{:S(2)}, u32[]{:S(2)}) collective-permute-start(bf16[256,256]{1,0:T(8,128)(2,1)S(1)} %copy-done.18), channel_id=1, source_target_pairs={{0,4},{4,0},{1,5},{5,1},{2,6},{6,2},{3,7},{7,3},{8,12},{12,8},{9,1... | collective-permute-start | bytes 393224 | tf_op jit(solution)/shard_map/ppermute | solution.py:26
  21.5 2.1 shard_map.137
  25.0 8.5 %collective-permute-done.4.plane_ref = bf16[8,256,256]{2,1,0:T(8,128)(2,1)S(1)} collective-permute-done((bf16[8,256,256]{2,1,0:T(8,128)(2,1)S(1)}, bf16[8,256,256]{2,1,0:T(8,128)(2,1)S(1)}, u32[]{:S(2)}, u32[]{:S(2)}) %collective-permute-start.4) | collective-permute-done | bytes 1048608 | tf_op jit(solution)/shard_map/ppermute | solution.py:33
  34.3 15.1 %collective-permute-done.6.plane_ref = bf16[8,256,256]{2,1,0:T(8,128)(2,1)S(1)} collective-permute-done((bf16[8,256,256]{2,1,0:T(8,128)(2,1)S(1)}, bf16[8,256,256]{2,1,0:T(8,128)(2,1)S(1)}, u32[]{:S(2)}, u32[]{:S(2)}) %collective-permute-start.6) | collective-permute-done | bytes 1048608 | tf_op jit(solution)/shard_map/ppermute | solution.py:33
  49.4 1.5 collective-permute-start.10
  51.8 13.7 %collective-permute-done.7.plane_ref = bf16[8,256,256]{2,1,0:T(8,128)(2,1)S(1)} collective-permute-done((bf16[8,256,256]{2,1,0:T(8,128)(2,1)S(1)}, bf16[8,256,256]{2,1,0:T(8,128)(2,1)S(1)}, u32[]{:S(2)}, u32[]{:S(2)}) %collective-permute-start.7) | collective-permute-done | bytes 1048608 | tf_op jit(solution)/shard_map/ppermute | solution.py:33
  66.3 2.8 %collective-permute-start.12 = (bf16[256,2048]{1,0:T(8,128)(2,1)S(1)}, bf16[256,2048]{1,0:T(8,128)(2,1)}, u32[]{:S(2)}, u32[]{:S(2)}) collective-permute-start(bf16[256,2048]{1,0:T(8,128)(2,1)S(1)} %copy-done.4), channel_id=1, source_target_pairs={{0,3},{1,0},{2,1},{3,2},{4,7},{5,4},{6,5},{7,6},{8,11},{9,8},{10,9... | collective-permute-start | bytes 3145736 | tf_op jit(solution)/shard_map/ppermute | solution.py:26
  69.4 7.1 %collective-permute-done.10.w1 = bf16[256,2048]{1,0:T(8,128)(2,1)S(1)} collective-permute-done((bf16[256,2048]{1,0:T(8,128)(2,1)S(1)}, bf16[256,2048]{1,0:T(8,128)(2,1)S(1)}, u32[]{:S(2)}, u32[]{:S(2)}) %collective-permute-start.10) | collective-permute-done | bytes 1048608 | tf_op jit(solution)/shard_map/ppermute | solution.py:26
  76.8 1.0 copy-done.20
  78.9 1.0 copy-done.24
  80.7 1.3 shard_map.141
  83.9 1.4 collective-permute-done.9
  85.3 1.1 slice_bitcast_fusion
  88.3 1.3 shard_map.142
  89.6 4.2 %all-to-all-start = ((bf16[4,64,256]{2,1,0:T(8,128)(2,1)}), bf16[4,64,256]{2,1,0:T(8,128)(2,1)S(1)}, u32[]{:S(2)}, u32[]{:S(2)}) async-start(bf16[4,64,256]{2,1,0:T(8,128)(2,1)} %bitcast.10), calls=%async_computation | async-start | bytes 262144 | tf_op jit(solution)/shard_map/all_to_all | solution.py:368
  94.2 9.4 %collective-permute-done.11.w2 = bf16[256,2048]{1,0:T(8,128)(2,1)} collective-permute-done((bf16[256,2048]{1,0:T(8,128)(2,1)S(1)}, bf16[256,2048]{1,0:T(8,128)(2,1)}, u32[]{:S(2)}, u32[]{:S(2)}) %collective-permute-start.11) | collective-permute-done | bytes 1048608 | tf_op jit(solution)/shard_map/ppermute | solution.py:26
  104.2 3.3 %shard_map.143 = (bf16[64,2048]{1,0:T(8,128)(2,1)S(1)}, bf16[64,2048]{1,0:T(8,128)(2,1)S(1)}, bf16[512,2048]{1,0:T(8,128)(2,1)S(1)}) custom-call(s32[4]{0:T(128)S(1)} %pad_add_fusion.at_ref, bf16[4,64,256]{2,1,0:T(8,128)(2,1)S(1)} %all-to-all-done.heads_ref, bf16[256,2048]{1,0:T(8,128)(2,1)S(1)} %copy-done.4, ...), custom_call_target="tpu_custom_call" | custom-call | flops 536870912 | bytes 1048576 | tf_op jit(solution)/shard_map/pallas_call | solution.py:37
  107.6 63.0 %all_to_all.15 = bf16[64,8,2048]{2,1,0:T(8,128)(2,1)S(1)} all-to-all(bf16[64,8,2048]{2,1,0:T(8,128)(2,1)S(1)} %bitcast.42), channel_id=1, replica_groups=mesh['sp_0'=8,'sp_1'=4,'sp_2'=2,'tp'=4] {'sp_0','sp_1','sp_2'}, dimensions={0} | all-to-all | bytes 4194304 | tf_op jit(solution)/shard_map/all_to_all | solution.py:379
  170.6 4.3 %shard_map.145 = bf16[512,2048]{1,0:T(8,128)(2,1)S(1)} custom-call(s32[4]{0:T(128)S(1)} %pad_add_fusion.at_ref, bf16[512,2048]{1,0:T(8,128)(2,1)S(1)} %bitcast.43, bf16[2048,384]{1,0:T(8,128)(2,1)S(1)} %bitcast.45, bf16[2048,384]{1,0:T(8,128)(2,1)S(1)} %bitcast.46, bf16[384,2048]{1,0:T(8,128)(2,1)S(1)} %bitcast.47), custom_call_target="tpu_custom_call" | custom-call | flops 4294967296 | bytes 1048576 | tf_op jit(solution)/shard_map/pallas_call | solution.py:37
  174.9 1.4 copy-done
  176.3 5.6 %all-to-all-start.2 = ((bf16[64,8,2048]{2,1,0:T(8,128)(2,1)}), bf16[64,8,2048]{2,1,0:T(8,128)(2,1)S(1)}, u32[]{:S(2)}, u32[]{:S(2)}) async-start(bf16[64,8,2048]{2,1,0:T(8,128)(2,1)} %bitcast.41), calls=%async_computation.2 | async-start | bytes 4194304 | tf_op jit(solution)/shard_map/all_to_all | solution.py:386
  182.0 1.4 copy-done.1
  183.4 1.4 copy-done.2
  184.8 1.4 copy-done.3
  186.2 1.5 shard_map.144.base_ref
  187.7 45.4 %all-to-all-done.2 = bf16[64,8,2048]{2,1,0:T(8,128)(2,1)S(1)} async-done(((bf16[64,8,2048]{2,1,0:T(8,128)(2,1)}), bf16[64,8,2048]{2,1,0:T(8,128)(2,1)S(1)}, u32[]{:S(2)}, u32[]{:S(2)}) %all-to-all-start.2) | async-done | bytes 2097184 | tf_op jit(solution)/shard_map/all_to_all | solution.py:386
  233.1 2.2 shard_map.146
  (88 shorter events, 16.3 us)
Async XLA Ops:
  1.7 5.3 %collective-permute-start = (bf16[256,256]{1,0:T(8,128)(2,1)S(1)}, bf16[256,256]{1,0:T(8,128)(2,1)S(1)}, u32[]{:S(2)}, u32[]{:S(2)}) collective-permute-start(bf16[256,256]{1,0:T(8,128)(2,1)S(1)} %constant_dynamic-update-slice_fusion), channel_id=1, source_target_pairs={{0,8},{8,16},{16,24},{24,0},{1,9},{9,17},{17,25},{25,1},{2,10},{10... | collective-permute-start | bytes 393224 | tf_op jit(solution)/shard_map/ppermute | solution.py:26
  3.4 5.2 %collective-permute-start.2 = (bf16[256,256]{1,0:T(8,128)(2,1)S(1)}, bf16[256,256]{1,0:T(8,128)(2,1)S(1)}, u32[]{:S(2)}, u32[]{:S(2)}) collective-permute-start(bf16[256,256]{1,0:T(8,128)(2,1)S(1)} %constant_dynamic-update-slice_fusion), channel_id=1, source_target_pairs={{0,24},{8,0},{16,8},{24,16},{1,25},{9,1},{17,9},{25,17},{2,26},{10... | collective-permute-start | bytes 393224 | tf_op jit(solution)/shard_map/ppermute | solution.py:26
  7.0 6.0 %collective-permute-start.1 = (bf16[256,256]{1,0:T(8,128)(2,1)S(1)}, bf16[256,256]{1,0:T(8,128)(2,1)S(1)}, u32[]{:S(2)}, u32[]{:S(2)}) collective-permute-start(bf16[256,256]{1,0:T(8,128)(2,1)S(1)} %collective-permute-done), channel_id=1, source_target_pairs={{0,8},{8,16},{16,24},{24,0},{1,9},{9,17},{17,25},{25,1},{2,10},{10... | collective-permute-start | bytes 393224 | tf_op jit(solution)/shard_map/ppermute | solution.py:26
  13.1 3.6 %copy-start.18 = (bf16[256,256]{1,0:T(8,128)(2,1)S(1)}, bf16[256,256]{1,0:T(8,128)(2,1)}, u32[]{:S(2)}) copy-start(bf16[256,256]{1,0:T(8,128)(2,1)} %own_ref.1) | copy-start | bytes 393220
  13.1 2.0 collective-permute-start.3
  15.8 17.6 %collective-permute-start.4 = (bf16[8,256,256]{2,1,0:T(8,128)(2,1)S(1)}, bf16[8,256,256]{2,1,0:T(8,128)(2,1)S(1)}, u32[]{:S(2)}, u32[]{:S(2)}) collective-permute-start(bf16[8,256,256]{2,1,0:T(8,128)(2,1)S(1)} %shard_map.136.plane_ref), channel_id=1, source_target_pairs={{0,32},{32,64},{64,96},{96,128},{128,160},{160,192},{192,224},{224... | collective-permute-start | bytes 3145736 | tf_op jit(solution)/shard_map/ppermute | solution.py:33
  16.7 4.8 %collective-permute-start.5 = (bf16[256,256]{1,0:T(8,128)(2,1)S(1)}, bf16[256,256]{1,0:T(8,128)(2,1)S(1)}, u32[]{:S(2)}, u32[]{:S(2)}) collective-permute-start(bf16[256,256]{1,0:T(8,128)(2,1)S(1)} %copy-done.18), channel_id=1, source_target_pairs={{0,4},{4,0},{1,5},{5,1},{2,6},{6,2},{3,7},{7,3},{8,12},{12,8},{9,1... | collective-permute-start | bytes 393224 | tf_op jit(solution)/shard_map/ppermute | solution.py:26
  25.0 26.0 %copy-start.19 = (bf16[1024,256]{1,0:T(8,128)(2,1)}, bf16[1024,256]{1,0:T(8,128)(2,1)S(1)}, u32[]{:S(2)}) copy-start(bf16[1024,256]{1,0:T(8,128)(2,1)S(1)} %get-tuple-element.26.q_ref) | copy-start | bytes 1572868
  33.4 16.0 %collective-permute-start.6 = (bf16[8,256,256]{2,1,0:T(8,128)(2,1)S(1)}, bf16[8,256,256]{2,1,0:T(8,128)(2,1)S(1)}, u32[]{:S(2)}, u32[]{:S(2)}) collective-permute-start(bf16[8,256,256]{2,1,0:T(8,128)(2,1)S(1)} %collective-permute-done.4.plane_ref), channel_id=1, source_target_pairs={{0,32},{32,64},{64,96},{96,128},{128,160},{160,192},{192,224},{224... | collective-permute-start | bytes 3145736 | tf_op jit(solution)/shard_map/ppermute | solution.py:33
  33.5 16.0 %copy-start.4 = (bf16[256,2048]{1,0:T(8,128)(2,1)S(1)}, bf16[256,2048]{1,0:T(8,128)(2,1)}, u32[]{:S(2)}) copy-start(bf16[256,2048]{1,0:T(8,128)(2,1)} %w0.1) | copy-start | bytes 3145732
  49.4 16.0 %collective-permute-start.7 = (bf16[8,256,256]{2,1,0:T(8,128)(2,1)S(1)}, bf16[8,256,256]{2,1,0:T(8,128)(2,1)S(1)}, u32[]{:S(2)}, u32[]{:S(2)}) collective-permute-start(bf16[8,256,256]{2,1,0:T(8,128)(2,1)S(1)} %collective-permute-done.6.plane_ref), channel_id=1, source_target_pairs={{0,32},{32,64},{64,96},{96,128},{128,160},{160,192},{192,224},{224... | collective-permute-start | bytes 3145736 | tf_op jit(solution)/shard_map/ppermute | solution.py:33
  49.4 27.1 %collective-permute-start.10 = (bf16[256,2048]{1,0:T(8,128)(2,1)S(1)}, bf16[256,2048]{1,0:T(8,128)(2,1)S(1)}, u32[]{:S(2)}, u32[]{:S(2)}) collective-permute-start(bf16[256,2048]{1,0:T(8,128)(2,1)S(1)} %copy-done.4), channel_id=1, source_target_pairs={{0,1},{1,2},{2,3},{3,0},{4,5},{5,6},{6,7},{7,4},{8,9},{9,10},{10,1... | collective-permute-start | bytes 3145736 | tf_op jit(solution)/shard_map/ppermute | solution.py:26
  50.9 18.2 %copy-start.25 = (s32[64,4]{0,1:T(4,128)S(1)}, s32[64,4]{0,1:T(4,128)}, u32[]{:S(2)}) copy-start(s32[64,4]{0,1:T(4,128)} %param.20) | copy-start | bytes 3076
  51.8 14.5 %copy-start.21 = (f32[1024,128]{1,0:T(8,128)}, f32[1024,128]{1,0:T(8,128)S(1)}, u32[]{:S(2)}) copy-start(f32[1024,128]{1,0:T(8,128)S(1)} %get-tuple-element.31.acc_in) | copy-start | bytes 1572868
  51.8 14.5 %copy-start.23 = (f32[1024,128]{1,0:T(8,128)}, f32[1024,128]{1,0:T(8,128)S(1)}, u32[]{:S(2)}) copy-start(f32[1024,128]{1,0:T(8,128)S(1)} %get-tuple-element.33.total_in) | copy-start | bytes 1572868
  66.3 14.5 %collective-permute-start.8 = (bf16[4,256,256]{2,1,0:T(8,128)(2,1)}, bf16[4,256,256]{2,1,0:T(8,128)(2,1)}, u32[]{:S(2)}, u32[]{:S(2)}) collective-permute-start(bf16[4,256,256]{2,1,0:T(8,128)(2,1)} %slice.21), channel_id=1, source_target_pairs={{0,32},{32,64},{64,96},{96,128},{128,160},{160,192},{192,224},{224... | collective-permute-start | bytes 1572872 | tf_op jit(solution)/shard_map/ppermute | solution.py:33
  66.3 27.9 %collective-permute-start.12 = (bf16[256,2048]{1,0:T(8,128)(2,1)S(1)}, bf16[256,2048]{1,0:T(8,128)(2,1)}, u32[]{:S(2)}, u32[]{:S(2)}) collective-permute-start(bf16[256,2048]{1,0:T(8,128)(2,1)S(1)} %copy-done.4), channel_id=1, source_target_pairs={{0,3},{1,0},{2,1},{3,2},{4,7},{5,4},{6,5},{7,6},{8,11},{9,8},{10,9... | collective-permute-start | bytes 3145736 | tf_op jit(solution)/shard_map/ppermute | solution.py:26
  76.5 27.1 %collective-permute-start.11 = (bf16[256,2048]{1,0:T(8,128)(2,1)S(1)}, bf16[256,2048]{1,0:T(8,128)(2,1)}, u32[]{:S(2)}, u32[]{:S(2)}) collective-permute-start(bf16[256,2048]{1,0:T(8,128)(2,1)S(1)} %collective-permute-done.10.w1), channel_id=1, source_target_pairs={{0,1},{1,2},{2,3},{3,0},{4,5},{5,6},{6,7},{7,4},{8,9},{9,10},{10,1... | collective-permute-start | bytes 3145736 | tf_op jit(solution)/shard_map/ppermute | solution.py:26
  83.0 2.3 collective-permute-start.9
  85.3 18.9 %copy-start.14 = (f32[2048]{0:T(1024)S(1)}, f32[2048]{0:T(1024)}, u32[]{:S(2)}) copy-start(f32[2048]{0:T(1024)} %param.19) | copy-start | bytes 24580
  86.4 17.9 %copy-start.5 = (bf16[64,2048]{1,0:T(8,128)(2,1)S(1)}, bf16[64,2048]{1,0:T(8,128)(2,1)}, u32[]{:S(2)}) copy-start(bf16[64,2048]{1,0:T(8,128)(2,1)} %stream_ref.1) | copy-start | bytes 786436
  89.6 14.6 %all-to-all-start = ((bf16[4,64,256]{2,1,0:T(8,128)(2,1)}), bf16[4,64,256]{2,1,0:T(8,128)(2,1)S(1)}, u32[]{:S(2)}, u32[]{:S(2)}) async-start(bf16[4,64,256]{2,1,0:T(8,128)(2,1)} %bitcast.10), calls=%async_computation | async-start | bytes 262144 | tf_op jit(solution)/shard_map/all_to_all | solution.py:368
  104.2 66.3 %copy-start.17 = (bf16[1,384,2048]{2,1,0:T(8,128)(2,1)S(1)}, bf16[1,384,2048]{2,1,0:T(8,128)(2,1)}, u32[]{:S(2)}) copy-start(bf16[1,384,2048]{2,1,0:T(8,128)(2,1)} %param.24) | copy-start | bytes 4718596
  107.5 63.0 %copy-start.10 = (bf16[64,2048]{1,0:T(8,128)(2,1)}, bf16[64,2048]{1,0:T(8,128)(2,1)S(1)}, u32[]{:S(2)}) copy-start(bf16[64,2048]{1,0:T(8,128)(2,1)S(1)} %get-tuple-element.39.mid_ref) | copy-start | bytes 786436
  107.5 63.0 %copy-start.12 = (bf16[64,2048]{1,0:T(8,128)(2,1)}, bf16[64,2048]{1,0:T(8,128)(2,1)S(1)}, u32[]{:S(2)}) copy-start(bf16[64,2048]{1,0:T(8,128)(2,1)S(1)} %get-tuple-element.38.normed_ref) | copy-start | bytes 786436
  107.5 63.0 %copy-start.15 = (bf16[1,2048,384]{2,1,0:T(8,128)(2,1)S(1)}, bf16[1,2048,384]{2,1,0:T(8,128)(2,1)}, u32[]{:S(2)}) copy-start(bf16[1,2048,384]{2,1,0:T(8,128)(2,1)} %param.22) | copy-start | bytes 4718596
  107.6 63.0 %copy-start.16 = (bf16[1,2048,384]{2,1,0:T(8,128)(2,1)S(1)}, bf16[1,2048,384]{2,1,0:T(8,128)(2,1)}, u32[]{:S(2)}) copy-start(bf16[1,2048,384]{2,1,0:T(8,128)(2,1)} %param.23) | copy-start | bytes 4718596
  176.3 5.6 %copy-start.26 = (f32[64,4]{0,1:T(4,128)S(1)}, f32[64,4]{0,1:T(4,128)}, u32[]{:S(2)}) copy-start(f32[64,4]{0,1:T(4,128)} %param.21) | copy-start | bytes 3076
  176.3 5.7 %copy-start.11 = (bf16[64,2048]{1,0:T(8,128)(2,1)S(1)}, bf16[64,2048]{1,0:T(8,128)(2,1)}, u32[]{:S(2)}) copy-start(bf16[64,2048]{1,0:T(8,128)(2,1)} %copy-done.10) | copy-start | bytes 786436
  176.3 5.7 %copy-start.13 = (bf16[64,2048]{1,0:T(8,128)(2,1)S(1)}, bf16[64,2048]{1,0:T(8,128)(2,1)}, u32[]{:S(2)}) copy-start(bf16[64,2048]{1,0:T(8,128)(2,1)} %copy-done.12) | copy-start | bytes 786436
  176.3 56.8 %all-to-all-start.2 = ((bf16[64,8,2048]{2,1,0:T(8,128)(2,1)}), bf16[64,8,2048]{2,1,0:T(8,128)(2,1)S(1)}, u32[]{:S(2)}, u32[]{:S(2)}) async-start(bf16[64,8,2048]{2,1,0:T(8,128)(2,1)} %bitcast.41), calls=%async_computation.2 | async-start | bytes 4194304 | tf_op jit(solution)/shard_map/all_to_all | solution.py:386
  182.0 1.4 copy-start.1
  (10 other events, 10.7 us)
where the time goes:
time: 236 us; the launch traced here: 235 us
  waiting for transfers between devices  111 us (47%)
  blocking collectives  63 us (27%)
  starting transfers between devices  23.1 us (10%)
  Pallas kernels  19.2 us (8%)
  local copies, waits for them, and re-layouts  16.6 us (7%)
    all_to_all x1, blocking collectives, per_device(): arrived = lax.all_to_all(outgoing.reshape(exchange), SP, 0, 0, tiled=True)  63 us
    all_to_all x1, waiting for transfers between devices, per_device(): returned = lax.all_to_all(produced.reshape(exchange), SP, 0, 0, tiled=True)  45.4 us
    ppermute x4, waiting for transfers between devices, counter_shifted(): return lax.ppermute(value, ('sp_0', 'sp_2'), pairs)  37.2 us
    ppermute x9, waiting for transfers between devices, shifted(): lax.ppermute(value, axis, [(i, (i + step) % size) for i in range(size)])  28.2 us
    pallas_call x11, Pallas kernels, call(): pl.pallas_call(kernel, out_shape=[jax.ShapeDtypeStruct(*out) for out in o...  19.2 us
    unnamed x57, local copies, waits for them, and re-layouts  13.2 us
    ppermute x9, starting transfers between devices, shifted(): lax.ppermute(value, axis, [(i, (i + step) % size) for i in range(size)])  12.4 us
    all_to_all x1, starting transfers between devices, per_device(): returned = lax.all_to_all(produced.reshape(exchange), SP, 0, 0, tiled=True)  5.56 us
  transfers between devices with their start and end apart: 15, of which 12 were waited for; matrix products, arithmetic and copies ran while one was open for 2% of the time, Pallas kernels for 4%

commit v1 on v0

--- a/solution.py
+++ b/solution.py
@@ -46,22 +46,27 @@
     )(*args)
 
 
-def assemble_kernel(y_size, at_ref, own_ref, other_ref, plane_ref):
-    row, core = at_ref[1], at_ref[2]
-    for k in range(y_size):
-        place = (2 * ((row + y_size - k) % y_size) + y_size * core) % (2 * y_size)
-        plane_ref[place + core] = own_ref[k]
-        plane_ref[place + 1 - core] = other_ref[k]
-
-
-def block_steps(
-    q_ref, plane_ref, acc, carry, tri, level_buf, penalty_buf, first_row, tok, turn
-):
+def assemble_kernel(at_ref, own_ref, other_ref, half_ref):
+    row, core = at_ref[1] % 2, at_ref[2]
+    for k in range(2):
+        place = 2 * jnp.where(row == k, 0, 1)
+        half_ref[place + core] = own_ref[k]
+        half_ref[place + 1 - core] = other_ref[k]
+
+
+def join_halves(at_ref, half_ref, across_ref, plane):
+    shards = half_ref.shape[0]
+    upper = at_ref[1] // 2
+    for k in range(shards):
+        plane[upper * shards + k] = half_ref[k]
+        plane[(1 - upper) * shards + k] = across_ref[k]
+
+
+def block_steps(q_ref, plane_ref, acc, carry, tri, level_buf, penalty_buf, first_row, tok):
     rows = acc.shape[0]
-    shards = plane_ref.shape[0]
 
     def scores(j, slot, diagonal=False):
-        keys = plane_ref[(j + turn) % shards, :, 0:HD]
+        keys = plane_ref[j, :, 0:HD]
         y = lax.dot_general(
             q_ref[pl.ds(first_row, rows), :],
             jnp.concatenate([keys, keys], axis=1),
@@ -88,7 +93,7 @@
         )
         acc[...] += jnp.dot(
             weights.astype(jnp.bfloat16),
-            plane_ref[(j + turn) % shards, :, HD : 2 * HD],
+            plane_ref[j, :, HD : 2 * HD],
             preferred_element_type=jnp.float32,
         )
 
@@ -108,7 +113,8 @@
 
 
 def own_plane_kernel(
-    at_ref, own_ref, other_ref, plane_ref, q_ref, acc, carry, tri, level_buf, penalty_buf
+    at_ref, own_ref, other_ref, half_ref, across_ref, q_ref, acc, carry,
+    tri, level_buf, penalty_buf, plane,
 ):
     tok = own_ref.shape[0]
     heads = own_ref.shape[1] // HD
@@ -122,10 +128,10 @@
             q_ref[target, 0:HD] = high
             q_ref[target, HD : 2 * HD] = (scaled - high.astype(jnp.float32)).astype(jnp.bfloat16)
     clear(acc, carry, tri)
+    join_halves(at_ref, half_ref, across_ref, plane)
     first_row = pl.multiple_of(core * rows, rows)
     scores, mix, both = block_steps(
-        q_ref, plane_ref, acc, carry, tri, level_buf, penalty_buf, first_row, tok,
-        plane_ref.shape[0] // 2 * core,
+        q_ref, plane, acc, carry, tri, level_buf, penalty_buf, first_row, tok
     )
     pos = 2 * at_ref[1] + core
     scores(pos, 0, diagonal=True)
@@ -148,24 +154,34 @@
 
 
 def plane_kernel(
-    distance, z_size, tok, last, at_ref, q_ref, plane_ref, acc_in, total_in, acc_out, total_out,
-    acc, carry, tri, level_buf, penalty_buf
+    distance, z_size, tok, last, at_ref, q_ref, half_ref, across_ref, acc_in, total_in, *refs
 ):
+    outs, (acc, carry, tri, level_buf, penalty_buf, plane) = refs[:2], refs[2:]
     rows = acc.shape[0]
     core = at_ref[2]
     below = jnp.where(core == 0, distance, z_size - distance)
-    shards = plane_ref.shape[0]
+    visible = below <= at_ref[0]
+    shards = half_ref.shape[0] if last else 2 * half_ref.shape[0]
+    upward = core == 0
+
+    @pl.when(visible)
+    def _():
+        if last:
+            direct = (at_ref[1] // 2) == 1 - core
+            for k in range(shards):
+                plane[k] = jnp.where(direct, half_ref[k], across_ref[k])
+        else:
+            join_halves(at_ref, half_ref, across_ref, plane)
 
     def part(h, _):
         first_row = pl.multiple_of(h * rows, rows)
         here = pl.ds(first_row, rows)
         clear(acc, carry, tri)
 
-        @pl.when(below <= at_ref[0])
+        @pl.when(visible)
         def _():
             scores, mix, both = block_steps(
-                q_ref, plane_ref, acc, carry, tri, level_buf, penalty_buf, first_row, tok,
-                0 if last else shards // 2 * core,
+                q_ref, plane, acc, carry, tri, level_buf, penalty_buf, first_row, tok
             )
             scores(shards - 1, 0)
 
@@ -180,27 +196,29 @@
 
         old, old_total = acc_in[here, :], total_in[here, :]
         new, new_total = acc[...], carry[...]
-        upward = core == 0
         result = old * jnp.exp2(jnp.where(upward, 0.0, -new_total))
         result = result + new * jnp.exp2(jnp.where(upward, -old_total, 0.0))
+        total = old_total + new_total
         if last:
-            place = jnp.where(h == core, 0, 1)
-            acc_out[place] = result
-            total_out[place] = old_total + new_total
+            for owned, out in ((True, outs[0]), (False, outs[1])):
+
+                @pl.when((h == core) == owned)
+                def _(out=out):
+                    out[0] = result
+                    out[1] = total
         else:
-            acc_out[here, :] = result
-            total_out[here, :] = old_total + new_total
+            outs[0][here, :] = result
+            outs[1][here, :] = total
         return 0
 
     lax.fori_loop(0, 2, part, 0)
 
 
-def merge_kernel(at_ref, own_ref, own_total, acc_ref, total_ref, theirs, their_total, out_ref):
+def merge_kernel(at_ref, own_ref, own_total, mine, theirs, out_ref):
     upward = at_ref[2] == 0
     tok = out_ref.shape[0]
-    mine, other = acc_ref[0], theirs[...]
-    newer_total = jnp.where(upward, total_ref[0], their_total[...])
-    newer, older = jnp.where(upward, mine, other), jnp.where(upward, other, mine)
+    newer_total = jnp.where(upward, mine[1], theirs[1])
+    newer, older = jnp.where(upward, mine[0], theirs[0]), jnp.where(upward, theirs[0], mine[0])
     mixed = own_ref[...] + jnp.exp2(-own_total[...]) * (newer + jnp.exp2(-newer_total) * older)
     for g in range(out_ref.shape[1] // HD):
         out_ref[:, g * HD : (g + 1) * HD] = mixed[g * tok : (g + 1) * tok].astype(out_ref.dtype)
@@ -210,59 +228,58 @@
     z_size, y_size = lax.axis_size("sp_0"), lax.axis_size("sp_1")
     tok = query.shape[0]
     rows = tok * (query.shape[1] // HD)
-    other_query = shifted(query, "sp_2", 1)
     pair = jnp.concatenate([keys, values], axis=1)
-    ring = [pair] + [None] * (y_size - 1)
-    down = up = pair
-    for k in range(1, y_size // 2 + 1):
-        down = ring[k] = shifted(down, "sp_1", 1)
-        if k < y_size - k:
-            up = ring[y_size - k] = shifted(up, "sp_1", -1)
-    own_rows = jnp.stack(ring)
-    (plane,) = call(
-        functools.partial(assemble_kernel, y_size),
-        [((2 * y_size, tok, 2 * HD), jnp.bfloat16)],
+    near = lax.ppermute(pair, "sp_1", [(i, i ^ 1) for i in range(y_size)])
+    own_rows = jnp.stack([pair, near])
+    (half,) = call(
+        assemble_kernel,
+        [((y_size, tok, 2 * HD), jnp.bfloat16)],
         (at, own_rows, shifted(own_rows, "sp_2", 1)),
     )
+
+    def from_across(value):
+        return lax.ppermute(value, "sp_1", [(i, y_size - 1 - i) for i in range(y_size)])
+
     scratch = [
         pltpu.VMEM((BK, BK), jnp.bfloat16),
         pltpu.VMEM((2, rows, BK), jnp.float32),
         pltpu.VMEM((2, rows, BK), jnp.bfloat16),
+        pltpu.VMEM((2 * y_size, tok, 2 * HD), jnp.bfloat16),
     ]
     state = ((rows, HD), jnp.float32)
     both_state = ((2 * rows, HD), jnp.float32)
     work = 2 * y_size * rows * BK * HD * 16
+    across = from_across(half)
+    other_query = shifted(query, "sp_2", 1)
     doubled, own, own_total = call(
         own_plane_kernel,
         [((2 * rows, 2 * HD), jnp.bfloat16), state, state],
-        (at, query, other_query, plane),
+        (at, query, other_query, half, across),
         scratch,
         work // 2,
     )
     acc = total = jnp.zeros(*both_state)
-    done = own
     for k in range(1, z_size // 2 + 1):
         last = k == z_size // 2
-        if k > 1:
-            plane, done = lax.optimization_barrier((plane, done))
-            if k == 2:
-                own = done
-            done = acc
-        if last:
-            plane = plane[y_size:]
-        plane = counter_shifted(plane)
+        if k == 3:
+            half, own = lax.optimization_barrier((half, own))
+        if k == 4:
+            half, before = lax.optimization_barrier((half, before))
+        half = counter_shifted(half)
+        across = from_across(half)
         acc, total = call(
             functools.partial(plane_kernel, k, z_size, tok, last),
             [((2, rows, HD), jnp.float32)] * 2 if last else [both_state] * 2,
-            (at, doubled, plane, acc, total),
+            (at, doubled, half, across, acc, total),
             [pltpu.VMEM((rows, HD), jnp.float32)] * 2 + scratch,
             work * 2,
         )
-    theirs = shifted(jnp.stack([acc[1], total[1]]), "sp_2", 1)
+        if k == 1:
+            before = acc
     return call(
         merge_kernel,
         [((tok, query.shape[1]), jnp.bfloat16)],
-        (at, own, own_total, acc, total, theirs[0], theirs[1]),
+        (at, own, own_total, acc, shifted(total, "sp_2", 1)),
     )[0]
 
 

time: 236 us -> 237 us (level)
  waiting for transfers between devices: 111 us -> 97.2 us
  starting transfers between devices: 23.1 us -> 32.7 us
  Pallas kernels: 19.2 us -> 21.7 us
    ppermute x4, waiting for transfers between devices: 37.2 us -> 17.5 us  [counter_shifted(): return lax.ppermute(value, ('sp_0', 'sp_2'), pairs)]
    ppermute x0 -> x6, waiting for transfers between devices: none -> 17.4 us  [the longest x5 14.3 us: from_across(): lax.ppermute(value, 'sp_1', [(i, y_size - 1 - i) for i in range(y_size)])]
    ppermute x9 -> x6, waiting for transfers between devices: 28.2 us -> 12 us  [shifted(): lax.ppermute(value, axis, [(i, (i + step) % size) for i in range(size)])]
    ppermute x0 -> x6, starting transfers between devices: none -> 9 us  [the longest x5 6.76 us: from_across(): lax.ppermute(value, 'sp_1', [(i, y_size - 1 - i) for i in range(y_size)])]
    all_to_all x1, waiting for transfers between devices: 0.6 us -> 5.01 us  [per_device(): lax.all_to_all(heads_out.reshape(-1, own_rows, heads_out.shape[1]), 'tp',...]
    ppermute x4, starting transfers between devices: 0.93 us -> 4.21 us  [counter_shifted(): return lax.ppermute(value, ('sp_0', 'sp_2'), pairs)]
    ppermute x9 -> x6, starting transfers between devices: 12.4 us -> 9.64 us  [shifted(): lax.ppermute(value, axis, [(i, (i + step) % size) for i in range(size)])]
    unnamed x57, local copies, waits for them, and re-layouts: 13.2 us -> 15.9 us
  transfers between devices with their start and end apart: 15 -> 18, of which waited for: 12 -> 13; matrix products, arithmetic and copies ran while one was open for 2% -> 1% of each run, Pallas kernels for 4% -> 5%
where the time goes in v1:
time: 237 us; the launch traced here: 236 us
  waiting for transfers between devices  97.2 us (41%)
  blocking collectives  65 us (27%)
  starting transfers between devices  32.7 us (14%)
  Pallas kernels  21.7 us (9%)
  local copies, waits for them, and re-layouts  17.9 us (8%)
    all_to_all x1, blocking collectives, per_device(): arrived = lax.all_to_all(outgoing.reshape(exchange), SP, 0, 0, tiled=True)  65 us
    all_to_all x1, waiting for transfers between devices, per_device(): returned = lax.all_to_all(produced.reshape(exchange), SP, 0, 0, tiled=True)  45.4 us
    pallas_call x11, Pallas kernels, call(): pl.pallas_call(kernel, out_shape=[jax.ShapeDtypeStruct(*out) for out in o...  21.7 us
    ppermute x4, waiting for transfers between devices, counter_shifted(): return lax.ppermute(value, ('sp_0', 'sp_2'), pairs)  17.5 us
    unnamed x57, local copies, waits for them, and re-layouts  15.9 us
    ppermute x5, waiting for transfers between devices, from_across(): lax.ppermute(value, 'sp_1', [(i, y_size - 1 - i) for i in range(y_size)])  14.3 us
    ppermute x6, waiting for transfers between devices, shifted(): lax.ppermute(value, axis, [(i, (i + step) % size) for i in range(size)])  12 us
    ppermute x6, starting transfers between devices, shifted(): lax.ppermute(value, axis, [(i, (i + step) % size) for i in range(size)])  9.64 us
  transfers between devices with their start and end apart: 18, of which 13 were waited for; matrix products, arithmetic and copies ran while one was open for 1% of the time, Pallas kernels for 5%

profile of v1, /device:TPU:8, one launch (start us, length us, event | category | flops | bytes accessed | tf_op | source)
XLA Modules:
  0.0 236.3 jit_solution(8945570640808346835)
XLA Ops:
  1.8 2.2 collective-permute-start
  4.0 3.1 %collective-permute-done = bf16[256,256]{1,0:T(8,128)(2,1)S(1)} collective-permute-done((bf16[256,256]{1,0:T(8,128)(2,1)S(1)}, bf16[256,256]{1,0:T(8,128)(2,1)S(1)}, u32[]{:S(2)}, u32[]{:S(2)}) %collective-permute-start) | collective-permute-done | bytes 131104 | tf_op jit(solution)/shard_map/ppermute | solution.py:232
  9.3 2.0 collective-permute-start.2
  11.3 1.6 collective-permute-start.5
  12.9 9.5 %collective-permute-done.2.half_ref = bf16[4,256,256]{2,1,0:T(8,128)(2,1)S(1)} collective-permute-done((bf16[4,256,256]{2,1,0:T(8,128)(2,1)S(1)}, bf16[4,256,256]{2,1,0:T(8,128)(2,1)S(1)}, u32[]{:S(2)}, u32[]{:S(2)}) %collective-permute-start.2) | collective-permute-done | bytes 524320 | tf_op jit(solution)/shard_map/ppermute | solution.py:33
  22.4 1.6 collective-permute-start.7
  24.0 1.7 collective-permute-start.4
  26.7 2.2 shard_map.137
  29.5 3.4 %collective-permute-done.3.half_ref = bf16[4,256,256]{2,1,0:T(8,128)(2,1)} collective-permute-done((bf16[4,256,256]{2,1,0:T(8,128)(2,1)S(1)}, bf16[4,256,256]{2,1,0:T(8,128)(2,1)}, u32[]{:S(2)}, u32[]{:S(2)}) %collective-permute-start.3) | collective-permute-done | bytes 524320 | tf_op jit(solution)/shard_map/ppermute | solution.py:33
  34.4 2.1 collective-permute-done.7.across_ref
  39.1 4.6 %collective-permute-done.6.half_ref = bf16[4,256,256]{2,1,0:T(8,128)(2,1)} collective-permute-done((bf16[4,256,256]{2,1,0:T(8,128)(2,1)}, bf16[4,256,256]{2,1,0:T(8,128)(2,1)}, u32[]{:S(2)}, u32[]{:S(2)}) %collective-permute-start.6) | collective-permute-done | bytes 524320 | tf_op jit(solution)/shard_map/ppermute | solution.py:33
  43.6 2.2 collective-permute-start.8
  45.9 1.6 collective-permute-start.11
  47.9 2.8 %collective-permute-start.15 = (bf16[256,2048]{1,0:T(8,128)(2,1)S(1)}, bf16[256,2048]{1,0:T(8,128)(2,1)S(1)}, u32[]{:S(2)}, u32[]{:S(2)}) collective-permute-start(bf16[256,2048]{1,0:T(8,128)(2,1)S(1)} %copy-done.4), channel_id=1, source_target_pairs={{0,3},{1,0},{2,1},{3,2},{4,7},{5,4},{6,5},{7,6},{8,11},{9,8},{10,9... | collective-permute-start | bytes 3145736 | tf_op jit(solution)/shard_map/ppermute | solution.py:26
  51.5 8.5 %collective-permute-done.13.w1 = bf16[256,2048]{1,0:T(8,128)(2,1)S(1)} collective-permute-done((bf16[256,2048]{1,0:T(8,128)(2,1)S(1)}, bf16[256,2048]{1,0:T(8,128)(2,1)S(1)}, u32[]{:S(2)}, u32[]{:S(2)}) %collective-permute-start.13) | collective-permute-done | bytes 1048608 | tf_op jit(solution)/shard_map/ppermute | solution.py:26
  60.3 1.6 collective-permute-start.9
  65.0 1.5 shard_map.139
  66.5 2.6 %collective-permute-done.10.across_ref = bf16[4,256,256]{2,1,0:T(8,128)(2,1)} collective-permute-done((bf16[4,256,256]{2,1,0:T(8,128)(2,1)}, bf16[4,256,256]{2,1,0:T(8,128)(2,1)}, u32[]{:S(2)}, u32[]{:S(2)}) %collective-permute-start.10) | collective-permute-done | bytes 524320 | tf_op jit(solution)/shard_map/ppermute | solution.py:241
  69.1 1.5 shard_map.140
  70.6 9.6 %collective-permute-done.9.across_ref = bf16[4,256,256]{2,1,0:T(8,128)(2,1)S(1)} collective-permute-done((bf16[4,256,256]{2,1,0:T(8,128)(2,1)}, bf16[4,256,256]{2,1,0:T(8,128)(2,1)S(1)}, u32[]{:S(2)}, u32[]{:S(2)}) %collective-permute-start.9) | collective-permute-done | bytes 524320 | tf_op jit(solution)/shard_map/ppermute | solution.py:241
  80.2 2.2 shard_map.141
  83.2 3.4 %collective-permute-start.12 = (f32[2,512,128]{2,1,0:T(8,128)}, f32[2,512,128]{2,1,0:T(8,128)}, u32[]{:S(2)}, u32[]{:S(2)}) collective-permute-start(f32[2,512,128]{2,1,0:T(8,128)} %get-tuple-element.35), channel_id=1, source_target_pairs={{0,4},{4,0},{1,5},{5,1},{2,6},{6,2},{3,7},{7,3},{8,12},{12,8},{9,1... | collective-permute-start | bytes 1572872 | tf_op jit(solution)/shard_map/ppermute | solution.py:26
  90.5 1.8 shard_map.142
  92.3 4.3 %all-to-all-start = ((bf16[4,64,256]{2,1,0:T(8,128)(2,1)}), bf16[4,64,256]{2,1,0:T(8,128)(2,1)S(1)}, u32[]{:S(2)}, u32[]{:S(2)}) async-start(bf16[4,64,256]{2,1,0:T(8,128)(2,1)} %bitcast.6), calls=%async_computation | async-start | bytes 262144 | tf_op jit(solution)/shard_map/all_to_all | solution.py:385
  97.6 5.0 %all-to-all-done.heads_ref = bf16[4,64,256]{2,1,0:T(8,128)(2,1)S(1)} async-done(((bf16[4,64,256]{2,1,0:T(8,128)(2,1)}), bf16[4,64,256]{2,1,0:T(8,128)(2,1)S(1)}, u32[]{:S(2)}, u32[]{:S(2)}) %all-to-all-start) | async-done | bytes 131104 | tf_op jit(solution)/shard_map/all_to_all | solution.py:385
  103.5 3.0 %shard_map.143 = (bf16[64,2048]{1,0:T(8,128)(2,1)S(1)}, bf16[64,2048]{1,0:T(8,128)(2,1)S(1)}, bf16[512,2048]{1,0:T(8,128)(2,1)S(1)}) custom-call(s32[4]{0:T(128)S(1)} %pad_add_fusion.at_ref, bf16[4,64,256]{2,1,0:T(8,128)(2,1)S(1)} %all-to-all-done.heads_ref, bf16[256,2048]{1,0:T(8,128)(2,1)S(1)} %copy-done.4, ...), custom_call_target="tpu_custom_call" | custom-call | flops 536870912 | bytes 1048576 | tf_op jit(solution)/shard_map/pallas_call | solution.py:37
  106.6 65.0 %all_to_all.15 = bf16[64,8,2048]{2,1,0:T(8,128)(2,1)S(1)} all-to-all(bf16[64,8,2048]{2,1,0:T(8,128)(2,1)S(1)} %bitcast.36), channel_id=1, replica_groups=mesh['sp_0'=8,'sp_1'=4,'sp_2'=2,'tp'=4] {'sp_0','sp_1','sp_2'}, dimensions={0} | all-to-all | bytes 4194304 | tf_op jit(solution)/shard_map/all_to_all | solution.py:396
  171.6 4.3 %shard_map.145 = bf16[512,2048]{1,0:T(8,128)(2,1)S(1)} custom-call(s32[4]{0:T(128)S(1)} %pad_add_fusion.at_ref, bf16[512,2048]{1,0:T(8,128)(2,1)S(1)} %bitcast.37, bf16[2048,384]{1,0:T(8,128)(2,1)S(1)} %bitcast.39, bf16[2048,384]{1,0:T(8,128)(2,1)S(1)} %bitcast.40, bf16[384,2048]{1,0:T(8,128)(2,1)S(1)} %bitcast.41), custom_call_target="tpu_custom_call" | custom-call | flops 4294967296 | bytes 1048576 | tf_op jit(solution)/shard_map/pallas_call | solution.py:37
  177.3 5.6 %all-to-all-start.2 = ((bf16[64,8,2048]{2,1,0:T(8,128)(2,1)}), bf16[64,8,2048]{2,1,0:T(8,128)(2,1)S(1)}, u32[]{:S(2)}, u32[]{:S(2)}) async-start(bf16[64,8,2048]{2,1,0:T(8,128)(2,1)} %bitcast.35), calls=%async_computation.2 | async-start | bytes 4194304 | tf_op jit(solution)/shard_map/all_to_all | solution.py:403
  187.3 1.5 shard_map.144.base_ref
  188.8 45.4 %all-to-all-done.2 = bf16[64,8,2048]{2,1,0:T(8,128)(2,1)S(1)} async-done(((bf16[64,8,2048]{2,1,0:T(8,128)(2,1)}), bf16[64,8,2048]{2,1,0:T(8,128)(2,1)S(1)}, u32[]{:S(2)}, u32[]{:S(2)}) %all-to-all-start.2) | async-done | bytes 2097184 | tf_op jit(solution)/shard_map/all_to_all | solution.py:403
  234.1 2.2 shard_map.146
  (89 shorter events, 26.6 us)
Async XLA Ops:
  0.0 24.0 %copy-start.18 = (bf16[256,256]{1,0:T(8,128)(2,1)S(1)}, bf16[256,256]{1,0:T(8,128)(2,1)}, u32[]{:S(2)}) copy-start(bf16[256,256]{1,0:T(8,128)(2,1)} %own_ref.1) | copy-start | bytes 393220
  1.8 5.3 %collective-permute-start = (bf16[256,256]{1,0:T(8,128)(2,1)S(1)}, bf16[256,256]{1,0:T(8,128)(2,1)S(1)}, u32[]{:S(2)}, u32[]{:S(2)}) collective-permute-start(bf16[256,256]{1,0:T(8,128)(2,1)S(1)} %constant_dynamic-update-slice_fusion), channel_id=1, source_target_pairs={{0,8},{8,0},{16,24},{24,16},{1,9},{9,1},{17,25},{25,17},{2,10},{10... | collective-permute-start | bytes 393224 | tf_op jit(solution)/shard_map/ppermute | solution.py:232
  7.1 1.6 collective-permute-start.1
  9.3 23.6 %copy-start.4 = (bf16[256,2048]{1,0:T(8,128)(2,1)S(1)}, bf16[256,2048]{1,0:T(8,128)(2,1)}, u32[]{:S(2)}) copy-start(bf16[256,2048]{1,0:T(8,128)(2,1)} %w0.1) | copy-start | bytes 3145732
  9.3 13.1 %collective-permute-start.2 = (bf16[4,256,256]{2,1,0:T(8,128)(2,1)S(1)}, bf16[4,256,256]{2,1,0:T(8,128)(2,1)S(1)}, u32[]{:S(2)}, u32[]{:S(2)}) collective-permute-start(bf16[4,256,256]{2,1,0:T(8,128)(2,1)S(1)} %shard_map.136.half_ref), channel_id=1, source_target_pairs={{0,32},{32,64},{64,96},{96,128},{128,160},{160,192},{192,224},{224... | collective-permute-start | bytes 1572872 | tf_op jit(solution)/shard_map/ppermute | solution.py:33
  11.3 15.3 %collective-permute-start.5 = (bf16[4,256,256]{2,1,0:T(8,128)(2,1)S(1)}, bf16[4,256,256]{2,1,0:T(8,128)(2,1)S(1)}, u32[]{:S(2)}, u32[]{:S(2)}) collective-permute-start(bf16[4,256,256]{2,1,0:T(8,128)(2,1)S(1)} %shard_map.136.half_ref), channel_id=1, source_target_pairs={{0,24},{8,16},{16,8},{24,0},{1,25},{9,17},{17,9},{25,1},{2,26},{10... | collective-permute-start | bytes 1572872 | tf_op jit(solution)/shard_map/ppermute | solution.py:241
  22.4 10.5 %collective-permute-start.3 = (bf16[4,256,256]{2,1,0:T(8,128)(2,1)S(1)}, bf16[4,256,256]{2,1,0:T(8,128)(2,1)}, u32[]{:S(2)}, u32[]{:S(2)}) collective-permute-start(bf16[4,256,256]{2,1,0:T(8,128)(2,1)S(1)} %collective-permute-done.2.half_ref), channel_id=1, source_target_pairs={{0,32},{32,64},{64,96},{96,128},{128,160},{160,192},{192,224},{224... | collective-permute-start | bytes 1572872 | tf_op jit(solution)/shard_map/ppermute | solution.py:33
  22.4 14.1 %collective-permute-start.7 = (bf16[4,256,256]{2,1,0:T(8,128)(2,1)S(1)}, bf16[4,256,256]{2,1,0:T(8,128)(2,1)S(1)}, u32[]{:S(2)}, u32[]{:S(2)}) collective-permute-start(bf16[4,256,256]{2,1,0:T(8,128)(2,1)S(1)} %collective-permute-done.2.half_ref), channel_id=1, source_target_pairs={{0,24},{8,16},{16,8},{24,0},{1,25},{9,17},{17,9},{25,1},{2,26},{10... | collective-permute-start | bytes 1572872 | tf_op jit(solution)/shard_map/ppermute | solution.py:241
  24.0 2.6 %collective-permute-start.4 = (bf16[256,256]{1,0:T(8,128)(2,1)S(1)}, bf16[256,256]{1,0:T(8,128)(2,1)S(1)}, u32[]{:S(2)}, u32[]{:S(2)}) collective-permute-start(bf16[256,256]{1,0:T(8,128)(2,1)S(1)} %copy-done.18), channel_id=1, source_target_pairs={{0,4},{4,0},{1,5},{5,1},{2,6},{6,2},{3,7},{7,3},{8,12},{12,8},{9,1... | collective-permute-start | bytes 393224 | tf_op jit(solution)/shard_map/ppermute | solution.py:26
  29.5 7.9 %copy-start.19 = (bf16[1024,256]{1,0:T(8,128)(2,1)}, bf16[1024,256]{1,0:T(8,128)(2,1)S(1)}, u32[]{:S(2)}) copy-start(bf16[1024,256]{1,0:T(8,128)(2,1)S(1)} %get-tuple-element.25.q_ref) | copy-start | bytes 1572868
  32.9 10.7 %collective-permute-start.6 = (bf16[4,256,256]{2,1,0:T(8,128)(2,1)}, bf16[4,256,256]{2,1,0:T(8,128)(2,1)}, u32[]{:S(2)}, u32[]{:S(2)}) collective-permute-start(bf16[4,256,256]{2,1,0:T(8,128)(2,1)} %collective-permute-done.3.half_ref), channel_id=1, source_target_pairs={{0,32},{32,64},{64,96},{96,128},{128,160},{160,192},{192,224},{224... | collective-permute-start | bytes 1572872 | tf_op jit(solution)/shard_map/ppermute | solution.py:33
  32.9 27.1 %collective-permute-start.13 = (bf16[256,2048]{1,0:T(8,128)(2,1)S(1)}, bf16[256,2048]{1,0:T(8,128)(2,1)S(1)}, u32[]{:S(2)}, u32[]{:S(2)}) collective-permute-start(bf16[256,2048]{1,0:T(8,128)(2,1)S(1)} %copy-done.4), channel_id=1, source_target_pairs={{0,1},{1,2},{2,3},{3,0},{4,5},{5,6},{6,7},{7,4},{8,9},{9,10},{10,1... | collective-permute-start | bytes 3145736 | tf_op jit(solution)/shard_map/ppermute | solution.py:26
  36.6 14.1 %copy-start.25 = (s32[64,4]{0,1:T(4,128)S(1)}, s32[64,4]{0,1:T(4,128)}, u32[]{:S(2)}) copy-start(s32[64,4]{0,1:T(4,128)} %param.20) | copy-start | bytes 3076
  43.6 16.6 %collective-permute-start.8 = (bf16[4,256,256]{2,1,0:T(8,128)(2,1)}, bf16[4,256,256]{2,1,0:T(8,128)(2,1)}, u32[]{:S(2)}, u32[]{:S(2)}) collective-permute-start(bf16[4,256,256]{2,1,0:T(8,128)(2,1)} %collective-permute-done.6.half_ref), channel_id=1, source_target_pairs={{0,32},{32,64},{64,96},{96,128},{128,160},{160,192},{192,224},{224... | collective-permute-start | bytes 1572872 | tf_op jit(solution)/shard_map/ppermute | solution.py:33
  45.9 16.0 %collective-permute-start.11 = (bf16[4,256,256]{2,1,0:T(8,128)(2,1)}, bf16[4,256,256]{2,1,0:T(8,128)(2,1)}, u32[]{:S(2)}, u32[]{:S(2)}) collective-permute-start(bf16[4,256,256]{2,1,0:T(8,128)(2,1)} %collective-permute-done.3.half_ref), channel_id=1, source_target_pairs={{0,24},{8,16},{16,8},{24,0},{1,25},{9,17},{17,9},{25,1},{2,26},{10... | collective-permute-start | bytes 1572872 | tf_op jit(solution)/shard_map/ppermute | solution.py:241
  47.4 21.6 %collective-permute-start.10 = (bf16[4,256,256]{2,1,0:T(8,128)(2,1)}, bf16[4,256,256]{2,1,0:T(8,128)(2,1)}, u32[]{:S(2)}, u32[]{:S(2)}) collective-permute-start(bf16[4,256,256]{2,1,0:T(8,128)(2,1)} %collective-permute-done.6.half_ref), channel_id=1, source_target_pairs={{0,24},{8,16},{16,8},{24,0},{1,25},{9,17},{17,9},{25,1},{2,26},{10... | collective-permute-start | bytes 1572872 | tf_op jit(solution)/shard_map/ppermute | solution.py:241
  47.9 49.7 %collective-permute-start.15 = (bf16[256,2048]{1,0:T(8,128)(2,1)S(1)}, bf16[256,2048]{1,0:T(8,128)(2,1)S(1)}, u32[]{:S(2)}, u32[]{:S(2)}) collective-permute-start(bf16[256,2048]{1,0:T(8,128)(2,1)S(1)} %copy-done.4), channel_id=1, source_target_pairs={{0,3},{1,0},{2,1},{3,2},{4,7},{5,4},{6,5},{7,6},{8,11},{9,8},{10,9... | collective-permute-start | bytes 3145736 | tf_op jit(solution)/shard_map/ppermute | solution.py:26
  60.0 37.6 %collective-permute-start.14 = (bf16[256,2048]{1,0:T(8,128)(2,1)S(1)}, bf16[256,2048]{1,0:T(8,128)(2,1)}, u32[]{:S(2)}, u32[]{:S(2)}) collective-permute-start(bf16[256,2048]{1,0:T(8,128)(2,1)S(1)} %collective-permute-done.13.w1), channel_id=1, source_target_pairs={{0,1},{1,2},{2,3},{3,0},{4,5},{5,6},{6,7},{7,4},{8,9},{9,10},{10,1... | collective-permute-start | bytes 3145736 | tf_op jit(solution)/shard_map/ppermute | solution.py:26
  60.3 19.9 %collective-permute-start.9 = (bf16[4,256,256]{2,1,0:T(8,128)(2,1)}, bf16[4,256,256]{2,1,0:T(8,128)(2,1)S(1)}, u32[]{:S(2)}, u32[]{:S(2)}) collective-permute-start(bf16[4,256,256]{2,1,0:T(8,128)(2,1)} %collective-permute-done.8.half_ref), channel_id=1, source_target_pairs={{0,24},{8,16},{16,8},{24,0},{1,25},{9,17},{17,9},{25,1},{2,26},{10... | collective-permute-start | bytes 1572872 | tf_op jit(solution)/shard_map/ppermute | solution.py:241
  83.2 19.3 %copy-start.14 = (f32[2048]{0:T(1024)S(1)}, f32[2048]{0:T(1024)}, u32[]{:S(2)}) copy-start(f32[2048]{0:T(1024)} %param.19) | copy-start | bytes 24580
  83.2 5.2 %collective-permute-start.12 = (f32[2,512,128]{2,1,0:T(8,128)}, f32[2,512,128]{2,1,0:T(8,128)}, u32[]{:S(2)}, u32[]{:S(2)}) collective-permute-start(f32[2,512,128]{2,1,0:T(8,128)} %get-tuple-element.35), channel_id=1, source_target_pairs={{0,4},{4,0},{1,5},{5,1},{2,6},{6,2},{3,7},{7,3},{8,12},{12,8},{9,1... | collective-permute-start | bytes 1572872 | tf_op jit(solution)/shard_map/ppermute | solution.py:26
  92.3 10.3 %all-to-all-start = ((bf16[4,64,256]{2,1,0:T(8,128)(2,1)}), bf16[4,64,256]{2,1,0:T(8,128)(2,1)S(1)}, u32[]{:S(2)}, u32[]{:S(2)}) async-start(bf16[4,64,256]{2,1,0:T(8,128)(2,1)} %bitcast.6), calls=%async_computation | async-start | bytes 262144 | tf_op jit(solution)/shard_map/all_to_all | solution.py:385
  103.5 68.1 %copy-start.17 = (bf16[1,384,2048]{2,1,0:T(8,128)(2,1)S(1)}, bf16[1,384,2048]{2,1,0:T(8,128)(2,1)}, u32[]{:S(2)}) copy-start(bf16[1,384,2048]{2,1,0:T(8,128)(2,1)} %param.24) | copy-start | bytes 4718596
  106.5 65.1 %copy-start.10 = (bf16[64,2048]{1,0:T(8,128)(2,1)}, bf16[64,2048]{1,0:T(8,128)(2,1)S(1)}, u32[]{:S(2)}) copy-start(bf16[64,2048]{1,0:T(8,128)(2,1)S(1)} %get-tuple-element.37.mid_ref) | copy-start | bytes 786436
  106.5 65.1 %copy-start.12 = (bf16[64,2048]{1,0:T(8,128)(2,1)}, bf16[64,2048]{1,0:T(8,128)(2,1)S(1)}, u32[]{:S(2)}) copy-start(bf16[64,2048]{1,0:T(8,128)(2,1)S(1)} %get-tuple-element.36.normed_ref) | copy-start | bytes 786436
  106.5 65.1 %copy-start.15 = (bf16[1,2048,384]{2,1,0:T(8,128)(2,1)S(1)}, bf16[1,2048,384]{2,1,0:T(8,128)(2,1)}, u32[]{:S(2)}) copy-start(bf16[1,2048,384]{2,1,0:T(8,128)(2,1)} %param.22) | copy-start | bytes 4718596
  106.6 65.1 %copy-start.16 = (bf16[1,2048,384]{2,1,0:T(8,128)(2,1)S(1)}, bf16[1,2048,384]{2,1,0:T(8,128)(2,1)}, u32[]{:S(2)}) copy-start(bf16[1,2048,384]{2,1,0:T(8,128)(2,1)} %param.23) | copy-start | bytes 4718596
  177.3 5.6 %copy-start.26 = (f32[64,4]{0,1:T(4,128)S(1)}, f32[64,4]{0,1:T(4,128)}, u32[]{:S(2)}) copy-start(f32[64,4]{0,1:T(4,128)} %param.21) | copy-start | bytes 3076
  177.3 5.7 %copy-start.11 = (bf16[64,2048]{1,0:T(8,128)(2,1)S(1)}, bf16[64,2048]{1,0:T(8,128)(2,1)}, u32[]{:S(2)}) copy-start(bf16[64,2048]{1,0:T(8,128)(2,1)} %copy-done.10) | copy-start | bytes 786436
  177.3 5.7 %copy-start.13 = (bf16[64,2048]{1,0:T(8,128)(2,1)S(1)}, bf16[64,2048]{1,0:T(8,128)(2,1)}, u32[]{:S(2)}) copy-start(bf16[64,2048]{1,0:T(8,128)(2,1)} %copy-done.12) | copy-start | bytes 786436
  177.3 56.8 %all-to-all-start.2 = ((bf16[64,8,2048]{2,1,0:T(8,128)(2,1)}), bf16[64,8,2048]{2,1,0:T(8,128)(2,1)S(1)}, u32[]{:S(2)}, u32[]{:S(2)}) async-start(bf16[64,8,2048]{2,1,0:T(8,128)(2,1)} %bitcast.35), calls=%async_computation.2 | async-start | bytes 4194304 | tf_op jit(solution)/shard_map/all_to_all | solution.py:403
  183.0 1.4 copy-start.1
  (13 other events, 13.4 us)

commit v2 on v1

--- a/solution.py
+++ b/solution.py
@@ -34,12 +34,13 @@
 
 
 def call(kernel, outs, args, scratch=(), flops=0):
+    near = pl.BlockSpec(memory_space=pltpu.VMEM)
     return pl.pallas_call(
         kernel,
         out_shape=[jax.ShapeDtypeStruct(*out) for out in outs],
         in_specs=[pl.BlockSpec(memory_space=pltpu.SMEM)]
-        + [pl.BlockSpec(memory_space=pltpu.VMEM)] * (len(args) - 1),
-        out_specs=[pl.BlockSpec(memory_space=pltpu.VMEM)] * len(outs),
+        + [near] * (len(args) - 1),
+        out_specs=[near] * len(outs),
         scratch_shapes=list(scratch),
         compiler_params=pltpu.CompilerParams(vmem_limit_bytes=24 * 2**20),
         cost_estimate=pl.CostEstimate(flops=flops, bytes_accessed=2**20, transcendentals=0),
@@ -112,26 +113,31 @@
     tri[...] = later.astype(jnp.float32).astype(jnp.bfloat16)
 
 
-def own_plane_kernel(
-    at_ref, own_ref, other_ref, half_ref, across_ref, q_ref, acc, carry,
-    tri, level_buf, penalty_buf, plane,
-):
+def scale_queries(at_ref, own_ref, other_ref, q_ref):
     tok = own_ref.shape[0]
     heads = own_ref.shape[1] // HD
-    rows = tok * heads
     core = at_ref[2]
     for place, ref in ((core, own_ref), (1 - core, other_ref)):
         for g in range(heads):
             scaled = ref[:, g * HD : (g + 1) * HD].astype(jnp.float32) * SCALE
             high = scaled.astype(jnp.bfloat16)
-            target = pl.ds(pl.multiple_of(place * rows + g * tok, tok), tok)
+            target = pl.ds(pl.multiple_of(place * tok * heads + g * tok, tok), tok)
             q_ref[target, 0:HD] = high
             q_ref[target, HD : 2 * HD] = (scaled - high.astype(jnp.float32)).astype(jnp.bfloat16)
+
+
+def own_plane_kernel(
+    at_ref, own_ref, other_ref, half_ref, across_ref, out_ref,
+    q_buf, acc, carry, tri, level_buf, penalty_buf, plane,
+):
+    rows = acc.shape[0]
+    core = at_ref[2]
+    scale_queries(at_ref, own_ref, other_ref, q_buf)
     clear(acc, carry, tri)
     join_halves(at_ref, half_ref, across_ref, plane)
     first_row = pl.multiple_of(core * rows, rows)
     scores, mix, both = block_steps(
-        q_ref, plane, acc, carry, tri, level_buf, penalty_buf, first_row, tok
+        q_buf, plane, acc, carry, tri, level_buf, penalty_buf, first_row, own_ref.shape[0]
     )
     pos = 2 * at_ref[1] + core
     scores(pos, 0, diagonal=True)
@@ -152,11 +158,19 @@
     def _():
         mix(0, 0)
 
-
-def plane_kernel(
-    distance, z_size, tok, last, at_ref, q_ref, half_ref, across_ref, acc_in, total_in, *refs
-):
-    outs, (acc, carry, tri, level_buf, penalty_buf, plane) = refs[:2], refs[2:]
+    out_ref[0] = acc[...]
+    out_ref[1] = carry[...]
+
+
+def plane_kernel(distance, z_size, first, last, at_ref, own_ref, other_ref, *refs):
+    half_ref, across_ref, *refs = refs
+    if not first:
+        state, *refs = refs
+    if last:
+        closest, mine_ref, theirs_ref, *refs = refs
+    else:
+        out_ref, *refs = refs
+    q_buf, acc, carry, tri, level_buf, penalty_buf, plane = refs
     rows = acc.shape[0]
     core = at_ref[2]
     below = jnp.where(core == 0, distance, z_size - distance)
@@ -166,6 +180,7 @@
 
     @pl.when(visible)
     def _():
+        scale_queries(at_ref, own_ref, other_ref, q_buf)
         if last:
             direct = (at_ref[1] // 2) == 1 - core
             for k in range(shards):
@@ -173,15 +188,16 @@
         else:
             join_halves(at_ref, half_ref, across_ref, plane)
 
-    def part(h, _):
-        first_row = pl.multiple_of(h * rows, rows)
+    def part(turn, _):
+        first_row = pl.multiple_of(jnp.where(turn == 0, 1 - core, core) * rows, rows)
         here = pl.ds(first_row, rows)
         clear(acc, carry, tri)
 
         @pl.when(visible)
         def _():
             scores, mix, both = block_steps(
-                q_ref, plane, acc, carry, tri, level_buf, penalty_buf, first_row, tok
+                q_buf, plane, acc, carry, tri, level_buf, penalty_buf, first_row,
+                own_ref.shape[0],
             )
             scores(shards - 1, 0)
 
@@ -194,32 +210,39 @@
             both(1, 0)
             mix(0, 1)
 
-        old, old_total = acc_in[here, :], total_in[here, :]
-        new, new_total = acc[...], carry[...]
-        result = old * jnp.exp2(jnp.where(upward, 0.0, -new_total))
-        result = result + new * jnp.exp2(jnp.where(upward, -old_total, 0.0))
-        total = old_total + new_total
-        if last:
-            for owned, out in ((True, outs[0]), (False, outs[1])):
-
-                @pl.when((h == core) == owned)
-                def _(out=out):
-                    out[0] = result
-                    out[1] = total
-        else:
-            outs[0][here, :] = result
-            outs[1][here, :] = total
+        result, total = acc[...], carry[...]
+        if not first:
+            old, old_total = state[0, here, :], state[1, here, :]
+            result = result * jnp.exp2(jnp.where(upward, -old_total, 0.0))
+            result = result + old * jnp.exp2(jnp.where(upward, 0.0, -total))
+            total = total + old_total
+        if not last:
+            out_ref[0, here, :] = result
+            out_ref[1, here, :] = total
+            return 0
+
+        @pl.when(turn == 0)
+        def _():
+            theirs_ref[0] = result
+            theirs_ref[1] = total
+
+        @pl.when(turn == 1)
+        def _():
+            left = jnp.exp2(-closest[1])
+            mine_ref[0] = closest[0] + jnp.where(upward, left * result, 0.0)
+            mine_ref[1] = jnp.where(upward, left * jnp.exp2(-total), left)
+            mine_ref[2] = jnp.where(upward, 0.0, left * result)
+
         return 0
 
     lax.fori_loop(0, 2, part, 0)
 
 
-def merge_kernel(at_ref, own_ref, own_total, mine, theirs, out_ref):
+def merge_kernel(at_ref, mine, theirs, out_ref):
     upward = at_ref[2] == 0
     tok = out_ref.shape[0]
-    newer_total = jnp.where(upward, mine[1], theirs[1])
-    newer, older = jnp.where(upward, mine[0], theirs[0]), jnp.where(upward, theirs[0], mine[0])
-    mixed = own_ref[...] + jnp.exp2(-own_total[...]) * (newer + jnp.exp2(-newer_total) * older)
+    older = jnp.where(upward, 0.0, jnp.exp2(-theirs[1])) * mine[2]
+    mixed = mine[0] + mine[1] * theirs[0] + older
     for g in range(out_ref.shape[1] // HD):
         out_ref[:, g * HD : (g + 1) * HD] = mixed[g * tok : (g + 1) * tok].astype(out_ref.dtype)
 
@@ -241,45 +264,50 @@
         return lax.ppermute(value, "sp_1", [(i, y_size - 1 - i) for i in range(y_size)])
 
     scratch = [
+        pltpu.VMEM((2 * rows, 2 * HD), jnp.bfloat16),
+        pltpu.VMEM((rows, HD), jnp.float32),
+        pltpu.VMEM((rows, HD), jnp.float32),
         pltpu.VMEM((BK, BK), jnp.bfloat16),
         pltpu.VMEM((2, rows, BK), jnp.float32),
         pltpu.VMEM((2, rows, BK), jnp.bfloat16),
         pltpu.VMEM((2 * y_size, tok, 2 * HD), jnp.bfloat16),
     ]
-    state = ((rows, HD), jnp.float32)
-    both_state = ((2 * rows, HD), jnp.float32)
     work = 2 * y_size * rows * BK * HD * 16
     across = from_across(half)
     other_query = shifted(query, "sp_2", 1)
-    doubled, own, own_total = call(
+    (closest,) = call(
         own_plane_kernel,
-        [((2 * rows, 2 * HD), jnp.bfloat16), state, state],
+        [((2, rows, HD), jnp.float32)],
         (at, query, other_query, half, across),
         scratch,
         work // 2,
     )
-    acc = total = jnp.zeros(*both_state)
+    state = ()
     for k in range(1, z_size // 2 + 1):
         last = k == z_size // 2
         if k == 3:
-            half, own = lax.optimization_barrier((half, own))
+            half, closest = lax.optimization_barrier((half, closest))
         if k == 4:
             half, before = lax.optimization_barrier((half, before))
         half = counter_shifted(half)
         across = from_across(half)
-        acc, total = call(
-            functools.partial(plane_kernel, k, z_size, tok, last),
-            [((2, rows, HD), jnp.float32)] * 2 if last else [both_state] * 2,
-            (at, doubled, half, across, acc, total),
-            [pltpu.VMEM((rows, HD), jnp.float32)] * 2 + scratch,
+        state = call(
+            functools.partial(plane_kernel, k, z_size, k == 1, last),
+            [((3, rows, HD), jnp.float32), ((2, rows, HD), jnp.float32)]
+            if last
+            else [((2, 2 * rows, HD), jnp.float32)],
+            (at, query, other_query, half, across) + state + ((closest,) if last else ()),
+            scratch,
             work * 2,
         )
+        state = tuple(state)
         if k == 1:
-            before = acc
+            before = state[0]
+    mine, theirs = state
     return call(
         merge_kernel,
         [((tok, query.shape[1]), jnp.bfloat16)],
-        (at, own, own_total, acc, shifted(total, "sp_2", 1)),
+        (at, mine, shifted(theirs, "sp_2", 1)),
     )[0]
 
 
@@ -292,14 +320,17 @@
 
 
 def project_kernel(
-    at_ref, heads_ref, w0, w1, w2, w3, stream_ref, gain_ref, slots_ref, mid_ref, normed_ref, out_ref
+    at_ref, heads_ref, w0, w1, far0, far1, w3, stream_ref, gain_ref, slots_ref, mid_ref, normed_ref, out_ref
 ):
-    weights = (w0, w1, w2, w3)
-    own = at_ref[3]
+    own, count = at_ref[3], heads_ref.shape[0]
     attended = jnp.zeros(stream_ref.shape, jnp.float32)
-    for k, weight in enumerate(weights):
-        source = (own + len(weights) - k) % len(weights)
-        attended += jnp.dot(heads_ref[source], weight[...], preferred_element_type=jnp.float32)
+    for k, weight in ((0, w0), (1, w1), (3, w3)):
+        heads = heads_ref[(own + count - k) % count]
+        attended += jnp.dot(heads, weight[...], preferred_element_type=jnp.float32)
+    heads = heads_ref[(own + count - 2) % count]
+    half = far0.shape[0]
+    attended += jnp.dot(heads[:, :half], far0[...], preferred_element_type=jnp.float32)
+    attended += jnp.dot(heads[:, half:], far1[...], preferred_element_type=jnp.float32)
     mid = (stream_ref[...].astype(jnp.float32) + attended).astype(jnp.bfloat16)
     mid_ref[...] = mid
     wide = mid.astype(jnp.float32)
@@ -368,8 +399,10 @@
     at = jnp.stack([lax.axis_index(axis) for axis in SP_TP])
     weight_below = shifted(out_weight, "tp", 1)
     weight_above = shifted(out_weight, "tp", -1)
-    weight_far = shifted(weight_below, "tp", 1)
-    out_weights = (out_weight, weight_below, weight_far, weight_above)
+    half = out_weight.shape[0] // 2
+    far0 = shifted(weight_below[:half], "tp", 1)
+    far1 = shifted(weight_above[half:], "tp", -1)
+    out_weights = (out_weight, weight_below, far0, far1, weight_above)
     own_rows = stream.shape[0]
     expert_count = lax.axis_size(SP) * expert_gate.shape[0]
     capacity = 2 * own_rows * TOP_K // expert_count

time: 237 us -> 236 us (level)
  local copies, waits for them, and re-layouts: 17.9 us -> 14.6 us
  starting transfers between devices: 32.7 us -> 35.3 us
    unnamed x57 -> x49, local copies, waits for them, and re-layouts: 15.9 us -> 11.5 us
    ppermute x6 -> x7, starting transfers between devices: 9.64 us -> 12.9 us  [shifted(): lax.ppermute(value, axis, [(i, (i + step) % size) for i in range(size)])]
    ppermute x6 -> x7, waiting for transfers between devices: 12 us -> 13 us  [shifted(): lax.ppermute(value, axis, [(i, (i + step) % size) for i in range(size)])]
  transfers between devices with their start and end apart: 18 -> 19, of which waited for: 13 -> 13; matrix products, arithmetic and copies ran while one was open for 1% -> 1% of each run, Pallas kernels for 5% -> 5%
where the time goes in v2:
time: 236 us; the launch traced here: 235 us
  waiting for transfers between devices  96.8 us (41%)
  blocking collectives  65.4 us (28%)
  starting transfers between devices  35.3 us (15%)
  Pallas kernels  21.6 us (9%)
  local copies, waits for them, and re-layouts  14.6 us (6%)
    all_to_all x1, blocking collectives, per_device(): arrived = lax.all_to_all(outgoing.reshape(exchange), SP, 0, 0, tiled=True)  65.4 us
    all_to_all x1, waiting for transfers between devices, per_device(): returned = lax.all_to_all(produced.reshape(exchange), SP, 0, 0, tiled=True)  45.4 us
    pallas_call x11, Pallas kernels, call(): pl.pallas_call(kernel, out_shape=[jax.ShapeDtypeStruct(*out) for out in o...  21.6 us
    ppermute x4, waiting for transfers between devices, counter_shifted(): return lax.ppermute(value, ('sp_0', 'sp_2'), pairs)  17.7 us
    ppermute x7, waiting for transfers between devices, shifted(): lax.ppermute(value, axis, [(i, (i + step) % size) for i in range(size)])  13 us
    ppermute x7, starting transfers between devices, shifted(): lax.ppermute(value, axis, [(i, (i + step) % size) for i in range(size)])  12.9 us
    ppermute x5, waiting for transfers between devices, from_across(): lax.ppermute(value, 'sp_1', [(i, y_size - 1 - i) for i in range(y_size)])  12.1 us
    unnamed x49, local copies, waits for them, and re-layouts  11.5 us
  transfers between devices with their start and end apart: 19, of which 13 were waited for; matrix products, arithmetic and copies ran while one was open for 1% of the time, Pallas kernels for 5%

profile of v2, /device:TPU:8, one launch (start us, length us, event | category | flops | bytes accessed | tf_op | source)
XLA Modules:
  0.0 234.8 jit_solution(4394548572925736823)
XLA Ops:
  1.8 2.2 collective-permute-start.1
  4.1 3.1 %collective-permute-done.1 = bf16[256,256]{1,0:T(8,128)(2,1)S(1)} collective-permute-done((bf16[256,256]{1,0:T(8,128)(2,1)S(1)}, bf16[256,256]{1,0:T(8,128)(2,1)S(1)}, u32[]{:S(2)}, u32[]{:S(2)}) %collective-permute-start.1) | collective-permute-done | bytes 131104 | tf_op jit(solution)/shard_map/ppermute | solution.py:255
  9.4 2.0 collective-permute-start.3
  11.4 1.6 collective-permute-start.5
  13.0 9.5 %collective-permute-done.3.refs_0_ = bf16[4,256,256]{2,1,0:T(8,128)(2,1)S(1)} collective-permute-done((bf16[4,256,256]{2,1,0:T(8,128)(2,1)S(1)}, bf16[4,256,256]{2,1,0:T(8,128)(2,1)S(1)}, u32[]{:S(2)}, u32[]{:S(2)}) %collective-permute-start.3) | collective-permute-done | bytes 524320 | tf_op jit(solution)/shard_map/ppermute | solution.py:33
  22.5 1.6 collective-permute-start.7
  24.1 1.7 collective-permute-start
  27.2 2.2 shard_map.137.refs_3_
  30.2 2.8 %collective-permute-done.4.refs_0_ = bf16[4,256,256]{2,1,0:T(8,128)(2,1)} collective-permute-done((bf16[4,256,256]{2,1,0:T(8,128)(2,1)S(1)}, bf16[4,256,256]{2,1,0:T(8,128)(2,1)}, u32[]{:S(2)}, u32[]{:S(2)}) %collective-permute-start.4) | collective-permute-done | bytes 524320 | tf_op jit(solution)/shard_map/ppermute | solution.py:33
  33.0 2.8 %collective-permute-start.15 = (bf16[256,2048]{1,0:T(8,128)(2,1)S(1)}, bf16[256,2048]{1,0:T(8,128)(2,1)S(1)}, u32[]{:S(2)}, u32[]{:S(2)}) collective-permute-start(bf16[256,2048]{1,0:T(8,128)(2,1)S(1)} %copy-done.4), channel_id=1, source_target_pairs={{0,3},{1,0},{2,1},{3,2},{4,7},{5,4},{6,5},{7,6},{8,11},{9,8},{10,9... | collective-permute-start | bytes 3145736 | tf_op jit(solution)/shard_map/ppermute | solution.py:26
  38.3 5.4 %collective-permute-done.6.refs_0_ = bf16[4,256,256]{2,1,0:T(8,128)(2,1)} collective-permute-done((bf16[4,256,256]{2,1,0:T(8,128)(2,1)}, bf16[4,256,256]{2,1,0:T(8,128)(2,1)}, u32[]{:S(2)}, u32[]{:S(2)}) %collective-permute-start.6) | collective-permute-done | bytes 524320 | tf_op jit(solution)/shard_map/ppermute | solution.py:33
  45.2 1.6 collective-permute-start.11
  47.4 4.7 %collective-permute-done.13.w1 = bf16[256,2048]{1,0:T(8,128)(2,1)S(1)} collective-permute-done((bf16[256,2048]{1,0:T(8,128)(2,1)S(1)}, bf16[256,2048]{1,0:T(8,128)(2,1)S(1)}, u32[]{:S(2)}, u32[]{:S(2)}) %collective-permute-start.13) | collective-permute-done | bytes 1048608 | tf_op jit(solution)/shard_map/ppermute | solution.py:26
  53.2 5.9 %collective-permute-done.15.w3 = bf16[256,2048]{1,0:T(8,128)(2,1)S(1)} collective-permute-done((bf16[256,2048]{1,0:T(8,128)(2,1)S(1)}, bf16[256,2048]{1,0:T(8,128)(2,1)S(1)}, u32[]{:S(2)}, u32[]{:S(2)}) %collective-permute-start.15) | collective-permute-done | bytes 1048608 | tf_op jit(solution)/shard_map/ppermute | solution.py:26
  59.9 3.7 %collective-permute-start.16 = (bf16[128,2048]{1,0:T(8,128)(2,1)}, bf16[128,2048]{1,0:T(8,128)(2,1)}, u32[]{:S(2)}, u32[]{:S(2)}) collective-permute-start(bf16[128,2048]{1,0:T(8,128)(2,1)} %slice.17), channel_id=1, source_target_pairs={{0,3},{1,0},{2,1},{3,2},{4,7},{5,4},{6,5},{7,6},{8,11},{9,8},{10,9... | collective-permute-start | bytes 1572872 | tf_op jit(solution)/shard_map/ppermute | solution.py:26
  63.6 1.6 collective-permute-start.9
  65.3 1.5 shard_map.139.refs_2_
  66.8 1.6 collective-permute-done.10.refs_1_
  68.4 1.5 shard_map.140.refs_2_
  69.9 9.6 %collective-permute-done.9.refs_1_ = bf16[4,256,256]{2,1,0:T(8,128)(2,1)S(1)} collective-permute-done((bf16[4,256,256]{2,1,0:T(8,128)(2,1)}, bf16[4,256,256]{2,1,0:T(8,128)(2,1)S(1)}, u32[]{:S(2)}, u32[]{:S(2)}) %collective-permute-start.9) | collective-permute-done | bytes 524320 | tf_op jit(solution)/shard_map/ppermute | solution.py:264
  79.5 2.3 shard_map.141
  82.8 3.0 %collective-permute-start.12 = (f32[2,512,128]{2,1,0:T(8,128)}, f32[2,512,128]{2,1,0:T(8,128)}, u32[]{:S(2)}, u32[]{:S(2)}) collective-permute-start(f32[2,512,128]{2,1,0:T(8,128)} %get-tuple-element.17), channel_id=1, source_target_pairs={{0,4},{4,0},{1,5},{5,1},{2,6},{6,2},{3,7},{7,3},{8,12},{12,8},{9,1... | collective-permute-start | bytes 1572872 | tf_op jit(solution)/shard_map/ppermute | solution.py:26
  88.7 1.8 shard_map.142
  90.5 4.3 %all-to-all-start = ((bf16[4,64,256]{2,1,0:T(8,128)(2,1)}), bf16[4,64,256]{2,1,0:T(8,128)(2,1)S(1)}, u32[]{:S(2)}, u32[]{:S(2)}) async-start(bf16[4,64,256]{2,1,0:T(8,128)(2,1)} %bitcast.6), calls=%async_computation | async-start | bytes 262144 | tf_op jit(solution)/shard_map/all_to_all | solution.py:418
  95.2 5.6 %all-to-all-done.heads_ref = bf16[4,64,256]{2,1,0:T(8,128)(2,1)S(1)} async-done(((bf16[4,64,256]{2,1,0:T(8,128)(2,1)}), bf16[4,64,256]{2,1,0:T(8,128)(2,1)S(1)}, u32[]{:S(2)}, u32[]{:S(2)}) %all-to-all-start) | async-done | bytes 131104 | tf_op jit(solution)/shard_map/all_to_all | solution.py:418
  101.8 3.0 %shard_map.143 = (bf16[64,2048]{1,0:T(8,128)(2,1)S(1)}, bf16[64,2048]{1,0:T(8,128)(2,1)S(1)}, bf16[512,2048]{1,0:T(8,128)(2,1)S(1)}) custom-call(s32[4]{0:T(128)S(1)} %pad_add_fusion.at_ref, bf16[4,64,256]{2,1,0:T(8,128)(2,1)S(1)} %all-to-all-done.heads_ref, bf16[256,2048]{1,0:T(8,128)(2,1)S(1)} %copy-done.4, ...), custom_call_target="tpu_custom_call" | custom-call | flops 536870912 | bytes 1048576 | tf_op jit(solution)/shard_map/pallas_call | solution.py:38
  104.8 65.4 %all_to_all.15 = bf16[64,8,2048]{2,1,0:T(8,128)(2,1)S(1)} all-to-all(bf16[64,8,2048]{2,1,0:T(8,128)(2,1)S(1)} %bitcast.36), channel_id=1, replica_groups=mesh['sp_0'=8,'sp_1'=4,'sp_2'=2,'tp'=4] {'sp_0','sp_1','sp_2'}, dimensions={0} | all-to-all | bytes 4194304 | tf_op jit(solution)/shard_map/all_to_all | solution.py:429
  170.2 4.3 %shard_map.145 = bf16[512,2048]{1,0:T(8,128)(2,1)S(1)} custom-call(s32[4]{0:T(128)S(1)} %pad_add_fusion.at_ref, bf16[512,2048]{1,0:T(8,128)(2,1)S(1)} %bitcast.37, bf16[2048,384]{1,0:T(8,128)(2,1)S(1)} %bitcast.39, bf16[2048,384]{1,0:T(8,128)(2,1)S(1)} %bitcast.40, bf16[384,2048]{1,0:T(8,128)(2,1)S(1)} %bitcast.41), custom_call_target="tpu_custom_call" | custom-call | flops 4294967296 | bytes 1048576 | tf_op jit(solution)/shard_map/pallas_call | solution.py:38
  175.8 5.6 %all-to-all-start.2 = ((bf16[64,8,2048]{2,1,0:T(8,128)(2,1)}), bf16[64,8,2048]{2,1,0:T(8,128)(2,1)S(1)}, u32[]{:S(2)}, u32[]{:S(2)}) async-start(bf16[64,8,2048]{2,1,0:T(8,128)(2,1)} %bitcast.35), calls=%async_computation.2 | async-start | bytes 4194304 | tf_op jit(solution)/shard_map/all_to_all | solution.py:436
  185.7 1.5 shard_map.144.base_ref
  187.3 45.4 %all-to-all-done.2 = bf16[64,8,2048]{2,1,0:T(8,128)(2,1)S(1)} async-done(((bf16[64,8,2048]{2,1,0:T(8,128)(2,1)}), bf16[64,8,2048]{2,1,0:T(8,128)(2,1)S(1)}, u32[]{:S(2)}, u32[]{:S(2)}) %all-to-all-start.2) | async-done | bytes 2097184 | tf_op jit(solution)/shard_map/all_to_all | solution.py:436
  232.6 2.2 shard_map.146
  (84 shorter events, 23.8 us)
Async XLA Ops:
  0.0 24.1 %copy-start.16 = (bf16[256,256]{1,0:T(8,128)(2,1)S(1)}, bf16[256,256]{1,0:T(8,128)(2,1)}, u32[]{:S(2)}) copy-start(bf16[256,256]{1,0:T(8,128)(2,1)} %own_ref.9) | copy-start | bytes 393220
  0.0 25.7 %copy-start.4 = (bf16[256,2048]{1,0:T(8,128)(2,1)S(1)}, bf16[256,2048]{1,0:T(8,128)(2,1)}, u32[]{:S(2)}) copy-start(bf16[256,2048]{1,0:T(8,128)(2,1)} %w0.1) | copy-start | bytes 3145732
  1.8 5.3 %collective-permute-start.1 = (bf16[256,256]{1,0:T(8,128)(2,1)S(1)}, bf16[256,256]{1,0:T(8,128)(2,1)S(1)}, u32[]{:S(2)}, u32[]{:S(2)}) collective-permute-start(bf16[256,256]{1,0:T(8,128)(2,1)S(1)} %constant_dynamic-update-slice_fusion), channel_id=1, source_target_pairs={{0,8},{8,0},{16,24},{24,16},{1,9},{9,1},{17,25},{25,17},{2,10},{10... | collective-permute-start | bytes 393224 | tf_op jit(solution)/shard_map/ppermute | solution.py:255
  7.2 1.6 collective-permute-start.2
  9.4 13.1 %collective-permute-start.3 = (bf16[4,256,256]{2,1,0:T(8,128)(2,1)S(1)}, bf16[4,256,256]{2,1,0:T(8,128)(2,1)S(1)}, u32[]{:S(2)}, u32[]{:S(2)}) collective-permute-start(bf16[4,256,256]{2,1,0:T(8,128)(2,1)S(1)} %shard_map.136.half_ref), channel_id=1, source_target_pairs={{0,32},{32,64},{64,96},{96,128},{128,160},{160,192},{192,224},{224... | collective-permute-start | bytes 1572872 | tf_op jit(solution)/shard_map/ppermute | solution.py:33
  11.4 15.8 %collective-permute-start.5 = (bf16[4,256,256]{2,1,0:T(8,128)(2,1)S(1)}, bf16[4,256,256]{2,1,0:T(8,128)(2,1)S(1)}, u32[]{:S(2)}, u32[]{:S(2)}) collective-permute-start(bf16[4,256,256]{2,1,0:T(8,128)(2,1)S(1)} %shard_map.136.half_ref), channel_id=1, source_target_pairs={{0,24},{8,16},{16,8},{24,0},{1,25},{9,17},{17,9},{25,1},{2,26},{10... | collective-permute-start | bytes 1572872 | tf_op jit(solution)/shard_map/ppermute | solution.py:264
  22.5 10.5 %collective-permute-start.4 = (bf16[4,256,256]{2,1,0:T(8,128)(2,1)S(1)}, bf16[4,256,256]{2,1,0:T(8,128)(2,1)}, u32[]{:S(2)}, u32[]{:S(2)}) collective-permute-start(bf16[4,256,256]{2,1,0:T(8,128)(2,1)S(1)} %collective-permute-done.3.refs_0_), channel_id=1, source_target_pairs={{0,32},{32,64},{64,96},{96,128},{128,160},{160,192},{192,224},{224... | collective-permute-start | bytes 1572872 | tf_op jit(solution)/shard_map/ppermute | solution.py:33
  22.5 14.1 %collective-permute-start.7 = (bf16[4,256,256]{2,1,0:T(8,128)(2,1)S(1)}, bf16[4,256,256]{2,1,0:T(8,128)(2,1)S(1)}, u32[]{:S(2)}, u32[]{:S(2)}) collective-permute-start(bf16[4,256,256]{2,1,0:T(8,128)(2,1)S(1)} %collective-permute-done.3.refs_0_), channel_id=1, source_target_pairs={{0,24},{8,16},{16,8},{24,0},{1,25},{9,17},{17,9},{25,1},{2,26},{10... | collective-permute-start | bytes 1572872 | tf_op jit(solution)/shard_map/ppermute | solution.py:264
  24.1 3.2 %collective-permute-start = (bf16[256,256]{1,0:T(8,128)(2,1)S(1)}, bf16[256,256]{1,0:T(8,128)(2,1)S(1)}, u32[]{:S(2)}, u32[]{:S(2)}) collective-permute-start(bf16[256,256]{1,0:T(8,128)(2,1)S(1)} %copy-done.16), channel_id=1, source_target_pairs={{0,4},{4,0},{1,5},{5,1},{2,6},{6,2},{3,7},{7,3},{8,12},{12,8},{9,1... | collective-permute-start | bytes 393224 | tf_op jit(solution)/shard_map/ppermute | solution.py:26
  25.7 26.4 %collective-permute-start.13 = (bf16[256,2048]{1,0:T(8,128)(2,1)S(1)}, bf16[256,2048]{1,0:T(8,128)(2,1)S(1)}, u32[]{:S(2)}, u32[]{:S(2)}) collective-permute-start(bf16[256,2048]{1,0:T(8,128)(2,1)S(1)} %copy-done.4), channel_id=1, source_target_pairs={{0,1},{1,2},{2,3},{3,0},{4,5},{5,6},{6,7},{7,4},{8,9},{9,10},{10,1... | collective-permute-start | bytes 3145736 | tf_op jit(solution)/shard_map/ppermute | solution.py:26
  30.2 17.0 %copy-start.21 = (s32[64,4]{0,1:T(4,128)S(1)}, s32[64,4]{0,1:T(4,128)}, u32[]{:S(2)}) copy-start(s32[64,4]{0,1:T(4,128)} %param.20) | copy-start | bytes 3076
  33.0 10.7 %collective-permute-start.6 = (bf16[4,256,256]{2,1,0:T(8,128)(2,1)}, bf16[4,256,256]{2,1,0:T(8,128)(2,1)}, u32[]{:S(2)}, u32[]{:S(2)}) collective-permute-start(bf16[4,256,256]{2,1,0:T(8,128)(2,1)} %collective-permute-done.4.refs_0_), channel_id=1, source_target_pairs={{0,32},{32,64},{64,96},{96,128},{128,160},{160,192},{192,224},{224... | collective-permute-start | bytes 1572872 | tf_op jit(solution)/shard_map/ppermute | solution.py:33
  33.0 26.1 %collective-permute-start.15 = (bf16[256,2048]{1,0:T(8,128)(2,1)S(1)}, bf16[256,2048]{1,0:T(8,128)(2,1)S(1)}, u32[]{:S(2)}, u32[]{:S(2)}) collective-permute-start(bf16[256,2048]{1,0:T(8,128)(2,1)S(1)} %copy-done.4), channel_id=1, source_target_pairs={{0,3},{1,0},{2,1},{3,2},{4,7},{5,4},{6,5},{7,6},{8,11},{9,8},{10,9... | collective-permute-start | bytes 3145736 | tf_op jit(solution)/shard_map/ppermute | solution.py:26
  43.7 19.9 %collective-permute-start.8 = (bf16[4,256,256]{2,1,0:T(8,128)(2,1)}, bf16[4,256,256]{2,1,0:T(8,128)(2,1)}, u32[]{:S(2)}, u32[]{:S(2)}) collective-permute-start(bf16[4,256,256]{2,1,0:T(8,128)(2,1)} %collective-permute-done.6.refs_0_), channel_id=1, source_target_pairs={{0,32},{32,64},{64,96},{96,128},{128,160},{160,192},{192,224},{224... | collective-permute-start | bytes 1572872 | tf_op jit(solution)/shard_map/ppermute | solution.py:33
  45.2 20.1 %collective-permute-start.11 = (bf16[4,256,256]{2,1,0:T(8,128)(2,1)}, bf16[4,256,256]{2,1,0:T(8,128)(2,1)}, u32[]{:S(2)}, u32[]{:S(2)}) collective-permute-start(bf16[4,256,256]{2,1,0:T(8,128)(2,1)} %collective-permute-done.4.refs_0_), channel_id=1, source_target_pairs={{0,24},{8,16},{16,8},{24,0},{1,25},{9,17},{17,9},{25,1},{2,26},{10... | collective-permute-start | bytes 1572872 | tf_op jit(solution)/shard_map/ppermute | solution.py:264
  46.7 21.6 %collective-permute-start.10 = (bf16[4,256,256]{2,1,0:T(8,128)(2,1)}, bf16[4,256,256]{2,1,0:T(8,128)(2,1)}, u32[]{:S(2)}, u32[]{:S(2)}) collective-permute-start(bf16[4,256,256]{2,1,0:T(8,128)(2,1)} %collective-permute-done.6.refs_0_), channel_id=1, source_target_pairs={{0,24},{8,16},{16,8},{24,0},{1,25},{9,17},{17,9},{25,1},{2,26},{10... | collective-permute-start | bytes 1572872 | tf_op jit(solution)/shard_map/ppermute | solution.py:264
  47.4 17.9 %copy-start.20 = (f32[2,1024,128]{2,1,0:T(8,128)S(1)}, f32[2,1024,128]{2,1,0:T(8,128)}, u32[]{:S(2)}) copy-start(f32[2,1024,128]{2,1,0:T(8,128)} %copy-done.19) | copy-start | bytes 3145732
  52.9 42.2 %collective-permute-start.14 = (bf16[128,2048]{1,0:T(8,128)(2,1)}, bf16[128,2048]{1,0:T(8,128)(2,1)}, u32[]{:S(2)}, u32[]{:S(2)}) collective-permute-start(bf16[128,2048]{1,0:T(8,128)(2,1)} %slice.16), channel_id=1, source_target_pairs={{0,1},{1,2},{2,3},{3,0},{4,5},{5,6},{6,7},{7,4},{8,9},{9,10},{10,1... | collective-permute-start | bytes 1572872 | tf_op jit(solution)/shard_map/ppermute | solution.py:26
  59.9 35.2 %collective-permute-start.16 = (bf16[128,2048]{1,0:T(8,128)(2,1)}, bf16[128,2048]{1,0:T(8,128)(2,1)}, u32[]{:S(2)}, u32[]{:S(2)}) collective-permute-start(bf16[128,2048]{1,0:T(8,128)(2,1)} %slice.17), channel_id=1, source_target_pairs={{0,3},{1,0},{2,1},{3,2},{4,7},{5,4},{6,5},{7,6},{8,11},{9,8},{10,9... | collective-permute-start | bytes 1572872 | tf_op jit(solution)/shard_map/ppermute | solution.py:26
  63.6 15.9 %collective-permute-start.9 = (bf16[4,256,256]{2,1,0:T(8,128)(2,1)}, bf16[4,256,256]{2,1,0:T(8,128)(2,1)S(1)}, u32[]{:S(2)}, u32[]{:S(2)}) collective-permute-start(bf16[4,256,256]{2,1,0:T(8,128)(2,1)} %collective-permute-done.8.refs_0_), channel_id=1, source_target_pairs={{0,24},{8,16},{16,8},{24,0},{1,25},{9,17},{17,9},{25,1},{2,26},{10... | collective-permute-start | bytes 1572872 | tf_op jit(solution)/shard_map/ppermute | solution.py:264
  66.8 12.7 %copy-start.18 = (f32[2,512,128]{2,1,0:T(8,128)S(1)}, f32[2,512,128]{2,1,0:T(8,128)}, u32[]{:S(2)}) copy-start(f32[2,512,128]{2,1,0:T(8,128)} %copy-done.17) | copy-start | bytes 1572868
  82.8 18.0 %copy-start.12 = (f32[2048]{0:T(1024)S(1)}, f32[2048]{0:T(1024)}, u32[]{:S(2)}) copy-start(f32[2048]{0:T(1024)} %param.19) | copy-start | bytes 24580
  82.8 4.8 %collective-permute-start.12 = (f32[2,512,128]{2,1,0:T(8,128)}, f32[2,512,128]{2,1,0:T(8,128)}, u32[]{:S(2)}, u32[]{:S(2)}) collective-permute-start(f32[2,512,128]{2,1,0:T(8,128)} %get-tuple-element.17), channel_id=1, source_target_pairs={{0,4},{4,0},{1,5},{5,1},{2,6},{6,2},{3,7},{7,3},{8,12},{12,8},{9,1... | collective-permute-start | bytes 1572872 | tf_op jit(solution)/shard_map/ppermute | solution.py:26
  90.5 10.3 %all-to-all-start = ((bf16[4,64,256]{2,1,0:T(8,128)(2,1)}), bf16[4,64,256]{2,1,0:T(8,128)(2,1)S(1)}, u32[]{:S(2)}, u32[]{:S(2)}) async-start(bf16[4,64,256]{2,1,0:T(8,128)(2,1)} %bitcast.6), calls=%async_computation | async-start | bytes 262144 | tf_op jit(solution)/shard_map/all_to_all | solution.py:418
  101.8 68.4 %copy-start.15 = (bf16[1,384,2048]{2,1,0:T(8,128)(2,1)S(1)}, bf16[1,384,2048]{2,1,0:T(8,128)(2,1)}, u32[]{:S(2)}) copy-start(bf16[1,384,2048]{2,1,0:T(8,128)(2,1)} %param.24) | copy-start | bytes 4718596
  104.7 65.4 %copy-start.8 = (bf16[64,2048]{1,0:T(8,128)(2,1)}, bf16[64,2048]{1,0:T(8,128)(2,1)S(1)}, u32[]{:S(2)}) copy-start(bf16[64,2048]{1,0:T(8,128)(2,1)S(1)} %get-tuple-element.19.mid_ref) | copy-start | bytes 786436
  104.7 65.4 %copy-start.10 = (bf16[64,2048]{1,0:T(8,128)(2,1)}, bf16[64,2048]{1,0:T(8,128)(2,1)S(1)}, u32[]{:S(2)}) copy-start(bf16[64,2048]{1,0:T(8,128)(2,1)S(1)} %get-tuple-element.18.normed_ref) | copy-start | bytes 786436
  104.8 65.4 %copy-start.13 = (bf16[1,2048,384]{2,1,0:T(8,128)(2,1)S(1)}, bf16[1,2048,384]{2,1,0:T(8,128)(2,1)}, u32[]{:S(2)}) copy-start(bf16[1,2048,384]{2,1,0:T(8,128)(2,1)} %param.22) | copy-start | bytes 4718596
  104.8 65.4 %copy-start.14 = (bf16[1,2048,384]{2,1,0:T(8,128)(2,1)S(1)}, bf16[1,2048,384]{2,1,0:T(8,128)(2,1)}, u32[]{:S(2)}) copy-start(bf16[1,2048,384]{2,1,0:T(8,128)(2,1)} %param.23) | copy-start | bytes 4718596
  175.8 5.7 %copy-start.9 = (bf16[64,2048]{1,0:T(8,128)(2,1)S(1)}, bf16[64,2048]{1,0:T(8,128)(2,1)}, u32[]{:S(2)}) copy-start(bf16[64,2048]{1,0:T(8,128)(2,1)} %copy-done.8) | copy-start | bytes 786436
  175.8 5.7 %copy-start.11 = (bf16[64,2048]{1,0:T(8,128)(2,1)S(1)}, bf16[64,2048]{1,0:T(8,128)(2,1)}, u32[]{:S(2)}) copy-start(bf16[64,2048]{1,0:T(8,128)(2,1)} %copy-done.10) | copy-start | bytes 786436
  175.8 56.8 %all-to-all-start.2 = ((bf16[64,8,2048]{2,1,0:T(8,128)(2,1)}), bf16[64,8,2048]{2,1,0:T(8,128)(2,1)S(1)}, u32[]{:S(2)}, u32[]{:S(2)}) async-start(bf16[64,8,2048]{2,1,0:T(8,128)(2,1)} %bitcast.35), calls=%async_computation.2 | async-start | bytes 4194304 | tf_op jit(solution)/shard_map/all_to_all | solution.py:436
  (10 other events, 15.9 us)

commit v3 on v2

--- a/solution.py
+++ b/solution.py
@@ -47,27 +47,27 @@
     )(*args)
 
 
-def assemble_kernel(at_ref, own_ref, other_ref, half_ref):
-    row, core = at_ref[1] % 2, at_ref[2]
-    for k in range(2):
-        place = 2 * jnp.where(row == k, 0, 1)
-        half_ref[place + core] = own_ref[k]
-        half_ref[place + 1 - core] = other_ref[k]
-
-
-def join_halves(at_ref, half_ref, across_ref, plane):
-    shards = half_ref.shape[0]
-    upper = at_ref[1] // 2
-    for k in range(shards):
-        plane[upper * shards + k] = half_ref[k]
-        plane[(1 - upper) * shards + k] = across_ref[k]
-
-
-def block_steps(q_ref, plane_ref, acc, carry, tri, level_buf, penalty_buf, first_row, tok):
+def assemble_kernel(at_ref, own_ref, other_ref, part_ref):
+    core = at_ref[2]
+    for k in range(own_ref.shape[0]):
+        part_ref[2 * k + core] = own_ref[k]
+        part_ref[2 * k + 1 - core] = other_ref[k]
+
+
+def join_plane(at_ref, part_ref, before_ref, after_ref, plane):
+    count = plane.shape[0] // 2
+    sources = ((0, part_ref, 0), (1, part_ref, 2), (2, after_ref, 0), (3, before_ref, 0))
+    for ahead, ref, first in sources:
+        place = 2 * ((at_ref[1] + ahead) % count)
+        for core in range(2):
+            plane[place + core] = ref[first + core]
+
+
+def block_steps(q_ref, plane_ref, acc, carry, tri, level_buf, penalty_buf, first_row, tok, base=0):
     rows = acc.shape[0]
 
     def scores(j, slot, diagonal=False):
-        keys = plane_ref[j, :, 0:HD]
+        keys = plane_ref[base + j, :, 0:HD]
         y = lax.dot_general(
             q_ref[pl.ds(first_row, rows), :],
             jnp.concatenate([keys, keys], axis=1),
@@ -94,7 +94,7 @@
         )
         acc[...] += jnp.dot(
             weights.astype(jnp.bfloat16),
-            plane_ref[j, :, HD : 2 * HD],
+            plane_ref[base + j, :, HD : 2 * HD],
             preferred_element_type=jnp.float32,
         )
 
@@ -127,14 +127,14 @@
 
 
 def own_plane_kernel(
-    at_ref, own_ref, other_ref, half_ref, across_ref, out_ref,
+    at_ref, own_ref, other_ref, part_ref, before_ref, after_ref, out_ref,
     q_buf, acc, carry, tri, level_buf, penalty_buf, plane,
 ):
     rows = acc.shape[0]
     core = at_ref[2]
     scale_queries(at_ref, own_ref, other_ref, q_buf)
     clear(acc, carry, tri)
-    join_halves(at_ref, half_ref, across_ref, plane)
+    join_plane(at_ref, part_ref, before_ref, after_ref, plane)
     first_row = pl.multiple_of(core * rows, rows)
     scores, mix, both = block_steps(
         q_buf, plane, acc, carry, tri, level_buf, penalty_buf, first_row, own_ref.shape[0]
@@ -163,7 +163,7 @@
 
 
 def plane_kernel(distance, z_size, first, last, at_ref, own_ref, other_ref, *refs):
-    half_ref, across_ref, *refs = refs
+    part_ref, before_ref, after_ref, *refs = refs
     if not first:
         state, *refs = refs
     if last:
@@ -175,18 +175,14 @@
     core = at_ref[2]
     below = jnp.where(core == 0, distance, z_size - distance)
     visible = below <= at_ref[0]
-    shards = half_ref.shape[0] if last else 2 * half_ref.shape[0]
+    shards = plane.shape[0] // 2 if last else plane.shape[0]
     upward = core == 0
+    base = shards * (1 - core) if last else 0
 
     @pl.when(visible)
     def _():
         scale_queries(at_ref, own_ref, other_ref, q_buf)
-        if last:
-            direct = (at_ref[1] // 2) == 1 - core
-            for k in range(shards):
-                plane[k] = jnp.where(direct, half_ref[k], across_ref[k])
-        else:
-            join_halves(at_ref, half_ref, across_ref, plane)
+        join_plane(at_ref, part_ref, before_ref, after_ref, plane)
 
     def part(turn, _):
         first_row = pl.multiple_of(jnp.where(turn == 0, 1 - core, core) * rows, rows)
@@ -197,7 +193,7 @@
         def _():
             scores, mix, both = block_steps(
                 q_buf, plane, acc, carry, tri, level_buf, penalty_buf, first_row,
-                own_ref.shape[0],
+                own_ref.shape[0], base,
             )
             scores(shards - 1, 0)
 
@@ -252,16 +248,17 @@
     tok = query.shape[0]
     rows = tok * (query.shape[1] // HD)
     pair = jnp.concatenate([keys, values], axis=1)
-    near = lax.ppermute(pair, "sp_1", [(i, i ^ 1) for i in range(y_size)])
-    own_rows = jnp.stack([pair, near])
-    (half,) = call(
+    own_rows = jnp.stack([pair, shifted(pair, "sp_1", -1)])
+    (part,) = call(
         assemble_kernel,
         [((y_size, tok, 2 * HD), jnp.bfloat16)],
         (at, own_rows, shifted(own_rows, "sp_2", 1)),
     )
 
-    def from_across(value):
-        return lax.ppermute(value, "sp_1", [(i, y_size - 1 - i) for i in range(y_size)])
+    def from_neighbours(value):
+        before = shifted(value[:2], "sp_1", 1)
+        after = shifted(value[2:], "sp_1", -1)
+        return value, before, after
 
     scratch = [
         pltpu.VMEM((2 * rows, 2 * HD), jnp.bfloat16),
@@ -273,12 +270,12 @@
         pltpu.VMEM((2 * y_size, tok, 2 * HD), jnp.bfloat16),
     ]
     work = 2 * y_size * rows * BK * HD * 16
-    across = from_across(half)
+    held = from_neighbours(part)
     other_query = shifted(query, "sp_2", 1)
     (closest,) = call(
         own_plane_kernel,
         [((2, rows, HD), jnp.float32)],
-        (at, query, other_query, half, across),
+        (at, query, other_query, *held),
         scratch,
         work // 2,
     )
@@ -286,23 +283,23 @@
     for k in range(1, z_size // 2 + 1):
         last = k == z_size // 2
         if k == 3:
-            half, closest = lax.optimization_barrier((half, closest))
+            part, closest = lax.optimization_barrier((part, closest))
         if k == 4:
-            half, before = lax.optimization_barrier((half, before))
-        half = counter_shifted(half)
-        across = from_across(half)
+            part, early = lax.optimization_barrier((part, early))
+        part = counter_shifted(part)
+        held = from_neighbours(part)
         state = call(
             functools.partial(plane_kernel, k, z_size, k == 1, last),
             [((3, rows, HD), jnp.float32), ((2, rows, HD), jnp.float32)]
             if last
             else [((2, 2 * rows, HD), jnp.float32)],
-            (at, query, other_query, half, across) + state + ((closest,) if last else ()),
+            (at, query, other_query, *held) + state + ((closest,) if last else ()),
             scratch,
             work * 2,
         )
         state = tuple(state)
         if k == 1:
-            before = state[0]
+            early = state[0]
     mine, theirs = state
     return call(
         merge_kernel,

time: 236 us -> 230 us (0.975)
  waiting for transfers between devices: 96.8 us -> 82.4 us
  starting transfers between devices: 35.3 us -> 39.2 us
  blocking collectives: 65.4 us -> 67.8 us
    ppermute x6 -> x0, waiting for transfers between devices: 15.1 us -> none  [the longest x5 12.1 us: from_across(): lax.ppermute(value, 'sp_1', [(i, y_size - 1 - i) for i in range(y_size)])]
    ppermute x7 -> x18, starting transfers between devices: 12.9 us -> 26 us  [shifted(): lax.ppermute(value, axis, [(i, (i + step) % size) for i in range(size)])]
    ppermute x6 -> x0, starting transfers between devices: 9.04 us -> none  [the longest x5 6.8 us: from_across(): lax.ppermute(value, 'sp_1', [(i, y_size - 1 - i) for i in range(y_size)])]
    slice x1 -> x6, local copies, waits for them, and re-layouts: 0.18 us -> 3.21 us  [the longest x5 3.03 us: from_neighbours(): after = shifted(value[2:], 'sp_1', -1)]
    unnamed x49 -> x43, local copies, waits for them, and re-layouts: 11.5 us -> 8.56 us
    all_to_all x1, blocking collectives: 65.4 us -> 67.8 us  [per_device(): arrived = lax.all_to_all(outgoing.reshape(exchange), SP, 0, 0, tiled=True)]
    ppermute x7 -> x18, waiting for transfers between devices: 13 us -> 14.8 us  [shifted(): lax.ppermute(value, axis, [(i, (i + step) % size) for i in range(size)])]
  transfers between devices with their start and end apart: 19 -> 24, of which waited for: 13 -> 11; matrix products, arithmetic and copies ran while one was open for 1% -> 4% of each run, Pallas kernels for 5% -> 5%
where the time goes in v3:
time: 230 us; the launch traced here: 229 us
  waiting for transfers between devices  82.4 us (36%)
  blocking collectives  67.8 us (29%)
  starting transfers between devices  39.2 us (17%)
  Pallas kernels  21.3 us (9%)
  local copies, waits for them, and re-layouts  15.5 us (7%)
    all_to_all x1, blocking collectives, per_device(): arrived = lax.all_to_all(outgoing.reshape(exchange), SP, 0, 0, tiled=True)  67.8 us
    all_to_all x1, waiting for transfers between devices, per_device(): returned = lax.all_to_all(produced.reshape(exchange), SP, 0, 0, tiled=True)  45.4 us
    ppermute x18, starting transfers between devices, shifted(): lax.ppermute(value, axis, [(i, (i + step) % size) for i in range(size)])  26 us
    pallas_call x11, Pallas kernels, call(): pl.pallas_call(kernel, out_shape=[jax.ShapeDtypeStruct(*out) for out in o...  21.3 us
    ppermute x4, waiting for transfers between devices, counter_shifted(): return lax.ppermute(value, ('sp_0', 'sp_2'), pairs)  16.4 us
    ppermute x18, waiting for transfers between devices, shifted(): lax.ppermute(value, axis, [(i, (i + step) % size) for i in range(size)])  14.8 us
    unnamed x43, local copies, waits for them, and re-layouts  8.56 us
    all_to_all x1, waiting for transfers between devices, per_device(): lax.all_to_all(heads_out.reshape(-1, own_rows, heads_out.shape[1]), 'tp',...  5.84 us
  transfers between devices with their start and end apart: 24, of which 11 were waited for; matrix products, arithmetic and copies ran while one was open for 4% of the time, Pallas kernels for 5%

profile of v3, /device:TPU:8, one launch (start us, length us, event | category | flops | bytes accessed | tf_op | source)
XLA Modules:
  0.0 228.8 jit_solution(6458233147953723307)
XLA Ops:
  1.8 2.2 collective-permute-start.1
  4.0 3.1 %collective-permute-done.1 = bf16[256,256]{1,0:T(8,128)(2,1)S(1)} collective-permute-done((bf16[256,256]{1,0:T(8,128)(2,1)S(1)}, bf16[256,256]{1,0:T(8,128)(2,1)S(1)}, u32[]{:S(2)}, u32[]{:S(2)}) %collective-permute-start.1) | collective-permute-done | bytes 131104 | tf_op jit(solution)/shard_map/ppermute | solution.py:26
  9.3 2.0 collective-permute-start.3
  11.3 1.5 collective-permute-start.18
  12.8 1.7 collective-permute-start.20
  14.5 3.2 %collective-permute-start = (bf16[256,256]{1,0:T(8,128)(2,1)S(1)}, bf16[256,256]{1,0:T(8,128)(2,1)S(1)}, u32[]{:S(2)}, u32[]{:S(2)}) collective-permute-start(bf16[256,256]{1,0:T(8,128)(2,1)S(1)} %copy-done.13), channel_id=1, source_target_pairs={{0,4},{4,0},{1,5},{5,1},{2,6},{6,2},{3,7},{7,3},{8,12},{12,8},{9,1... | collective-permute-start | bytes 393224 | tf_op jit(solution)/shard_map/ppermute | solution.py:26
  17.8 4.7 %collective-permute-done.3.refs_0_ = bf16[4,256,256]{2,1,0:T(8,128)(2,1)} collective-permute-done((bf16[4,256,256]{2,1,0:T(8,128)(2,1)S(1)}, bf16[4,256,256]{2,1,0:T(8,128)(2,1)}, u32[]{:S(2)}, u32[]{:S(2)}) %collective-permute-start.3) | collective-permute-done | bytes 524320 | tf_op jit(solution)/shard_map/ppermute | solution.py:33
  23.3 1.6 collective-permute-start.5
  26.6 4.9 %collective-permute-done.5.before_ref = bf16[2,256,256]{2,1,0:T(8,128)(2,1)S(1)} collective-permute-done((bf16[2,256,256]{2,1,0:T(8,128)(2,1)}, bf16[2,256,256]{2,1,0:T(8,128)(2,1)S(1)}, u32[]{:S(2)}, u32[]{:S(2)}) %collective-permute-start.5) | collective-permute-done | bytes 262176 | tf_op jit(solution)/shard_map/ppermute | solution.py:26
  31.6 1.7 collective-permute-start.8
  34.9 2.2 shard_map.137.refs_4_
  38.0 1.7 collective-permute-start.19
  40.5 1.6 collective-permute-start.21
  44.4 1.9 collective-permute-start.15
  48.2 6.7 %collective-permute-done.7.refs_0_ = bf16[4,256,256]{2,1,0:T(8,128)(2,1)S(1)} collective-permute-done((bf16[4,256,256]{2,1,0:T(8,128)(2,1)}, bf16[4,256,256]{2,1,0:T(8,128)(2,1)S(1)}, u32[]{:S(2)}, u32[]{:S(2)}) %collective-permute-start.7) | collective-permute-done | bytes 524320 | tf_op jit(solution)/shard_map/ppermute | solution.py:33
  56.1 2.6 %collective-permute-start.13 = (bf16[2,256,256]{2,1,0:T(8,128)(2,1)S(1)}, bf16[2,256,256]{2,1,0:T(8,128)(2,1)S(1)}, u32[]{:S(2)}, u32[]{:S(2)}) collective-permute-start(bf16[2,256,256]{2,1,0:T(8,128)(2,1)S(1)} %get-tuple-element.24), channel_id=1, source_target_pairs={{0,8},{8,16},{16,24},{24,0},{1,9},{9,17},{17,25},{25,1},{2,10},{10... | collective-permute-start | bytes 786440 | tf_op jit(solution)/shard_map/ppermute | solution.py:26
  60.9 5.0 %collective-permute-done.10.refs_0_ = bf16[4,256,256]{2,1,0:T(8,128)(2,1)S(1)} collective-permute-done((bf16[4,256,256]{2,1,0:T(8,128)(2,1)S(1)}, bf16[4,256,256]{2,1,0:T(8,128)(2,1)S(1)}, u32[]{:S(2)}, u32[]{:S(2)}) %collective-permute-start.10) | collective-permute-done | bytes 524320 | tf_op jit(solution)/shard_map/ppermute | solution.py:33
  65.9 2.1 collective-permute-start.11
  68.0 1.7 collective-permute-start.12
  70.6 2.5 %collective-permute-done.11.refs_1_ = bf16[2,256,256]{2,1,0:T(8,128)(2,1)S(1)} collective-permute-done((bf16[2,256,256]{2,1,0:T(8,128)(2,1)S(1)}, bf16[2,256,256]{2,1,0:T(8,128)(2,1)S(1)}, u32[]{:S(2)}, u32[]{:S(2)}) %collective-permute-start.11) | collective-permute-done | bytes 262176 | tf_op jit(solution)/shard_map/ppermute | solution.py:26
  73.1 2.5 %collective-permute-done.12.refs_2_ = bf16[2,256,256]{2,1,0:T(8,128)(2,1)S(1)} collective-permute-done((bf16[2,256,256]{2,1,0:T(8,128)(2,1)S(1)}, bf16[2,256,256]{2,1,0:T(8,128)(2,1)S(1)}, u32[]{:S(2)}, u32[]{:S(2)}) %collective-permute-start.12) | collective-permute-done | bytes 262176 | tf_op jit(solution)/shard_map/ppermute | solution.py:26
  75.6 2.1 shard_map.141
  80.7 1.8 shard_map.142
  82.6 3.3 %all-to-all-start = ((bf16[4,64,256]{2,1,0:T(8,128)(2,1)}), bf16[4,64,256]{2,1,0:T(8,128)(2,1)S(1)}, u32[]{:S(2)}, u32[]{:S(2)}) async-start(bf16[4,64,256]{2,1,0:T(8,128)(2,1)} %bitcast.6), calls=%async_computation | async-start | bytes 262144 | tf_op jit(solution)/shard_map/all_to_all | solution.py:415
  86.2 5.8 %all-to-all-done.heads_ref = bf16[4,64,256]{2,1,0:T(8,128)(2,1)S(1)} async-done(((bf16[4,64,256]{2,1,0:T(8,128)(2,1)}), bf16[4,64,256]{2,1,0:T(8,128)(2,1)S(1)}, u32[]{:S(2)}, u32[]{:S(2)}) %all-to-all-start) | async-done | bytes 131104 | tf_op jit(solution)/shard_map/all_to_all | solution.py:415
  93.0 3.1 %shard_map.143 = (bf16[64,2048]{1,0:T(8,128)(2,1)S(1)}, bf16[64,2048]{1,0:T(8,128)(2,1)S(1)}, bf16[512,2048]{1,0:T(8,128)(2,1)S(1)}) custom-call(s32[4]{0:T(128)S(1)} %pad_add_fusion.at_ref, bf16[4,64,256]{2,1,0:T(8,128)(2,1)S(1)} %all-to-all-done.heads_ref, bf16[256,2048]{1,0:T(8,128)(2,1)} %w0.1, bf16[256,2048]{1,0:T(8,128)(2,1)S(1)} %collective-permute-done.18.w1, ...), custom_call_target="tpu_custom_call" | custom-call | flops 536870912 | bytes 1048576 | tf_op jit(solution)/shard_map/pallas_call | solution.py:38
  96.2 67.8 %all_to_all.15 = bf16[64,8,2048]{2,1,0:T(8,128)(2,1)S(1)} all-to-all(bf16[64,8,2048]{2,1,0:T(8,128)(2,1)S(1)} %bitcast.36), channel_id=1, replica_groups=mesh['sp_0'=8,'sp_1'=4,'sp_2'=2,'tp'=4] {'sp_0','sp_1','sp_2'}, dimensions={0} | all-to-all | bytes 4194304 | tf_op jit(solution)/shard_map/all_to_all | solution.py:426
  164.1 4.3 %shard_map.145 = bf16[512,2048]{1,0:T(8,128)(2,1)S(1)} custom-call(s32[4]{0:T(128)S(1)} %pad_add_fusion.at_ref, bf16[512,2048]{1,0:T(8,128)(2,1)S(1)} %bitcast.37, bf16[2048,384]{1,0:T(8,128)(2,1)S(1)} %bitcast.39, bf16[2048,384]{1,0:T(8,128)(2,1)S(1)} %bitcast.40, bf16[384,2048]{1,0:T(8,128)(2,1)S(1)} %bitcast.41), custom_call_target="tpu_custom_call" | custom-call | flops 4294967296 | bytes 1048576 | tf_op jit(solution)/shard_map/pallas_call | solution.py:38
  169.7 5.6 %all-to-all-start.2 = ((bf16[64,8,2048]{2,1,0:T(8,128)(2,1)}), bf16[64,8,2048]{2,1,0:T(8,128)(2,1)S(1)}, u32[]{:S(2)}, u32[]{:S(2)}) async-start(bf16[64,8,2048]{2,1,0:T(8,128)(2,1)} %bitcast.35), calls=%async_computation.2 | async-start | bytes 4194304 | tf_op jit(solution)/shard_map/all_to_all | solution.py:433
  179.7 1.5 shard_map.144.base_ref
  181.2 45.4 %all-to-all-done.2 = bf16[64,8,2048]{2,1,0:T(8,128)(2,1)S(1)} async-done(((bf16[64,8,2048]{2,1,0:T(8,128)(2,1)}), bf16[64,8,2048]{2,1,0:T(8,128)(2,1)S(1)}, u32[]{:S(2)}, u32[]{:S(2)}) %all-to-all-start.2) | async-done | bytes 2097184 | tf_op jit(solution)/shard_map/all_to_all | solution.py:433
  226.6 2.2 shard_map.146
  (93 shorter events, 28.4 us)
Async XLA Ops:
  0.0 14.5 %copy-start.13 = (bf16[256,256]{1,0:T(8,128)(2,1)S(1)}, bf16[256,256]{1,0:T(8,128)(2,1)}, u32[]{:S(2)}) copy-start(bf16[256,256]{1,0:T(8,128)(2,1)} %own_ref.9) | copy-start | bytes 393220
  0.0 25.4 %copy-start.18 = (s32[64,4]{0,1:T(4,128)S(1)}, s32[64,4]{0,1:T(4,128)}, u32[]{:S(2)}) copy-start(s32[64,4]{0,1:T(4,128)} %param.20) | copy-start | bytes 3076
  1.8 5.3 %collective-permute-start.1 = (bf16[256,256]{1,0:T(8,128)(2,1)S(1)}, bf16[256,256]{1,0:T(8,128)(2,1)S(1)}, u32[]{:S(2)}, u32[]{:S(2)}) collective-permute-start(bf16[256,256]{1,0:T(8,128)(2,1)S(1)} %constant_dynamic-update-slice_fusion), channel_id=1, source_target_pairs={{0,24},{8,0},{16,8},{24,16},{1,25},{9,1},{17,9},{25,17},{2,26},{10... | collective-permute-start | bytes 393224 | tf_op jit(solution)/shard_map/ppermute | solution.py:26
  7.1 1.6 collective-permute-start.2
  9.3 13.2 %collective-permute-start.3 = (bf16[4,256,256]{2,1,0:T(8,128)(2,1)S(1)}, bf16[4,256,256]{2,1,0:T(8,128)(2,1)}, u32[]{:S(2)}, u32[]{:S(2)}) collective-permute-start(bf16[4,256,256]{2,1,0:T(8,128)(2,1)S(1)} %shard_map.136.part_ref), channel_id=1, source_target_pairs={{0,32},{32,64},{64,96},{96,128},{128,160},{160,192},{192,224},{224... | collective-permute-start | bytes 1572872 | tf_op jit(solution)/shard_map/ppermute | solution.py:33
  11.3 25.8 %collective-permute-start.18 = (bf16[256,2048]{1,0:T(8,128)(2,1)}, bf16[256,2048]{1,0:T(8,128)(2,1)S(1)}, u32[]{:S(2)}, u32[]{:S(2)}) collective-permute-start(bf16[256,2048]{1,0:T(8,128)(2,1)} %w0.1), channel_id=1, source_target_pairs={{0,1},{1,2},{2,3},{3,0},{4,5},{5,6},{6,7},{7,4},{8,9},{9,10},{10,1... | collective-permute-start | bytes 3145736 | tf_op jit(solution)/shard_map/ppermute | solution.py:26
  12.8 26.9 %collective-permute-start.20 = (bf16[256,2048]{1,0:T(8,128)(2,1)}, bf16[256,2048]{1,0:T(8,128)(2,1)S(1)}, u32[]{:S(2)}, u32[]{:S(2)}) collective-permute-start(bf16[256,2048]{1,0:T(8,128)(2,1)} %w0.1), channel_id=1, source_target_pairs={{0,3},{1,0},{2,1},{3,2},{4,7},{5,4},{6,5},{7,6},{8,11},{9,8},{10,9... | collective-permute-start | bytes 3145736 | tf_op jit(solution)/shard_map/ppermute | solution.py:26
  14.5 10.4 %collective-permute-start = (bf16[256,256]{1,0:T(8,128)(2,1)S(1)}, bf16[256,256]{1,0:T(8,128)(2,1)S(1)}, u32[]{:S(2)}, u32[]{:S(2)}) collective-permute-start(bf16[256,256]{1,0:T(8,128)(2,1)S(1)} %copy-done.13), channel_id=1, source_target_pairs={{0,4},{4,0},{1,5},{5,1},{2,6},{6,2},{3,7},{7,3},{8,12},{12,8},{9,1... | collective-permute-start | bytes 393224 | tf_op jit(solution)/shard_map/ppermute | solution.py:26
  22.5 19.6 %collective-permute-start.4 = (bf16[4,256,256]{2,1,0:T(8,128)(2,1)}, bf16[4,256,256]{2,1,0:T(8,128)(2,1)}, u32[]{:S(2)}, u32[]{:S(2)}) collective-permute-start(bf16[4,256,256]{2,1,0:T(8,128)(2,1)} %collective-permute-done.3.refs_0_), channel_id=1, source_target_pairs={{0,32},{32,64},{64,96},{96,128},{128,160},{160,192},{192,224},{224... | collective-permute-start | bytes 1572872 | tf_op jit(solution)/shard_map/ppermute | solution.py:33
  23.3 8.2 %collective-permute-start.5 = (bf16[2,256,256]{2,1,0:T(8,128)(2,1)}, bf16[2,256,256]{2,1,0:T(8,128)(2,1)S(1)}, u32[]{:S(2)}, u32[]{:S(2)}) collective-permute-start(bf16[2,256,256]{2,1,0:T(8,128)(2,1)} %get-tuple-element.30), channel_id=1, source_target_pairs={{0,8},{8,16},{16,24},{24,0},{1,9},{9,17},{17,25},{25,1},{2,10},{10... | collective-permute-start | bytes 786440 | tf_op jit(solution)/shard_map/ppermute | solution.py:26
  24.9 8.7 %collective-permute-start.6 = (bf16[2,256,256]{2,1,0:T(8,128)(2,1)}, bf16[2,256,256]{2,1,0:T(8,128)(2,1)S(1)}, u32[]{:S(2)}, u32[]{:S(2)}) collective-permute-start(bf16[2,256,256]{2,1,0:T(8,128)(2,1)} %get-tuple-element.29), channel_id=1, source_target_pairs={{0,24},{8,0},{16,8},{24,16},{1,25},{9,1},{17,9},{25,17},{2,26},{10... | collective-permute-start | bytes 786440 | tf_op jit(solution)/shard_map/ppermute | solution.py:26
  31.6 12.8 %collective-permute-start.8 = (bf16[2,256,256]{2,1,0:T(8,128)(2,1)S(1)}, bf16[2,256,256]{2,1,0:T(8,128)(2,1)S(1)}, u32[]{:S(2)}, u32[]{:S(2)}) collective-permute-start(bf16[2,256,256]{2,1,0:T(8,128)(2,1)S(1)} %get-tuple-element.28), channel_id=1, source_target_pairs={{0,8},{8,16},{16,24},{24,0},{1,9},{9,17},{17,25},{25,1},{2,10},{10... | collective-permute-start | bytes 786440 | tf_op jit(solution)/shard_map/ppermute | solution.py:26
  33.6 12.6 %collective-permute-start.9 = (bf16[2,256,256]{2,1,0:T(8,128)(2,1)S(1)}, bf16[2,256,256]{2,1,0:T(8,128)(2,1)S(1)}, u32[]{:S(2)}, u32[]{:S(2)}) collective-permute-start(bf16[2,256,256]{2,1,0:T(8,128)(2,1)S(1)} %get-tuple-element.27), channel_id=1, source_target_pairs={{0,24},{8,0},{16,8},{24,16},{1,25},{9,1},{17,9},{25,17},{2,26},{10... | collective-permute-start | bytes 786440 | tf_op jit(solution)/shard_map/ppermute | solution.py:26
  38.0 48.2 %collective-permute-start.19 = (bf16[128,2048]{1,0:T(8,128)(2,1)}, bf16[128,2048]{1,0:T(8,128)(2,1)S(1)}, u32[]{:S(2)}, u32[]{:S(2)}) collective-permute-start(bf16[128,2048]{1,0:T(8,128)(2,1)} %slice.66), channel_id=1, source_target_pairs={{0,1},{1,2},{2,3},{3,0},{4,5},{5,6},{6,7},{7,4},{8,9},{9,10},{10,1... | collective-permute-start | bytes 1572872 | tf_op jit(solution)/shard_map/ppermute | solution.py:26
  40.5 45.7 %collective-permute-start.21 = (bf16[128,2048]{1,0:T(8,128)(2,1)}, bf16[128,2048]{1,0:T(8,128)(2,1)}, u32[]{:S(2)}, u32[]{:S(2)}) collective-permute-start(bf16[128,2048]{1,0:T(8,128)(2,1)} %slice.67), channel_id=1, source_target_pairs={{0,3},{1,0},{2,1},{3,2},{4,7},{5,4},{6,5},{7,6},{8,11},{9,8},{10,9... | collective-permute-start | bytes 1572872 | tf_op jit(solution)/shard_map/ppermute | solution.py:26
  42.1 12.8 %collective-permute-start.7 = (bf16[4,256,256]{2,1,0:T(8,128)(2,1)}, bf16[4,256,256]{2,1,0:T(8,128)(2,1)S(1)}, u32[]{:S(2)}, u32[]{:S(2)}) collective-permute-start(bf16[4,256,256]{2,1,0:T(8,128)(2,1)} %collective-permute-done.4.refs_0_), channel_id=1, source_target_pairs={{0,32},{32,64},{64,96},{96,128},{128,160},{160,192},{192,224},{224... | collective-permute-start | bytes 1572872 | tf_op jit(solution)/shard_map/ppermute | solution.py:33
  44.4 11.7 %collective-permute-start.15 = (bf16[2,256,256]{2,1,0:T(8,128)(2,1)S(1)}, bf16[2,256,256]{2,1,0:T(8,128)(2,1)S(1)}, u32[]{:S(2)}, u32[]{:S(2)}) collective-permute-start(bf16[2,256,256]{2,1,0:T(8,128)(2,1)S(1)} %get-tuple-element.22), channel_id=1, source_target_pairs={{0,8},{8,16},{16,24},{24,0},{1,9},{9,17},{17,25},{25,1},{2,10},{10... | collective-permute-start | bytes 786440 | tf_op jit(solution)/shard_map/ppermute | solution.py:26
  46.2 12.4 %collective-permute-start.16 = (bf16[2,256,256]{2,1,0:T(8,128)(2,1)S(1)}, bf16[2,256,256]{2,1,0:T(8,128)(2,1)S(1)}, u32[]{:S(2)}, u32[]{:S(2)}) collective-permute-start(bf16[2,256,256]{2,1,0:T(8,128)(2,1)S(1)} %get-tuple-element.21), channel_id=1, source_target_pairs={{0,24},{8,0},{16,8},{24,16},{1,25},{9,1},{17,9},{25,17},{2,26},{10... | collective-permute-start | bytes 786440 | tf_op jit(solution)/shard_map/ppermute | solution.py:26
  54.9 10.9 %collective-permute-start.10 = (bf16[4,256,256]{2,1,0:T(8,128)(2,1)S(1)}, bf16[4,256,256]{2,1,0:T(8,128)(2,1)S(1)}, u32[]{:S(2)}, u32[]{:S(2)}) collective-permute-start(bf16[4,256,256]{2,1,0:T(8,128)(2,1)S(1)} %collective-permute-done.7.refs_0_), channel_id=1, source_target_pairs={{0,32},{32,64},{64,96},{96,128},{128,160},{160,192},{192,224},{224... | collective-permute-start | bytes 1572872 | tf_op jit(solution)/shard_map/ppermute | solution.py:33
  56.1 11.9 %collective-permute-start.13 = (bf16[2,256,256]{2,1,0:T(8,128)(2,1)S(1)}, bf16[2,256,256]{2,1,0:T(8,128)(2,1)S(1)}, u32[]{:S(2)}, u32[]{:S(2)}) collective-permute-start(bf16[2,256,256]{2,1,0:T(8,128)(2,1)S(1)} %get-tuple-element.24), channel_id=1, source_target_pairs={{0,8},{8,16},{16,24},{24,0},{1,9},{9,17},{17,25},{25,1},{2,10},{10... | collective-permute-start | bytes 786440 | tf_op jit(solution)/shard_map/ppermute | solution.py:26
  58.7 11.0 %collective-permute-start.14 = (bf16[2,256,256]{2,1,0:T(8,128)(2,1)S(1)}, bf16[2,256,256]{2,1,0:T(8,128)(2,1)S(1)}, u32[]{:S(2)}, u32[]{:S(2)}) collective-permute-start(bf16[2,256,256]{2,1,0:T(8,128)(2,1)S(1)} %get-tuple-element.23), channel_id=1, source_target_pairs={{0,24},{8,0},{16,8},{24,16},{1,25},{9,1},{17,9},{25,17},{2,26},{10... | collective-permute-start | bytes 786440 | tf_op jit(solution)/shard_map/ppermute | solution.py:26
  65.9 7.2 %collective-permute-start.11 = (bf16[2,256,256]{2,1,0:T(8,128)(2,1)S(1)}, bf16[2,256,256]{2,1,0:T(8,128)(2,1)S(1)}, u32[]{:S(2)}, u32[]{:S(2)}) collective-permute-start(bf16[2,256,256]{2,1,0:T(8,128)(2,1)S(1)} %get-tuple-element.26), channel_id=1, source_target_pairs={{0,8},{8,16},{16,24},{24,0},{1,9},{9,17},{17,25},{25,1},{2,10},{10... | collective-permute-start | bytes 786440 | tf_op jit(solution)/shard_map/ppermute | solution.py:26
  68.0 7.5 %collective-permute-start.12 = (bf16[2,256,256]{2,1,0:T(8,128)(2,1)S(1)}, bf16[2,256,256]{2,1,0:T(8,128)(2,1)S(1)}, u32[]{:S(2)}, u32[]{:S(2)}) collective-permute-start(bf16[2,256,256]{2,1,0:T(8,128)(2,1)S(1)} %get-tuple-element.25), channel_id=1, source_target_pairs={{0,24},{8,0},{16,8},{24,16},{1,25},{9,1},{17,9},{25,17},{2,26},{10... | collective-permute-start | bytes 786440 | tf_op jit(solution)/shard_map/ppermute | solution.py:26
  77.7 14.4 %copy-start.9 = (f32[2048]{0:T(1024)S(1)}, f32[2048]{0:T(1024)}, u32[]{:S(2)}) copy-start(f32[2048]{0:T(1024)} %param.19) | copy-start | bytes 24580
  77.7 3.1 %collective-permute-start.17 = (f32[2,512,128]{2,1,0:T(8,128)}, f32[2,512,128]{2,1,0:T(8,128)}, u32[]{:S(2)}, u32[]{:S(2)}) collective-permute-start(f32[2,512,128]{2,1,0:T(8,128)} %get-tuple-element.17), channel_id=1, source_target_pairs={{0,4},{4,0},{1,5},{5,1},{2,6},{6,2},{3,7},{7,3},{8,12},{12,8},{9,1... | collective-permute-start | bytes 1572872 | tf_op jit(solution)/shard_map/ppermute | solution.py:26
  82.6 9.5 %all-to-all-start = ((bf16[4,64,256]{2,1,0:T(8,128)(2,1)}), bf16[4,64,256]{2,1,0:T(8,128)(2,1)S(1)}, u32[]{:S(2)}, u32[]{:S(2)}) async-start(bf16[4,64,256]{2,1,0:T(8,128)(2,1)} %bitcast.6), calls=%async_computation | async-start | bytes 262144 | tf_op jit(solution)/shard_map/all_to_all | solution.py:415
  93.0 71.0 %copy-start.12 = (bf16[1,384,2048]{2,1,0:T(8,128)(2,1)S(1)}, bf16[1,384,2048]{2,1,0:T(8,128)(2,1)}, u32[]{:S(2)}) copy-start(bf16[1,384,2048]{2,1,0:T(8,128)(2,1)} %param.24) | copy-start | bytes 4718596
  96.2 67.9 %copy-start.5 = (bf16[64,2048]{1,0:T(8,128)(2,1)}, bf16[64,2048]{1,0:T(8,128)(2,1)S(1)}, u32[]{:S(2)}) copy-start(bf16[64,2048]{1,0:T(8,128)(2,1)S(1)} %get-tuple-element.19.mid_ref) | copy-start | bytes 786436
  96.2 67.9 %copy-start.7 = (bf16[64,2048]{1,0:T(8,128)(2,1)}, bf16[64,2048]{1,0:T(8,128)(2,1)S(1)}, u32[]{:S(2)}) copy-start(bf16[64,2048]{1,0:T(8,128)(2,1)S(1)} %get-tuple-element.18.normed_ref) | copy-start | bytes 786436
  96.2 67.9 %copy-start.10 = (bf16[1,2048,384]{2,1,0:T(8,128)(2,1)S(1)}, bf16[1,2048,384]{2,1,0:T(8,128)(2,1)}, u32[]{:S(2)}) copy-start(bf16[1,2048,384]{2,1,0:T(8,128)(2,1)} %param.22) | copy-start | bytes 4718596
  96.2 67.9 %copy-start.11 = (bf16[1,2048,384]{2,1,0:T(8,128)(2,1)S(1)}, bf16[1,2048,384]{2,1,0:T(8,128)(2,1)}, u32[]{:S(2)}) copy-start(bf16[1,2048,384]{2,1,0:T(8,128)(2,1)} %param.23) | copy-start | bytes 4718596
  169.7 56.8 %all-to-all-start.2 = ((bf16[64,8,2048]{2,1,0:T(8,128)(2,1)}), bf16[64,8,2048]{2,1,0:T(8,128)(2,1)S(1)}, u32[]{:S(2)}, u32[]{:S(2)}) async-start(bf16[64,8,2048]{2,1,0:T(8,128)(2,1)} %bitcast.35), calls=%async_computation.2 | async-start | bytes 4194304 | tf_op jit(solution)/shard_map/all_to_all | solution.py:433
  (12 other events, 52.6 us)

commit v4 on v3

--- a/solution.py
+++ b/solution.py
@@ -63,10 +63,10 @@
             plane[place + core] = ref[first + core]
 
 
-def block_steps(q_ref, plane_ref, acc, carry, tri, level_buf, penalty_buf, first_row, tok, base=0):
-    rows = acc.shape[0]
-
-    def scores(j, slot, diagonal=False):
+def block_steps(q_ref, plane_ref, acc, carry, tri, level_buf, penalty_buf, tok, base=0):
+    rows = level_buf.shape[1]
+
+    def scores(first_row, j, slot, diagonal=False):
         keys = plane_ref[base + j, :, 0:HD]
         y = lax.dot_general(
             q_ref[pl.ds(first_row, rows), :],
@@ -84,25 +84,22 @@
         level_buf[slot] = level
         penalty_buf[slot] = penalty.astype(jnp.bfloat16)
 
-    def mix(j, slot):
+    def mix(first_row, j, slot):
+        here = pl.ds(first_row, rows)
         penalty = penalty_buf[slot]
         after = jnp.dot(penalty, tri[...], preferred_element_type=jnp.float32)
-        so_far = carry[...]
+        so_far = carry[here, :]
         weights = jnp.exp2(level_buf[slot] - after - jnp.concatenate([so_far, so_far], axis=1))
-        carry[...] = so_far + jnp.broadcast_to(
+        carry[here, :] = so_far + jnp.broadcast_to(
             after[:, 0:1] + penalty[:, 0:1].astype(jnp.float32), (rows, HD)
         )
-        acc[...] += jnp.dot(
+        acc[here, :] += jnp.dot(
             weights.astype(jnp.bfloat16),
             plane_ref[base + j, :, HD : 2 * HD],
             preferred_element_type=jnp.float32,
         )
 
-    def both(j, slot):
-        mix(j, slot)
-        scores(j - 1, 1 - slot)
-
-    return scores, mix, both
+    return scores, mix
 
 
 def clear(acc, carry, tri):
@@ -136,11 +133,15 @@
     clear(acc, carry, tri)
     join_plane(at_ref, part_ref, before_ref, after_ref, plane)
     first_row = pl.multiple_of(core * rows, rows)
-    scores, mix, both = block_steps(
-        q_buf, plane, acc, carry, tri, level_buf, penalty_buf, first_row, own_ref.shape[0]
+    scores, mix = block_steps(
+        q_buf, plane, acc, carry, tri, level_buf, penalty_buf, own_ref.shape[0]
     )
     pos = 2 * at_ref[1] + core
-    scores(pos, 0, diagonal=True)
+    scores(first_row, pos, 0, diagonal=True)
+
+    def both(j, slot):
+        mix(0, j, slot)
+        scores(first_row, j - 1, 1 - slot)
 
     def step(i, _):
         both(pos - 2 * i, 0)
@@ -152,11 +153,11 @@
     @pl.when(pos % 2 == 1)
     def _():
         both(1, 0)
-        mix(0, 1)
+        mix(0, 0, 1)
 
     @pl.when(pos % 2 == 0)
     def _():
-        mix(0, 0)
+        mix(0, 0, 0)
 
     out_ref[0] = acc[...]
     out_ref[1] = carry[...]
@@ -171,7 +172,7 @@
     else:
         out_ref, *refs = refs
     q_buf, acc, carry, tri, level_buf, penalty_buf, plane = refs
-    rows = acc.shape[0]
+    rows = level_buf.shape[1]
     core = at_ref[2]
     below = jnp.where(core == 0, distance, z_size - distance)
     visible = below <= at_ref[0]
@@ -179,34 +180,32 @@
     upward = core == 0
     base = shards * (1 - core) if last else 0
 
+    clear(acc, carry, tri)
+
     @pl.when(visible)
     def _():
         scale_queries(at_ref, own_ref, other_ref, q_buf)
         join_plane(at_ref, part_ref, before_ref, after_ref, plane)
+        scores, mix = block_steps(
+            q_buf, plane, acc, carry, tri, level_buf, penalty_buf, own_ref.shape[0], base
+        )
+
+        def unit(u):
+            return pl.multiple_of(u // shards * rows, rows), shards - 1 - u % shards
+
+        def step(i, _):
+            for slot in range(2):
+                mix(*unit(2 * i + slot), slot)
+                scores(*unit(jnp.minimum(2 * i + slot + 1, 2 * shards - 1)), 1 - slot)
+            return 0
+
+        scores(*unit(jnp.int32(0)), 0)
+        lax.fori_loop(0, shards, step, 0)
 
     def part(turn, _):
         first_row = pl.multiple_of(jnp.where(turn == 0, 1 - core, core) * rows, rows)
         here = pl.ds(first_row, rows)
-        clear(acc, carry, tri)
-
-        @pl.when(visible)
-        def _():
-            scores, mix, both = block_steps(
-                q_buf, plane, acc, carry, tri, level_buf, penalty_buf, first_row,
-                own_ref.shape[0], base,
-            )
-            scores(shards - 1, 0)
-
-            def step(i, _):
-                both(shards - 1 - 2 * i, 0)
-                both(shards - 2 - 2 * i, 1)
-                return 0
-
-            lax.fori_loop(0, shards // 2 - 1, step, 0)
-            both(1, 0)
-            mix(0, 1)
-
-        result, total = acc[...], carry[...]
+        result, total = acc[here, :], carry[here, :]
         if not first:
             old, old_total = state[0, here, :], state[1, here, :]
             result = result * jnp.exp2(jnp.where(upward, -old_total, 0.0))
@@ -260,15 +259,17 @@
         after = shifted(value[2:], "sp_1", -1)
         return value, before, after
 
-    scratch = [
-        pltpu.VMEM((2 * rows, 2 * HD), jnp.bfloat16),
-        pltpu.VMEM((rows, HD), jnp.float32),
-        pltpu.VMEM((rows, HD), jnp.float32),
-        pltpu.VMEM((BK, BK), jnp.bfloat16),
-        pltpu.VMEM((2, rows, BK), jnp.float32),
-        pltpu.VMEM((2, rows, BK), jnp.bfloat16),
-        pltpu.VMEM((2 * y_size, tok, 2 * HD), jnp.bfloat16),
-    ]
+    def scratch(state_rows):
+        return [
+            pltpu.VMEM((2 * rows, 2 * HD), jnp.bfloat16),
+            pltpu.VMEM((state_rows, HD), jnp.float32),
+            pltpu.VMEM((state_rows, HD), jnp.float32),
+            pltpu.VMEM((BK, BK), jnp.bfloat16),
+            pltpu.VMEM((2, rows, BK), jnp.float32),
+            pltpu.VMEM((2, rows, BK), jnp.bfloat16),
+            pltpu.VMEM((2 * y_size, tok, 2 * HD), jnp.bfloat16),
+        ]
+
     work = 2 * y_size * rows * BK * HD * 16
     held = from_neighbours(part)
     other_query = shifted(query, "sp_2", 1)
@@ -276,7 +277,7 @@
         own_plane_kernel,
         [((2, rows, HD), jnp.float32)],
         (at, query, other_query, *held),
-        scratch,
+        scratch(rows),
         work // 2,
     )
     state = ()
@@ -294,7 +295,7 @@
             if last
             else [((2, 2 * rows, HD), jnp.float32)],
             (at, query, other_query, *held) + state + ((closest,) if last else ()),
-            scratch,
+            scratch(2 * rows),
             work * 2,
         )
         state = tuple(state)

time: 230 us -> 229 us (level)
  no operation moved by 1% of the time
where the time goes in v4:
time: 229 us
  waiting for transfers between devices  82.3 us (36%)
  blocking collectives  67.9 us (30%)
  starting transfers between devices  39.3 us (17%)
  Pallas kernels  21 us (9%)
  local copies, waits for them, and re-layouts  15.5 us (7%)
    all_to_all x1, blocking collectives, per_device(): arrived = lax.all_to_all(outgoing.reshape(exchange), SP, 0, 0, tiled=True)  67.9 us
    all_to_all x1, waiting for transfers between devices, per_device(): returned = lax.all_to_all(produced.reshape(exchange), SP, 0, 0, tiled=True)  45.4 us
    ppermute x18, starting transfers between devices, shifted(): lax.ppermute(value, axis, [(i, (i + step) % size) for i in range(size)])  26 us
    pallas_call x11, Pallas kernels, call(): pl.pallas_call(kernel, out_shape=[jax.ShapeDtypeStruct(*out) for out in o...  21 us
    ppermute x4, waiting for transfers between devices, counter_shifted(): return lax.ppermute(value, ('sp_0', 'sp_2'), pairs)  16.5 us
    ppermute x18, waiting for transfers between devices, shifted(): lax.ppermute(value, axis, [(i, (i + step) % size) for i in range(size)])  14.8 us
    unnamed x43, local copies, waits for them, and re-layouts  8.56 us
    all_to_all x1, waiting for transfers between devices, per_device(): lax.all_to_all(heads_out.reshape(-1, own_rows, heads_out.shape[1]), 'tp',...  5.62 us
  transfers between devices with their start and end apart: 24, of which 11 were waited for; matrix products, arithmetic and copies ran while one was open for 4% of the time, Pallas kernels for 5%

profile of v4, /device:TPU:8, one launch (start us, length us, event | category | flops | bytes accessed | tf_op | source)
XLA Modules:
  0.0 228.6 jit_solution(9978311162275409979)
XLA Ops:
  1.8 2.2 collective-permute-start.1
  4.0 3.1 %collective-permute-done.1 = bf16[256,256]{1,0:T(8,128)(2,1)S(1)} collective-permute-done((bf16[256,256]{1,0:T(8,128)(2,1)S(1)}, bf16[256,256]{1,0:T(8,128)(2,1)S(1)}, u32[]{:S(2)}, u32[]{:S(2)}) %collective-permute-start.1) | collective-permute-done | bytes 131104 | tf_op jit(solution)/shard_map/ppermute | solution.py:26
  9.3 2.0 collective-permute-start.3
  11.3 1.5 collective-permute-start.18
  12.8 1.7 collective-permute-start.20
  14.5 3.2 %collective-permute-start = (bf16[256,256]{1,0:T(8,128)(2,1)S(1)}, bf16[256,256]{1,0:T(8,128)(2,1)S(1)}, u32[]{:S(2)}, u32[]{:S(2)}) collective-permute-start(bf16[256,256]{1,0:T(8,128)(2,1)S(1)} %copy-done.13), channel_id=1, source_target_pairs={{0,4},{4,0},{1,5},{5,1},{2,6},{6,2},{3,7},{7,3},{8,12},{12,8},{9,1... | collective-permute-start | bytes 393224 | tf_op jit(solution)/shard_map/ppermute | solution.py:26
  17.8 4.7 %collective-permute-done.3.refs_0_ = bf16[4,256,256]{2,1,0:T(8,128)(2,1)} collective-permute-done((bf16[4,256,256]{2,1,0:T(8,128)(2,1)S(1)}, bf16[4,256,256]{2,1,0:T(8,128)(2,1)}, u32[]{:S(2)}, u32[]{:S(2)}) %collective-permute-start.3) | collective-permute-done | bytes 524320 | tf_op jit(solution)/shard_map/ppermute | solution.py:33
  23.3 1.6 collective-permute-start.5
  26.6 4.9 %collective-permute-done.5.before_ref = bf16[2,256,256]{2,1,0:T(8,128)(2,1)S(1)} collective-permute-done((bf16[2,256,256]{2,1,0:T(8,128)(2,1)}, bf16[2,256,256]{2,1,0:T(8,128)(2,1)S(1)}, u32[]{:S(2)}, u32[]{:S(2)}) %collective-permute-start.5) | collective-permute-done | bytes 262176 | tf_op jit(solution)/shard_map/ppermute | solution.py:26
  31.6 1.7 collective-permute-start.8
  34.9 2.2 shard_map.137.refs_4_
  38.0 1.7 collective-permute-start.19
  40.5 1.6 collective-permute-start.21
  44.4 1.9 collective-permute-start.15
  48.2 6.7 %collective-permute-done.7.refs_0_ = bf16[4,256,256]{2,1,0:T(8,128)(2,1)S(1)} collective-permute-done((bf16[4,256,256]{2,1,0:T(8,128)(2,1)}, bf16[4,256,256]{2,1,0:T(8,128)(2,1)S(1)}, u32[]{:S(2)}, u32[]{:S(2)}) %collective-permute-start.7) | collective-permute-done | bytes 524320 | tf_op jit(solution)/shard_map/ppermute | solution.py:33
  56.0 2.6 %collective-permute-start.13 = (bf16[2,256,256]{2,1,0:T(8,128)(2,1)S(1)}, bf16[2,256,256]{2,1,0:T(8,128)(2,1)S(1)}, u32[]{:S(2)}, u32[]{:S(2)}) collective-permute-start(bf16[2,256,256]{2,1,0:T(8,128)(2,1)S(1)} %get-tuple-element.24), channel_id=1, source_target_pairs={{0,8},{8,16},{16,24},{24,0},{1,9},{9,17},{17,25},{25,1},{2,10},{10... | collective-permute-start | bytes 786440 | tf_op jit(solution)/shard_map/ppermute | solution.py:26
  60.7 5.0 %collective-permute-done.10.refs_0_ = bf16[4,256,256]{2,1,0:T(8,128)(2,1)S(1)} collective-permute-done((bf16[4,256,256]{2,1,0:T(8,128)(2,1)S(1)}, bf16[4,256,256]{2,1,0:T(8,128)(2,1)S(1)}, u32[]{:S(2)}, u32[]{:S(2)}) %collective-permute-start.10) | collective-permute-done | bytes 524320 | tf_op jit(solution)/shard_map/ppermute | solution.py:33
  65.8 2.1 collective-permute-start.11
  67.9 1.7 collective-permute-start.12
  70.5 2.5 %collective-permute-done.11.refs_1_ = bf16[2,256,256]{2,1,0:T(8,128)(2,1)S(1)} collective-permute-done((bf16[2,256,256]{2,1,0:T(8,128)(2,1)S(1)}, bf16[2,256,256]{2,1,0:T(8,128)(2,1)S(1)}, u32[]{:S(2)}, u32[]{:S(2)}) %collective-permute-start.11) | collective-permute-done | bytes 262176 | tf_op jit(solution)/shard_map/ppermute | solution.py:26
  73.0 2.5 %collective-permute-done.12.refs_2_ = bf16[2,256,256]{2,1,0:T(8,128)(2,1)S(1)} collective-permute-done((bf16[2,256,256]{2,1,0:T(8,128)(2,1)S(1)}, bf16[2,256,256]{2,1,0:T(8,128)(2,1)S(1)}, u32[]{:S(2)}, u32[]{:S(2)}) %collective-permute-start.12) | collective-permute-done | bytes 262176 | tf_op jit(solution)/shard_map/ppermute | solution.py:26
  75.5 1.9 shard_map.141
  80.4 1.8 shard_map.142
  82.3 3.5 %all-to-all-start = ((bf16[4,64,256]{2,1,0:T(8,128)(2,1)}), bf16[4,64,256]{2,1,0:T(8,128)(2,1)S(1)}, u32[]{:S(2)}, u32[]{:S(2)}) async-start(bf16[4,64,256]{2,1,0:T(8,128)(2,1)} %bitcast.6), calls=%async_computation | async-start | bytes 262144 | tf_op jit(solution)/shard_map/all_to_all | solution.py:416
  86.1 5.6 %all-to-all-done.heads_ref = bf16[4,64,256]{2,1,0:T(8,128)(2,1)S(1)} async-done(((bf16[4,64,256]{2,1,0:T(8,128)(2,1)}), bf16[4,64,256]{2,1,0:T(8,128)(2,1)S(1)}, u32[]{:S(2)}, u32[]{:S(2)}) %all-to-all-start) | async-done | bytes 131104 | tf_op jit(solution)/shard_map/all_to_all | solution.py:416
  92.7 3.1 %shard_map.143 = (bf16[64,2048]{1,0:T(8,128)(2,1)S(1)}, bf16[64,2048]{1,0:T(8,128)(2,1)S(1)}, bf16[512,2048]{1,0:T(8,128)(2,1)S(1)}) custom-call(s32[4]{0:T(128)S(1)} %pad_add_fusion.at_ref, bf16[4,64,256]{2,1,0:T(8,128)(2,1)S(1)} %all-to-all-done.heads_ref, bf16[256,2048]{1,0:T(8,128)(2,1)} %w0.1, bf16[256,2048]{1,0:T(8,128)(2,1)S(1)} %collective-permute-done.18.w1, ...), custom_call_target="tpu_custom_call" | custom-call | flops 536870912 | bytes 1048576 | tf_op jit(solution)/shard_map/pallas_call | solution.py:38
  95.9 67.9 %all_to_all.15 = bf16[64,8,2048]{2,1,0:T(8,128)(2,1)S(1)} all-to-all(bf16[64,8,2048]{2,1,0:T(8,128)(2,1)S(1)} %bitcast.36), channel_id=1, replica_groups=mesh['sp_0'=8,'sp_1'=4,'sp_2'=2,'tp'=4] {'sp_0','sp_1','sp_2'}, dimensions={0} | all-to-all | bytes 4194304 | tf_op jit(solution)/shard_map/all_to_all | solution.py:427
  163.9 4.3 %shard_map.145 = bf16[512,2048]{1,0:T(8,128)(2,1)S(1)} custom-call(s32[4]{0:T(128)S(1)} %pad_add_fusion.at_ref, bf16[512,2048]{1,0:T(8,128)(2,1)S(1)} %bitcast.37, bf16[2048,384]{1,0:T(8,128)(2,1)S(1)} %bitcast.39, bf16[2048,384]{1,0:T(8,128)(2,1)S(1)} %bitcast.40, bf16[384,2048]{1,0:T(8,128)(2,1)S(1)} %bitcast.41), custom_call_target="tpu_custom_call" | custom-call | flops 4294967296 | bytes 1048576 | tf_op jit(solution)/shard_map/pallas_call | solution.py:38
  169.6 5.5 %all-to-all-start.2 = ((bf16[64,8,2048]{2,1,0:T(8,128)(2,1)}), bf16[64,8,2048]{2,1,0:T(8,128)(2,1)S(1)}, u32[]{:S(2)}, u32[]{:S(2)}) async-start(bf16[64,8,2048]{2,1,0:T(8,128)(2,1)} %bitcast.35), calls=%async_computation.2 | async-start | bytes 4194304 | tf_op jit(solution)/shard_map/all_to_all | solution.py:434
  179.5 1.5 shard_map.144.base_ref
  181.0 45.4 %all-to-all-done.2 = bf16[64,8,2048]{2,1,0:T(8,128)(2,1)S(1)} async-done(((bf16[64,8,2048]{2,1,0:T(8,128)(2,1)}), bf16[64,8,2048]{2,1,0:T(8,128)(2,1)S(1)}, u32[]{:S(2)}, u32[]{:S(2)}) %all-to-all-start.2) | async-done | bytes 2097184 | tf_op jit(solution)/shard_map/all_to_all | solution.py:434
  226.4 2.2 shard_map.146
  (93 shorter events, 28.2 us)
Async XLA Ops:
  0.0 14.5 %copy-start.13 = (bf16[256,256]{1,0:T(8,128)(2,1)S(1)}, bf16[256,256]{1,0:T(8,128)(2,1)}, u32[]{:S(2)}) copy-start(bf16[256,256]{1,0:T(8,128)(2,1)} %own_ref.9) | copy-start | bytes 393220
  0.0 25.4 %copy-start.18 = (s32[64,4]{0,1:T(4,128)S(1)}, s32[64,4]{0,1:T(4,128)}, u32[]{:S(2)}) copy-start(s32[64,4]{0,1:T(4,128)} %param.20) | copy-start | bytes 3076
  1.8 5.3 %collective-permute-start.1 = (bf16[256,256]{1,0:T(8,128)(2,1)S(1)}, bf16[256,256]{1,0:T(8,128)(2,1)S(1)}, u32[]{:S(2)}, u32[]{:S(2)}) collective-permute-start(bf16[256,256]{1,0:T(8,128)(2,1)S(1)} %constant_dynamic-update-slice_fusion), channel_id=1, source_target_pairs={{0,24},{8,0},{16,8},{24,16},{1,25},{9,1},{17,9},{25,17},{2,26},{10... | collective-permute-start | bytes 393224 | tf_op jit(solution)/shard_map/ppermute | solution.py:26
  7.1 1.6 collective-permute-start.2
  9.3 13.2 %collective-permute-start.3 = (bf16[4,256,256]{2,1,0:T(8,128)(2,1)S(1)}, bf16[4,256,256]{2,1,0:T(8,128)(2,1)}, u32[]{:S(2)}, u32[]{:S(2)}) collective-permute-start(bf16[4,256,256]{2,1,0:T(8,128)(2,1)S(1)} %shard_map.136.part_ref), channel_id=1, source_target_pairs={{0,32},{32,64},{64,96},{96,128},{128,160},{160,192},{192,224},{224... | collective-permute-start | bytes 1572872 | tf_op jit(solution)/shard_map/ppermute | solution.py:33
  11.3 25.8 %collective-permute-start.18 = (bf16[256,2048]{1,0:T(8,128)(2,1)}, bf16[256,2048]{1,0:T(8,128)(2,1)S(1)}, u32[]{:S(2)}, u32[]{:S(2)}) collective-permute-start(bf16[256,2048]{1,0:T(8,128)(2,1)} %w0.1), channel_id=1, source_target_pairs={{0,1},{1,2},{2,3},{3,0},{4,5},{5,6},{6,7},{7,4},{8,9},{9,10},{10,1... | collective-permute-start | bytes 3145736 | tf_op jit(solution)/shard_map/ppermute | solution.py:26
  12.8 26.9 %collective-permute-start.20 = (bf16[256,2048]{1,0:T(8,128)(2,1)}, bf16[256,2048]{1,0:T(8,128)(2,1)S(1)}, u32[]{:S(2)}, u32[]{:S(2)}) collective-permute-start(bf16[256,2048]{1,0:T(8,128)(2,1)} %w0.1), channel_id=1, source_target_pairs={{0,3},{1,0},{2,1},{3,2},{4,7},{5,4},{6,5},{7,6},{8,11},{9,8},{10,9... | collective-permute-start | bytes 3145736 | tf_op jit(solution)/shard_map/ppermute | solution.py:26
  14.5 10.4 %collective-permute-start = (bf16[256,256]{1,0:T(8,128)(2,1)S(1)}, bf16[256,256]{1,0:T(8,128)(2,1)S(1)}, u32[]{:S(2)}, u32[]{:S(2)}) collective-permute-start(bf16[256,256]{1,0:T(8,128)(2,1)S(1)} %copy-done.13), channel_id=1, source_target_pairs={{0,4},{4,0},{1,5},{5,1},{2,6},{6,2},{3,7},{7,3},{8,12},{12,8},{9,1... | collective-permute-start | bytes 393224 | tf_op jit(solution)/shard_map/ppermute | solution.py:26
  22.5 19.6 %collective-permute-start.4 = (bf16[4,256,256]{2,1,0:T(8,128)(2,1)}, bf16[4,256,256]{2,1,0:T(8,128)(2,1)}, u32[]{:S(2)}, u32[]{:S(2)}) collective-permute-start(bf16[4,256,256]{2,1,0:T(8,128)(2,1)} %collective-permute-done.3.refs_0_), channel_id=1, source_target_pairs={{0,32},{32,64},{64,96},{96,128},{128,160},{160,192},{192,224},{224... | collective-permute-start | bytes 1572872 | tf_op jit(solution)/shard_map/ppermute | solution.py:33
  23.3 8.2 %collective-permute-start.5 = (bf16[2,256,256]{2,1,0:T(8,128)(2,1)}, bf16[2,256,256]{2,1,0:T(8,128)(2,1)S(1)}, u32[]{:S(2)}, u32[]{:S(2)}) collective-permute-start(bf16[2,256,256]{2,1,0:T(8,128)(2,1)} %get-tuple-element.30), channel_id=1, source_target_pairs={{0,8},{8,16},{16,24},{24,0},{1,9},{9,17},{17,25},{25,1},{2,10},{10... | collective-permute-start | bytes 786440 | tf_op jit(solution)/shard_map/ppermute | solution.py:26
  24.9 8.7 %collective-permute-start.6 = (bf16[2,256,256]{2,1,0:T(8,128)(2,1)}, bf16[2,256,256]{2,1,0:T(8,128)(2,1)S(1)}, u32[]{:S(2)}, u32[]{:S(2)}) collective-permute-start(bf16[2,256,256]{2,1,0:T(8,128)(2,1)} %get-tuple-element.29), channel_id=1, source_target_pairs={{0,24},{8,0},{16,8},{24,16},{1,25},{9,1},{17,9},{25,17},{2,26},{10... | collective-permute-start | bytes 786440 | tf_op jit(solution)/shard_map/ppermute | solution.py:26
  31.6 12.8 %collective-permute-start.8 = (bf16[2,256,256]{2,1,0:T(8,128)(2,1)S(1)}, bf16[2,256,256]{2,1,0:T(8,128)(2,1)S(1)}, u32[]{:S(2)}, u32[]{:S(2)}) collective-permute-start(bf16[2,256,256]{2,1,0:T(8,128)(2,1)S(1)} %get-tuple-element.28), channel_id=1, source_target_pairs={{0,8},{8,16},{16,24},{24,0},{1,9},{9,17},{17,25},{25,1},{2,10},{10... | collective-permute-start | bytes 786440 | tf_op jit(solution)/shard_map/ppermute | solution.py:26
  33.6 12.6 %collective-permute-start.9 = (bf16[2,256,256]{2,1,0:T(8,128)(2,1)S(1)}, bf16[2,256,256]{2,1,0:T(8,128)(2,1)S(1)}, u32[]{:S(2)}, u32[]{:S(2)}) collective-permute-start(bf16[2,256,256]{2,1,0:T(8,128)(2,1)S(1)} %get-tuple-element.27), channel_id=1, source_target_pairs={{0,24},{8,0},{16,8},{24,16},{1,25},{9,1},{17,9},{25,17},{2,26},{10... | collective-permute-start | bytes 786440 | tf_op jit(solution)/shard_map/ppermute | solution.py:26
  38.0 48.1 %collective-permute-start.19 = (bf16[128,2048]{1,0:T(8,128)(2,1)}, bf16[128,2048]{1,0:T(8,128)(2,1)S(1)}, u32[]{:S(2)}, u32[]{:S(2)}) collective-permute-start(bf16[128,2048]{1,0:T(8,128)(2,1)} %slice.66), channel_id=1, source_target_pairs={{0,1},{1,2},{2,3},{3,0},{4,5},{5,6},{6,7},{7,4},{8,9},{9,10},{10,1... | collective-permute-start | bytes 1572872 | tf_op jit(solution)/shard_map/ppermute | solution.py:26
  40.5 45.6 %collective-permute-start.21 = (bf16[128,2048]{1,0:T(8,128)(2,1)}, bf16[128,2048]{1,0:T(8,128)(2,1)}, u32[]{:S(2)}, u32[]{:S(2)}) collective-permute-start(bf16[128,2048]{1,0:T(8,128)(2,1)} %slice.67), channel_id=1, source_target_pairs={{0,3},{1,0},{2,1},{3,2},{4,7},{5,4},{6,5},{7,6},{8,11},{9,8},{10,9... | collective-permute-start | bytes 1572872 | tf_op jit(solution)/shard_map/ppermute | solution.py:26
  42.1 12.8 %collective-permute-start.7 = (bf16[4,256,256]{2,1,0:T(8,128)(2,1)}, bf16[4,256,256]{2,1,0:T(8,128)(2,1)S(1)}, u32[]{:S(2)}, u32[]{:S(2)}) collective-permute-start(bf16[4,256,256]{2,1,0:T(8,128)(2,1)} %collective-permute-done.4.refs_0_), channel_id=1, source_target_pairs={{0,32},{32,64},{64,96},{96,128},{128,160},{160,192},{192,224},{224... | collective-permute-start | bytes 1572872 | tf_op jit(solution)/shard_map/ppermute | solution.py:33
  44.4 11.6 %collective-permute-start.15 = (bf16[2,256,256]{2,1,0:T(8,128)(2,1)S(1)}, bf16[2,256,256]{2,1,0:T(8,128)(2,1)S(1)}, u32[]{:S(2)}, u32[]{:S(2)}) collective-permute-start(bf16[2,256,256]{2,1,0:T(8,128)(2,1)S(1)} %get-tuple-element.22), channel_id=1, source_target_pairs={{0,8},{8,16},{16,24},{24,0},{1,9},{9,17},{17,25},{25,1},{2,10},{10... | collective-permute-start | bytes 786440 | tf_op jit(solution)/shard_map/ppermute | solution.py:26
  46.2 12.3 %collective-permute-start.16 = (bf16[2,256,256]{2,1,0:T(8,128)(2,1)S(1)}, bf16[2,256,256]{2,1,0:T(8,128)(2,1)S(1)}, u32[]{:S(2)}, u32[]{:S(2)}) collective-permute-start(bf16[2,256,256]{2,1,0:T(8,128)(2,1)S(1)} %get-tuple-element.21), channel_id=1, source_target_pairs={{0,24},{8,0},{16,8},{24,16},{1,25},{9,1},{17,9},{25,17},{2,26},{10... | collective-permute-start | bytes 786440 | tf_op jit(solution)/shard_map/ppermute | solution.py:26
  54.9 10.8 %collective-permute-start.10 = (bf16[4,256,256]{2,1,0:T(8,128)(2,1)S(1)}, bf16[4,256,256]{2,1,0:T(8,128)(2,1)S(1)}, u32[]{:S(2)}, u32[]{:S(2)}) collective-permute-start(bf16[4,256,256]{2,1,0:T(8,128)(2,1)S(1)} %collective-permute-done.7.refs_0_), channel_id=1, source_target_pairs={{0,32},{32,64},{64,96},{96,128},{128,160},{160,192},{192,224},{224... | collective-permute-start | bytes 1572872 | tf_op jit(solution)/shard_map/ppermute | solution.py:33
  56.0 11.9 %collective-permute-start.13 = (bf16[2,256,256]{2,1,0:T(8,128)(2,1)S(1)}, bf16[2,256,256]{2,1,0:T(8,128)(2,1)S(1)}, u32[]{:S(2)}, u32[]{:S(2)}) collective-permute-start(bf16[2,256,256]{2,1,0:T(8,128)(2,1)S(1)} %get-tuple-element.24), channel_id=1, source_target_pairs={{0,8},{8,16},{16,24},{24,0},{1,9},{9,17},{17,25},{25,1},{2,10},{10... | collective-permute-start | bytes 786440 | tf_op jit(solution)/shard_map/ppermute | solution.py:26
  58.6 11.1 %collective-permute-start.14 = (bf16[2,256,256]{2,1,0:T(8,128)(2,1)S(1)}, bf16[2,256,256]{2,1,0:T(8,128)(2,1)S(1)}, u32[]{:S(2)}, u32[]{:S(2)}) collective-permute-start(bf16[2,256,256]{2,1,0:T(8,128)(2,1)S(1)} %get-tuple-element.23), channel_id=1, source_target_pairs={{0,24},{8,0},{16,8},{24,16},{1,25},{9,1},{17,9},{25,17},{2,26},{10... | collective-permute-start | bytes 786440 | tf_op jit(solution)/shard_map/ppermute | solution.py:26
  65.8 7.2 %collective-permute-start.11 = (bf16[2,256,256]{2,1,0:T(8,128)(2,1)S(1)}, bf16[2,256,256]{2,1,0:T(8,128)(2,1)S(1)}, u32[]{:S(2)}, u32[]{:S(2)}) collective-permute-start(bf16[2,256,256]{2,1,0:T(8,128)(2,1)S(1)} %get-tuple-element.26), channel_id=1, source_target_pairs={{0,8},{8,16},{16,24},{24,0},{1,9},{9,17},{17,25},{25,1},{2,10},{10... | collective-permute-start | bytes 786440 | tf_op jit(solution)/shard_map/ppermute | solution.py:26
  67.9 7.6 %collective-permute-start.12 = (bf16[2,256,256]{2,1,0:T(8,128)(2,1)S(1)}, bf16[2,256,256]{2,1,0:T(8,128)(2,1)S(1)}, u32[]{:S(2)}, u32[]{:S(2)}) collective-permute-start(bf16[2,256,256]{2,1,0:T(8,128)(2,1)S(1)} %get-tuple-element.25), channel_id=1, source_target_pairs={{0,24},{8,0},{16,8},{24,16},{1,25},{9,1},{17,9},{25,17},{2,26},{10... | collective-permute-start | bytes 786440 | tf_op jit(solution)/shard_map/ppermute | solution.py:26
  77.4 14.4 %copy-start.9 = (f32[2048]{0:T(1024)S(1)}, f32[2048]{0:T(1024)}, u32[]{:S(2)}) copy-start(f32[2048]{0:T(1024)} %param.19) | copy-start | bytes 24580
  77.4 3.1 %collective-permute-start.17 = (f32[2,512,128]{2,1,0:T(8,128)}, f32[2,512,128]{2,1,0:T(8,128)}, u32[]{:S(2)}, u32[]{:S(2)}) collective-permute-start(f32[2,512,128]{2,1,0:T(8,128)} %get-tuple-element.17), channel_id=1, source_target_pairs={{0,4},{4,0},{1,5},{5,1},{2,6},{6,2},{3,7},{7,3},{8,12},{12,8},{9,1... | collective-permute-start | bytes 1572872 | tf_op jit(solution)/shard_map/ppermute | solution.py:26
  82.3 9.5 %all-to-all-start = ((bf16[4,64,256]{2,1,0:T(8,128)(2,1)}), bf16[4,64,256]{2,1,0:T(8,128)(2,1)S(1)}, u32[]{:S(2)}, u32[]{:S(2)}) async-start(bf16[4,64,256]{2,1,0:T(8,128)(2,1)} %bitcast.6), calls=%async_computation | async-start | bytes 262144 | tf_op jit(solution)/shard_map/all_to_all | solution.py:416
  92.7 71.1 %copy-start.12 = (bf16[1,384,2048]{2,1,0:T(8,128)(2,1)S(1)}, bf16[1,384,2048]{2,1,0:T(8,128)(2,1)}, u32[]{:S(2)}) copy-start(bf16[1,384,2048]{2,1,0:T(8,128)(2,1)} %param.24) | copy-start | bytes 4718596
  95.9 68.0 %copy-start.5 = (bf16[64,2048]{1,0:T(8,128)(2,1)}, bf16[64,2048]{1,0:T(8,128)(2,1)S(1)}, u32[]{:S(2)}) copy-start(bf16[64,2048]{1,0:T(8,128)(2,1)S(1)} %get-tuple-element.19.mid_ref) | copy-start | bytes 786436
  95.9 68.0 %copy-start.7 = (bf16[64,2048]{1,0:T(8,128)(2,1)}, bf16[64,2048]{1,0:T(8,128)(2,1)S(1)}, u32[]{:S(2)}) copy-start(bf16[64,2048]{1,0:T(8,128)(2,1)S(1)} %get-tuple-element.18.normed_ref) | copy-start | bytes 786436
  95.9 68.0 %copy-start.10 = (bf16[1,2048,384]{2,1,0:T(8,128)(2,1)S(1)}, bf16[1,2048,384]{2,1,0:T(8,128)(2,1)}, u32[]{:S(2)}) copy-start(bf16[1,2048,384]{2,1,0:T(8,128)(2,1)} %param.22) | copy-start | bytes 4718596
  95.9 68.0 %copy-start.11 = (bf16[1,2048,384]{2,1,0:T(8,128)(2,1)S(1)}, bf16[1,2048,384]{2,1,0:T(8,128)(2,1)}, u32[]{:S(2)}) copy-start(bf16[1,2048,384]{2,1,0:T(8,128)(2,1)} %param.23) | copy-start | bytes 4718596
  169.6 56.8 %all-to-all-start.2 = ((bf16[64,8,2048]{2,1,0:T(8,128)(2,1)}), bf16[64,8,2048]{2,1,0:T(8,128)(2,1)S(1)}, u32[]{:S(2)}, u32[]{:S(2)}) async-start(bf16[64,8,2048]{2,1,0:T(8,128)(2,1)} %bitcast.35), calls=%async_computation.2 | async-start | bytes 4194304 | tf_op jit(solution)/shard_map/all_to_all | solution.py:434
  (12 other events, 52.5 us)

commit v5 on v4

--- a/solution.py
+++ b/solution.py
@@ -318,17 +318,13 @@
 
 
 def project_kernel(
-    at_ref, heads_ref, w0, w1, far0, far1, w3, stream_ref, gain_ref, slots_ref, mid_ref, normed_ref, out_ref
+    at_ref, heads_ref, w0, w1, w2, w3, stream_ref, gain_ref, slots_ref, mid_ref, normed_ref, out_ref
 ):
     own, count = at_ref[3], heads_ref.shape[0]
     attended = jnp.zeros(stream_ref.shape, jnp.float32)
-    for k, weight in ((0, w0), (1, w1), (3, w3)):
+    for k, weight in enumerate((w0, w1, w2, w3)):
         heads = heads_ref[(own + count - k) % count]
         attended += jnp.dot(heads, weight[...], preferred_element_type=jnp.float32)
-    heads = heads_ref[(own + count - 2) % count]
-    half = far0.shape[0]
-    attended += jnp.dot(heads[:, :half], far0[...], preferred_element_type=jnp.float32)
-    attended += jnp.dot(heads[:, half:], far1[...], preferred_element_type=jnp.float32)
     mid = (stream_ref[...].astype(jnp.float32) + attended).astype(jnp.bfloat16)
     mid_ref[...] = mid
     wide = mid.astype(jnp.float32)
@@ -397,10 +393,8 @@
     at = jnp.stack([lax.axis_index(axis) for axis in SP_TP])
     weight_below = shifted(out_weight, "tp", 1)
     weight_above = shifted(out_weight, "tp", -1)
-    half = out_weight.shape[0] // 2
-    far0 = shifted(weight_below[:half], "tp", 1)
-    far1 = shifted(weight_above[half:], "tp", -1)
-    out_weights = (out_weight, weight_below, far0, far1, weight_above)
+    weight_far = shifted(weight_below, "tp", 1)
+    out_weights = (out_weight, weight_below, weight_far, weight_above)
     own_rows = stream.shape[0]
     expert_count = lax.axis_size(SP) * expert_gate.shape[0]
     capacity = 2 * own_rows * TOP_K // expert_count

time: 229 us -> 225 us (0.983)
  starting transfers between devices: 39.3 us -> 35.5 us
    ppermute x18 -> x17, starting transfers between devices: 26 us -> 22.8 us  [shifted(): lax.ppermute(value, axis, [(i, (i + step) % size) for i in range(size)])]
    ppermute x4, waiting for transfers between devices: 16.5 us -> 19.2 us  [counter_shifted(): return lax.ppermute(value, ('sp_0', 'sp_2'), pairs)]
    ppermute x18 -> x17, waiting for transfers between devices: 14.8 us -> 12.7 us  [shifted(): lax.ppermute(value, axis, [(i, (i + step) % size) for i in range(size)])]
    unnamed x43 -> x35, local copies, waits for them, and re-layouts: 8.56 us -> 9.95 us
  transfers between devices with their start and end apart: 24 -> 23, of which waited for: 11 -> 11; matrix products, arithmetic and copies ran while one was open for 4% -> 3% of each run, Pallas kernels for 5% -> 5%
where the time goes in v5:
time: 225 us
  waiting for transfers between devices  82.1 us (36%)
  blocking collectives  67.4 us (30%)
  starting transfers between devices  35.5 us (16%)
  Pallas kernels  21.8 us (10%)
  local copies, waits for them, and re-layouts  16 us (7%)
    all_to_all x1, blocking collectives, per_device(): arrived = lax.all_to_all(outgoing.reshape(exchange), SP, 0, 0, tiled=True)  67.4 us
    all_to_all x1, waiting for transfers between devices, per_device(): returned = lax.all_to_all(produced.reshape(exchange), SP, 0, 0, tiled=True)  45.4 us
    ppermute x17, starting transfers between devices, shifted(): lax.ppermute(value, axis, [(i, (i + step) % size) for i in range(size)])  22.8 us
    pallas_call x11, Pallas kernels, call(): pl.pallas_call(kernel, out_shape=[jax.ShapeDtypeStruct(*out) for out in o...  21.8 us
    ppermute x4, waiting for transfers between devices, counter_shifted(): return lax.ppermute(value, ('sp_0', 'sp_2'), pairs)  19.2 us
    ppermute x17, waiting for transfers between devices, shifted(): lax.ppermute(value, axis, [(i, (i + step) % size) for i in range(size)])  12.7 us
    unnamed x35, local copies, waits for them, and re-layouts  9.95 us
    all_to_all x1, starting transfers between devices, per_device(): returned = lax.all_to_all(produced.reshape(exchange), SP, 0, 0, tiled=True)  5.56 us
  transfers between devices with their start and end apart: 23, of which 11 were waited for; matrix products, arithmetic and copies ran while one was open for 3% of the time, Pallas kernels for 5%

profile of v5, /device:TPU:8, one launch (start us, length us, event | category | flops | bytes accessed | tf_op | source)
XLA Modules:
  0.0 224.5 jit_solution(3417098002728771931)
XLA Ops:
  1.8 2.2 collective-permute-start.1
  4.1 3.1 %collective-permute-done.1 = bf16[256,256]{1,0:T(8,128)(2,1)S(1)} collective-permute-done((bf16[256,256]{1,0:T(8,128)(2,1)S(1)}, bf16[256,256]{1,0:T(8,128)(2,1)S(1)}, u32[]{:S(2)}, u32[]{:S(2)}) %collective-permute-start.1) | collective-permute-done | bytes 131104 | tf_op jit(solution)/shard_map/ppermute | solution.py:26
  7.4 1.4 collective-permute-done.2.other_ref
  9.4 2.0 collective-permute-start.3
  11.4 1.5 collective-permute-start.18
  12.9 9.7 %collective-permute-done.3.refs_0_ = bf16[4,256,256]{2,1,0:T(8,128)(2,1)} collective-permute-done((bf16[4,256,256]{2,1,0:T(8,128)(2,1)S(1)}, bf16[4,256,256]{2,1,0:T(8,128)(2,1)}, u32[]{:S(2)}, u32[]{:S(2)}) %collective-permute-start.3) | collective-permute-done | bytes 524320 | tf_op jit(solution)/shard_map/ppermute | solution.py:33
  23.4 1.6 collective-permute-start.5
  25.4 1.6 collective-permute-start
  29.1 1.4 eq.25
  31.6 2.6 %collective-permute-start.20 = (bf16[256,2048]{1,0:T(8,128)(2,1)S(1)}, bf16[256,2048]{1,0:T(8,128)(2,1)}, u32[]{:S(2)}, u32[]{:S(2)}) collective-permute-start(bf16[256,2048]{1,0:T(8,128)(2,1)S(1)} %copy-done.4), channel_id=1, source_target_pairs={{0,3},{1,0},{2,1},{3,2},{4,7},{5,4},{6,5},{7,6},{8,11},{9,8},{10,9... | collective-permute-start | bytes 3145736 | tf_op jit(solution)/shard_map/ppermute | solution.py:26
  34.9 2.3 %collective-permute-start.8 = (bf16[2,256,256]{2,1,0:T(8,128)(2,1)S(1)}, bf16[2,256,256]{2,1,0:T(8,128)(2,1)S(1)}, u32[]{:S(2)}, u32[]{:S(2)}) collective-permute-start(bf16[2,256,256]{2,1,0:T(8,128)(2,1)S(1)} %get-tuple-element.28), channel_id=1, source_target_pairs={{0,8},{8,16},{16,24},{24,0},{1,9},{9,17},{17,25},{25,1},{2,10},{10... | collective-permute-start | bytes 786440 | tf_op jit(solution)/shard_map/ppermute | solution.py:26
  38.8 2.7 %shard_map.137.refs_4_ = f32[2,512,128]{2,1,0:T(8,128)S(1)} custom-call(s32[4]{0:T(128)S(1)} %pad_add_fusion.at_ref, bf16[256,256]{1,0:T(8,128)(2,1)S(1)} %copy-done.12, bf16[256,256]{1,0:T(8,128)(2,1)} %collective-permute-done.other_ref, bf16[4,256,256]{2,1,0:T(8,128)(2,1)S(1)} %shard_map.136.part_ref, bf16[2,256,256]{2,1,0:T(8,128)(2,1)S(1)} %copy-done.11, ...), custom_call_target="tpu_custom_call" | custom-call | flops 1073741824 | bytes 1048576 | tf_op jit(solution)/shard_map/pallas_call | solution.py:38
  41.8 2.3 %collective-permute-done.8.refs_1_ = bf16[2,256,256]{2,1,0:T(8,128)(2,1)S(1)} collective-permute-done((bf16[2,256,256]{2,1,0:T(8,128)(2,1)S(1)}, bf16[2,256,256]{2,1,0:T(8,128)(2,1)S(1)}, u32[]{:S(2)}, u32[]{:S(2)}) %collective-permute-start.8) | collective-permute-done | bytes 262176 | tf_op jit(solution)/shard_map/ppermute | solution.py:26
  45.2 1.8 collective-permute-start.16
  48.3 3.8 %collective-permute-done.7.refs_0_ = bf16[4,256,256]{2,1,0:T(8,128)(2,1)S(1)} collective-permute-done((bf16[4,256,256]{2,1,0:T(8,128)(2,1)S(1)}, bf16[4,256,256]{2,1,0:T(8,128)(2,1)S(1)}, u32[]{:S(2)}, u32[]{:S(2)}) %collective-permute-start.7) | collective-permute-done | bytes 524320 | tf_op jit(solution)/shard_map/ppermute | solution.py:33
  52.1 1.5 collective-permute-start.10
  53.6 1.9 collective-permute-start.13
  55.5 1.5 collective-permute-start.14
  58.3 5.7 %collective-permute-done.10.refs_0_ = bf16[4,256,256]{2,1,0:T(8,128)(2,1)S(1)} collective-permute-done((bf16[4,256,256]{2,1,0:T(8,128)(2,1)S(1)}, bf16[4,256,256]{2,1,0:T(8,128)(2,1)S(1)}, u32[]{:S(2)}, u32[]{:S(2)}) %collective-permute-start.10) | collective-permute-done | bytes 524320 | tf_op jit(solution)/shard_map/ppermute | solution.py:33
  64.8 2.6 %collective-permute-start.12 = (bf16[2,256,256]{2,1,0:T(8,128)(2,1)S(1)}, bf16[2,256,256]{2,1,0:T(8,128)(2,1)S(1)}, u32[]{:S(2)}, u32[]{:S(2)}) collective-permute-start(bf16[2,256,256]{2,1,0:T(8,128)(2,1)S(1)} %get-tuple-element.25), channel_id=1, source_target_pairs={{0,24},{8,0},{16,8},{24,16},{1,25},{9,1},{17,9},{25,17},{2,26},{10... | collective-permute-start | bytes 786440 | tf_op jit(solution)/shard_map/ppermute | solution.py:26
  68.7 3.0 %collective-permute-done.11.refs_1_ = bf16[2,256,256]{2,1,0:T(8,128)(2,1)S(1)} collective-permute-done((bf16[2,256,256]{2,1,0:T(8,128)(2,1)S(1)}, bf16[2,256,256]{2,1,0:T(8,128)(2,1)S(1)}, u32[]{:S(2)}, u32[]{:S(2)}) %collective-permute-start.11) | collective-permute-done | bytes 262176 | tf_op jit(solution)/shard_map/ppermute | solution.py:26
  71.7 1.6 collective-permute-done.12.refs_2_
  73.3 2.2 shard_map.141
  78.9 3.5 %all-to-all-start = ((bf16[4,64,256]{2,1,0:T(8,128)(2,1)}), bf16[4,64,256]{2,1,0:T(8,128)(2,1)S(1)}, u32[]{:S(2)}, u32[]{:S(2)}) async-start(bf16[4,64,256]{2,1,0:T(8,128)(2,1)} %bitcast.6), calls=%async_computation | async-start | bytes 262144 | tf_op jit(solution)/shard_map/all_to_all | solution.py:410
  83.4 4.7 %all-to-all-done.heads_ref = bf16[4,64,256]{2,1,0:T(8,128)(2,1)S(1)} async-done(((bf16[4,64,256]{2,1,0:T(8,128)(2,1)}), bf16[4,64,256]{2,1,0:T(8,128)(2,1)S(1)}, u32[]{:S(2)}, u32[]{:S(2)}) %all-to-all-start) | async-done | bytes 131104 | tf_op jit(solution)/shard_map/all_to_all | solution.py:410
  89.1 3.3 %shard_map.143 = (bf16[64,2048]{1,0:T(8,128)(2,1)S(1)}, bf16[64,2048]{1,0:T(8,128)(2,1)S(1)}, bf16[512,2048]{1,0:T(8,128)(2,1)S(1)}) custom-call(s32[4]{0:T(128)S(1)} %pad_add_fusion.at_ref, bf16[4,64,256]{2,1,0:T(8,128)(2,1)S(1)} %all-to-all-done.heads_ref, bf16[256,2048]{1,0:T(8,128)(2,1)S(1)} %copy-done.4, ...), custom_call_target="tpu_custom_call" | custom-call | flops 536870912 | bytes 1048576 | tf_op jit(solution)/shard_map/pallas_call | solution.py:38
  92.5 67.4 %all_to_all.15 = bf16[64,8,2048]{2,1,0:T(8,128)(2,1)S(1)} all-to-all(bf16[64,8,2048]{2,1,0:T(8,128)(2,1)S(1)} %bitcast.36), channel_id=1, replica_groups=mesh['sp_0'=8,'sp_1'=4,'sp_2'=2,'tp'=4] {'sp_0','sp_1','sp_2'}, dimensions={0} | all-to-all | bytes 4194304 | tf_op jit(solution)/shard_map/all_to_all | solution.py:421
  159.9 4.3 %shard_map.145 = bf16[512,2048]{1,0:T(8,128)(2,1)S(1)} custom-call(s32[4]{0:T(128)S(1)} %pad_add_fusion.at_ref, bf16[512,2048]{1,0:T(8,128)(2,1)S(1)} %bitcast.37, bf16[2048,384]{1,0:T(8,128)(2,1)S(1)} %bitcast.39, bf16[2048,384]{1,0:T(8,128)(2,1)S(1)} %bitcast.40, bf16[384,2048]{1,0:T(8,128)(2,1)S(1)} %bitcast.41), custom_call_target="tpu_custom_call" | custom-call | flops 4294967296 | bytes 1048576 | tf_op jit(solution)/shard_map/pallas_call | solution.py:38
  165.5 5.6 %all-to-all-start.2 = ((bf16[64,8,2048]{2,1,0:T(8,128)(2,1)}), bf16[64,8,2048]{2,1,0:T(8,128)(2,1)S(1)}, u32[]{:S(2)}, u32[]{:S(2)}) async-start(bf16[64,8,2048]{2,1,0:T(8,128)(2,1)} %bitcast.35), calls=%async_computation.2 | async-start | bytes 4194304 | tf_op jit(solution)/shard_map/all_to_all | solution.py:428
  175.4 1.5 shard_map.144.base_ref
  177.0 45.4 %all-to-all-done.2 = bf16[64,8,2048]{2,1,0:T(8,128)(2,1)S(1)} async-done(((bf16[64,8,2048]{2,1,0:T(8,128)(2,1)}), bf16[64,8,2048]{2,1,0:T(8,128)(2,1)S(1)}, u32[]{:S(2)}, u32[]{:S(2)}) %all-to-all-start.2) | async-done | bytes 2097184 | tf_op jit(solution)/shard_map/all_to_all | solution.py:428
  222.3 2.2 shard_map.146
  (81 shorter events, 26.2 us)
Async XLA Ops:
  0.0 11.4 %copy-start.4 = (bf16[256,2048]{1,0:T(8,128)(2,1)S(1)}, bf16[256,2048]{1,0:T(8,128)(2,1)}, u32[]{:S(2)}) copy-start(bf16[256,2048]{1,0:T(8,128)(2,1)} %w0.1) | copy-start | bytes 3145732
  0.0 25.4 %copy-start.12 = (bf16[256,256]{1,0:T(8,128)(2,1)S(1)}, bf16[256,256]{1,0:T(8,128)(2,1)}, u32[]{:S(2)}) copy-start(bf16[256,256]{1,0:T(8,128)(2,1)} %own_ref.9) | copy-start | bytes 393220
  0.0 27.0 %copy-start.13 = (s32[64,4]{0,1:T(4,128)S(1)}, s32[64,4]{0,1:T(4,128)}, u32[]{:S(2)}) copy-start(s32[64,4]{0,1:T(4,128)} %param.20) | copy-start | bytes 3076
  1.8 5.3 %collective-permute-start.1 = (bf16[256,256]{1,0:T(8,128)(2,1)S(1)}, bf16[256,256]{1,0:T(8,128)(2,1)S(1)}, u32[]{:S(2)}, u32[]{:S(2)}) collective-permute-start(bf16[256,256]{1,0:T(8,128)(2,1)S(1)} %constant_dynamic-update-slice_fusion), channel_id=1, source_target_pairs={{0,24},{8,0},{16,8},{24,16},{1,25},{9,1},{17,9},{25,17},{2,26},{10... | collective-permute-start | bytes 393224 | tf_op jit(solution)/shard_map/ppermute | solution.py:26
  7.2 1.6 collective-permute-start.2
  9.4 13.2 %collective-permute-start.3 = (bf16[4,256,256]{2,1,0:T(8,128)(2,1)S(1)}, bf16[4,256,256]{2,1,0:T(8,128)(2,1)}, u32[]{:S(2)}, u32[]{:S(2)}) collective-permute-start(bf16[4,256,256]{2,1,0:T(8,128)(2,1)S(1)} %shard_map.136.part_ref), channel_id=1, source_target_pairs={{0,32},{32,64},{64,96},{96,128},{128,160},{160,192},{192,224},{224... | collective-permute-start | bytes 1572872 | tf_op jit(solution)/shard_map/ppermute | solution.py:33
  11.4 30.1 %collective-permute-start.18 = (bf16[256,2048]{1,0:T(8,128)(2,1)S(1)}, bf16[256,2048]{1,0:T(8,128)(2,1)S(1)}, u32[]{:S(2)}, u32[]{:S(2)}) collective-permute-start(bf16[256,2048]{1,0:T(8,128)(2,1)S(1)} %copy-done.4), channel_id=1, source_target_pairs={{0,1},{1,2},{2,3},{3,0},{4,5},{5,6},{6,7},{7,4},{8,9},{9,10},{10,1... | collective-permute-start | bytes 3145736 | tf_op jit(solution)/shard_map/ppermute | solution.py:26
  22.6 19.0 %collective-permute-start.4 = (bf16[4,256,256]{2,1,0:T(8,128)(2,1)}, bf16[4,256,256]{2,1,0:T(8,128)(2,1)S(1)}, u32[]{:S(2)}, u32[]{:S(2)}) collective-permute-start(bf16[4,256,256]{2,1,0:T(8,128)(2,1)} %collective-permute-done.3.refs_0_), channel_id=1, source_target_pairs={{0,32},{32,64},{64,96},{96,128},{128,160},{160,192},{192,224},{224... | collective-permute-start | bytes 1572872 | tf_op jit(solution)/shard_map/ppermute | solution.py:33
  23.4 10.8 %collective-permute-start.5 = (bf16[2,256,256]{2,1,0:T(8,128)(2,1)}, bf16[2,256,256]{2,1,0:T(8,128)(2,1)S(1)}, u32[]{:S(2)}, u32[]{:S(2)}) collective-permute-start(bf16[2,256,256]{2,1,0:T(8,128)(2,1)} %get-tuple-element.30), channel_id=1, source_target_pairs={{0,8},{8,16},{16,24},{24,0},{1,9},{9,17},{17,25},{25,1},{2,10},{10... | collective-permute-start | bytes 786440 | tf_op jit(solution)/shard_map/ppermute | solution.py:26
  25.0 12.3 %collective-permute-start.6 = (bf16[2,256,256]{2,1,0:T(8,128)(2,1)}, bf16[2,256,256]{2,1,0:T(8,128)(2,1)}, u32[]{:S(2)}, u32[]{:S(2)}) collective-permute-start(bf16[2,256,256]{2,1,0:T(8,128)(2,1)} %get-tuple-element.29), channel_id=1, source_target_pairs={{0,24},{8,0},{16,8},{24,16},{1,25},{9,1},{17,9},{25,17},{2,26},{10... | collective-permute-start | bytes 786440 | tf_op jit(solution)/shard_map/ppermute | solution.py:26
  25.4 6.2 %collective-permute-start = (bf16[256,256]{1,0:T(8,128)(2,1)S(1)}, bf16[256,256]{1,0:T(8,128)(2,1)}, u32[]{:S(2)}, u32[]{:S(2)}) collective-permute-start(bf16[256,256]{1,0:T(8,128)(2,1)S(1)} %copy-done.12), channel_id=1, source_target_pairs={{0,4},{4,0},{1,5},{5,1},{2,6},{6,2},{3,7},{7,3},{8,12},{12,8},{9,1... | collective-permute-start | bytes 393224 | tf_op jit(solution)/shard_map/ppermute | solution.py:26
  31.6 51.8 %collective-permute-start.20 = (bf16[256,2048]{1,0:T(8,128)(2,1)S(1)}, bf16[256,2048]{1,0:T(8,128)(2,1)}, u32[]{:S(2)}, u32[]{:S(2)}) collective-permute-start(bf16[256,2048]{1,0:T(8,128)(2,1)S(1)} %copy-done.4), channel_id=1, source_target_pairs={{0,3},{1,0},{2,1},{3,2},{4,7},{5,4},{6,5},{7,6},{8,11},{9,8},{10,9... | collective-permute-start | bytes 3145736 | tf_op jit(solution)/shard_map/ppermute | solution.py:26
  34.9 9.1 %collective-permute-start.8 = (bf16[2,256,256]{2,1,0:T(8,128)(2,1)S(1)}, bf16[2,256,256]{2,1,0:T(8,128)(2,1)S(1)}, u32[]{:S(2)}, u32[]{:S(2)}) collective-permute-start(bf16[2,256,256]{2,1,0:T(8,128)(2,1)S(1)} %get-tuple-element.28), channel_id=1, source_target_pairs={{0,8},{8,16},{16,24},{24,0},{1,9},{9,17},{17,25},{25,1},{2,10},{10... | collective-permute-start | bytes 786440 | tf_op jit(solution)/shard_map/ppermute | solution.py:26
  37.3 7.9 %collective-permute-start.9 = (bf16[2,256,256]{2,1,0:T(8,128)(2,1)S(1)}, bf16[2,256,256]{2,1,0:T(8,128)(2,1)S(1)}, u32[]{:S(2)}, u32[]{:S(2)}) collective-permute-start(bf16[2,256,256]{2,1,0:T(8,128)(2,1)S(1)} %get-tuple-element.27), channel_id=1, source_target_pairs={{0,24},{8,0},{16,8},{24,16},{1,25},{9,1},{17,9},{25,17},{2,26},{10... | collective-permute-start | bytes 786440 | tf_op jit(solution)/shard_map/ppermute | solution.py:26
  41.5 41.9 %collective-permute-start.19 = (bf16[256,2048]{1,0:T(8,128)(2,1)S(1)}, bf16[256,2048]{1,0:T(8,128)(2,1)}, u32[]{:S(2)}, u32[]{:S(2)}) collective-permute-start(bf16[256,2048]{1,0:T(8,128)(2,1)S(1)} %collective-permute-done.18.w1), channel_id=1, source_target_pairs={{0,1},{1,2},{2,3},{3,0},{4,5},{5,6},{6,7},{7,4},{8,9},{9,10},{10,1... | collective-permute-start | bytes 3145736 | tf_op jit(solution)/shard_map/ppermute | solution.py:26
  41.6 10.5 %collective-permute-start.7 = (bf16[4,256,256]{2,1,0:T(8,128)(2,1)S(1)}, bf16[4,256,256]{2,1,0:T(8,128)(2,1)S(1)}, u32[]{:S(2)}, u32[]{:S(2)}) collective-permute-start(bf16[4,256,256]{2,1,0:T(8,128)(2,1)S(1)} %collective-permute-done.4.refs_0_), channel_id=1, source_target_pairs={{0,32},{32,64},{64,96},{96,128},{128,160},{160,192},{192,224},{224... | collective-permute-start | bytes 1572872 | tf_op jit(solution)/shard_map/ppermute | solution.py:33
  44.1 9.6 %collective-permute-start.15 = (bf16[2,256,256]{2,1,0:T(8,128)(2,1)S(1)}, bf16[2,256,256]{2,1,0:T(8,128)(2,1)S(1)}, u32[]{:S(2)}, u32[]{:S(2)}) collective-permute-start(bf16[2,256,256]{2,1,0:T(8,128)(2,1)S(1)} %get-tuple-element.22), channel_id=1, source_target_pairs={{0,8},{8,16},{16,24},{24,0},{1,9},{9,17},{17,25},{25,1},{2,10},{10... | collective-permute-start | bytes 786440 | tf_op jit(solution)/shard_map/ppermute | solution.py:26
  45.2 10.3 %collective-permute-start.16 = (bf16[2,256,256]{2,1,0:T(8,128)(2,1)S(1)}, bf16[2,256,256]{2,1,0:T(8,128)(2,1)S(1)}, u32[]{:S(2)}, u32[]{:S(2)}) collective-permute-start(bf16[2,256,256]{2,1,0:T(8,128)(2,1)S(1)} %get-tuple-element.21), channel_id=1, source_target_pairs={{0,24},{8,0},{16,8},{24,16},{1,25},{9,1},{17,9},{25,17},{2,26},{10... | collective-permute-start | bytes 786440 | tf_op jit(solution)/shard_map/ppermute | solution.py:26
  52.1 11.9 %collective-permute-start.10 = (bf16[4,256,256]{2,1,0:T(8,128)(2,1)S(1)}, bf16[4,256,256]{2,1,0:T(8,128)(2,1)S(1)}, u32[]{:S(2)}, u32[]{:S(2)}) collective-permute-start(bf16[4,256,256]{2,1,0:T(8,128)(2,1)S(1)} %collective-permute-done.7.refs_0_), channel_id=1, source_target_pairs={{0,32},{32,64},{64,96},{96,128},{128,160},{160,192},{192,224},{224... | collective-permute-start | bytes 1572872 | tf_op jit(solution)/shard_map/ppermute | solution.py:33
  53.6 11.2 %collective-permute-start.13 = (bf16[2,256,256]{2,1,0:T(8,128)(2,1)S(1)}, bf16[2,256,256]{2,1,0:T(8,128)(2,1)S(1)}, u32[]{:S(2)}, u32[]{:S(2)}) collective-permute-start(bf16[2,256,256]{2,1,0:T(8,128)(2,1)S(1)} %get-tuple-element.24), channel_id=1, source_target_pairs={{0,8},{8,16},{16,24},{24,0},{1,9},{9,17},{17,25},{25,1},{2,10},{10... | collective-permute-start | bytes 786440 | tf_op jit(solution)/shard_map/ppermute | solution.py:26
  55.5 11.9 %collective-permute-start.14 = (bf16[2,256,256]{2,1,0:T(8,128)(2,1)S(1)}, bf16[2,256,256]{2,1,0:T(8,128)(2,1)S(1)}, u32[]{:S(2)}, u32[]{:S(2)}) collective-permute-start(bf16[2,256,256]{2,1,0:T(8,128)(2,1)S(1)} %get-tuple-element.23), channel_id=1, source_target_pairs={{0,24},{8,0},{16,8},{24,16},{1,25},{9,1},{17,9},{25,17},{2,26},{10... | collective-permute-start | bytes 786440 | tf_op jit(solution)/shard_map/ppermute | solution.py:26
  64.0 7.7 %collective-permute-start.11 = (bf16[2,256,256]{2,1,0:T(8,128)(2,1)S(1)}, bf16[2,256,256]{2,1,0:T(8,128)(2,1)S(1)}, u32[]{:S(2)}, u32[]{:S(2)}) collective-permute-start(bf16[2,256,256]{2,1,0:T(8,128)(2,1)S(1)} %get-tuple-element.26), channel_id=1, source_target_pairs={{0,8},{8,16},{16,24},{24,0},{1,9},{9,17},{17,25},{25,1},{2,10},{10... | collective-permute-start | bytes 786440 | tf_op jit(solution)/shard_map/ppermute | solution.py:26
  64.8 8.5 %collective-permute-start.12 = (bf16[2,256,256]{2,1,0:T(8,128)(2,1)S(1)}, bf16[2,256,256]{2,1,0:T(8,128)(2,1)S(1)}, u32[]{:S(2)}, u32[]{:S(2)}) collective-permute-start(bf16[2,256,256]{2,1,0:T(8,128)(2,1)S(1)} %get-tuple-element.25), channel_id=1, source_target_pairs={{0,24},{8,0},{16,8},{24,16},{1,25},{9,1},{17,9},{25,17},{2,26},{10... | collective-permute-start | bytes 786440 | tf_op jit(solution)/shard_map/ppermute | solution.py:26
  68.7 6.8 %copy-start.14 = (s32[2,128]{1,0:T(2,128)S(1)}, s32[2,128]{1,0:T(2,128)}, u32[]{:S(2)}) copy-start(s32[2,128]{1,0:T(2,128)} %eq.29) | copy-start | bytes 3076
  75.5 12.7 %copy-start.6 = (f32[2048]{0:T(1024)S(1)}, f32[2048]{0:T(1024)}, u32[]{:S(2)}) copy-start(f32[2048]{0:T(1024)} %param.19) | copy-start | bytes 24580
  75.5 2.1 collective-permute-start.17
  78.9 9.3 %all-to-all-start = ((bf16[4,64,256]{2,1,0:T(8,128)(2,1)}), bf16[4,64,256]{2,1,0:T(8,128)(2,1)S(1)}, u32[]{:S(2)}, u32[]{:S(2)}) async-start(bf16[4,64,256]{2,1,0:T(8,128)(2,1)} %bitcast.6), calls=%async_computation | async-start | bytes 262144 | tf_op jit(solution)/shard_map/all_to_all | solution.py:410
  89.1 70.7 %copy-start.9 = (bf16[1,384,2048]{2,1,0:T(8,128)(2,1)S(1)}, bf16[1,384,2048]{2,1,0:T(8,128)(2,1)}, u32[]{:S(2)}) copy-start(bf16[1,384,2048]{2,1,0:T(8,128)(2,1)} %param.24) | copy-start | bytes 4718596
  92.5 67.4 %copy-start.7 = (bf16[1,2048,384]{2,1,0:T(8,128)(2,1)S(1)}, bf16[1,2048,384]{2,1,0:T(8,128)(2,1)}, u32[]{:S(2)}) copy-start(bf16[1,2048,384]{2,1,0:T(8,128)(2,1)} %param.22) | copy-start | bytes 4718596
  92.5 67.4 %copy-start.8 = (bf16[1,2048,384]{2,1,0:T(8,128)(2,1)S(1)}, bf16[1,2048,384]{2,1,0:T(8,128)(2,1)}, u32[]{:S(2)}) copy-start(bf16[1,2048,384]{2,1,0:T(8,128)(2,1)} %param.23) | copy-start | bytes 4718596
  165.5 5.6 %copy-start.15 = (f32[64,4]{0,1:T(4,128)S(1)}, f32[64,4]{0,1:T(4,128)}, u32[]{:S(2)}) copy-start(f32[64,4]{0,1:T(4,128)} %param.21) | copy-start | bytes 3076
  165.5 56.8 %all-to-all-start.2 = ((bf16[64,8,2048]{2,1,0:T(8,128)(2,1)}), bf16[64,8,2048]{2,1,0:T(8,128)(2,1)S(1)}, u32[]{:S(2)}, u32[]{:S(2)}) async-start(bf16[64,8,2048]{2,1,0:T(8,128)(2,1)} %bitcast.35), calls=%async_computation.2 | async-start | bytes 4194304 | tf_op jit(solution)/shard_map/all_to_all | solution.py:428
  (7 other events, 8.2 us)
